TPU v7x, 512 devices: a whole 4x8x8 slice. The times are simulated.
512 devices in a mesh: sp: 32 (over z, x), tp: 16 (over y, core).
Axes of the slice: x: 4, y: 8, z: 8, core: 2. Of those that a mesh axis runs over, the one named last changes fastest.
Arguments:
- skip_stream_entering: bfloat16 [4096, 2048], P('sp', 'tp'), may hold values from -24 to 24
- unfiltered_channel_feed: bfloat16 [4096, 2048], P('sp', 'tp'), may hold values from -6 to 6
- unfiltered_state_entry: bfloat16 [4096, 2048], P('sp', 'tp'), may hold values from -6 to 6
- unfiltered_state_exit: bfloat16 [4096, 2048], P('sp', 'tp'), may hold values from -6 to 6
- final_valve_preactivation: bfloat16 [4096, 2048], P('sp', 'tp'), may hold values from -6 to 6
- increment_preactivation: float32 [2, 32, 4096], P(None, 'tp', 'sp'), may hold values from -8 to 8
- summed_attenuation_both_ways: float32 [2, 32, 4096], P(None, 'tp', 'sp'), may hold values from -0.7 to 0, as said below
- channel_fading_speed: float32 [2, 32], P(None, 'tp'), may hold values from 4.8828125e-05 to 0.03, as said below
- channel_feed_filter: float32 [5, 2048], P(None, 'tp'), may hold values from -2.5 to 2.5
- state_entry_filter: float32 [5, 2048], P(None, 'tp'), may hold values from -2.5 to 2.5
- state_exit_filter: float32 [5, 2048], P(None, 'tp'), may hold values from -2.5 to 2.5
- clustered_rescale_factor: float32 [2048], P('tp'), may hold values from 0.1 to 1.9
- final_projection_weights: bfloat16 [2048, 2048], P(None, 'tp'), may hold values from -0.125 to 0.125
- specialist_rescale_factor: float32 [2048], replicated, may hold values from 0.1 to 1.9
- item_specialist_couple: int32 [4096, 2], P('sp'), may hold values from 0 to 31, all different within a row; in each aligned block of 128 rows (0 to 127, 128 to 255, ...) at most 16 rows name the same one
- selected_cluster_likelihood: float32 [4096], P('sp'), may hold values from 0.3 to 1
- selected_twin_scores_raw: float32 [4096, 2], P('sp'), may hold values from -6 to 6
- specialist_gating_weights: bfloat16 [32, 2048, 4096], P('sp', None, 'tp'), may hold values from -0.125 to 0.125
- specialist_raising_weights: bfloat16 [32, 2048, 4096], P('sp', None, 'tp'), may hold values from -0.125 to 0.125
- specialist_lowering_weights: bfloat16 [32, 4096, 2048], P('sp', 'tp'), may hold values from -0.09375 to 0.09375
Outputs:
- layer_out: bfloat16 [4096, 2048], P('sp', 'tp')
Inputs may be any that keep to these rules, and one draw needn't show every extreme that they name: For every head, dt times channel_fading_speed at the rate of the draw sets how far a state is carried; summed_attenuation_both_ways holds a few sharp losses of state. `summed_attenuation_both_ways`: mostly zero. `item_specialist_couple`: the two experts of a row differ. Among the rows of one index of sp (aligned blocks of 128 rows) no expert is named by more than 16 rows, a bound that some expert reaches in some blocks.
All inputs are finite; a program needn't handle non-finite values.
Results may differ from a plain program's by a relative error of at most 0.0095.
Values may be sent and summed in bfloat16 or wider, within the bound.
No kernel may reach another device: no remote copies, remote signals or barrier semaphores. Data moves between devices by JAX's collectives and lax.ppermute only.
A program may use at most 64 MiB of HBM per device.

v0:
```python
import jax
import jax.numpy as jnp
from jax import lax
from jax.sharding import Mesh
from jax.sharding import PartitionSpec as P

D = 2048
HD = 64
NS = 128
CONV = 5
SP = ("sp_0", "sp_1")


HIGHEST = lax.Precision.HIGHEST
group_eps = 1e-05
stream_eps = 1e-06


def extended(cells, sides, width):
    for axis, dim in sides:
        count = lax.axis_size(axis)
        ends = count - 1
        head = lax.slice_in_dim(cells, 0, width, axis=dim)
        tail = lax.slice_in_dim(cells, cells.shape[dim] - width, cells.shape[dim], axis=dim)
        cells = jnp.concatenate(
            [
                lax.ppermute(tail, axis, [(i, (i + 1) % count) for i in range(ends)]),
                cells,
                lax.ppermute(head, axis, [((i + 1) % count, i) for i in range(ends)]),
            ],
            axis=dim,
        )
    return cells


def filled_with(shard, identity):
    return jax.tree.map(
        lambda a, e: jnp.broadcast_to(jnp.asarray(e, a.dtype), a.shape), shard, identity
    )


def all_in_one(shard, axis):
    leaves = jax.tree.leaves(shard)
    sequence = sorted(range(len(leaves)), key=lambda k: -leaves[k].size)
    width = (1, *leaves[sequence[0]].shape)[-1]
    lines = [
        jnp.pad(leaves[k].reshape(-1), (0, -leaves[k].size % width)).reshape(-1, width)
        for k in sequence
    ]
    both, at, found = (lax.all_gather(jnp.concatenate(lines), axis), 0, {})
    for k, line in zip(sequence, lines):
        share = both[:, at : at + len(line)].reshape(len(both), -1)
        found[k] = share[:, : leaves[k].size].reshape(-1, *leaves[k].shape)
        at += len(line)
    numbers = iter(range(len(leaves)))
    return jax.tree.map(lambda _: found[next(numbers)], shard)


def carried_in(shard, axes, combine, identity, reverse):
    before = start = filled_with(shard, identity)
    so_far = shard
    for axis in reversed(axes):
        peers, mine = (lax.axis_size(axis), lax.axis_index(axis))
        pieces = all_in_one(
            jax.tree.map(
                lambda part, kind: part.astype(kind), so_far, (jnp.bfloat16, jnp.bfloat16)
            ),
            axis,
        )
        inside, so_far = (start, start)
        for k in reversed(range(peers)) if reverse else range(peers):
            passed = k > mine if reverse else k < mine
            so_far = combine(
                so_far, jax.tree.map(lambda part, own: part[k].astype(own.dtype), pieces, shard)
            )
            inside = jax.tree.map(lambda new, old: jnp.where(passed, new, old), so_far, inside)
        before = combine(inside, before)
    return before


def in_blocks(shard, dim, peers):
    shape = shard.shape
    parts = shard.reshape(*shape[:dim], peers, shape[dim] // peers, *shape[dim + 1 :])
    return jnp.moveaxis(parts, dim, 0)


def sum_at_owner(shard, axis, dim):
    peers = lax.axis_size(axis)
    parts = lax.all_to_all(in_blocks(shard, dim, peers), axis, 0, 0, tiled=True)
    return jnp.sum(parts.astype(jnp.float32), axis=0)


def block_parts(x_short, b_short, c_short, step_f, step_b, log_f, log_b):
    head_count = x_short.shape[1]
    group_count = b_short.shape[1]
    per_group = head_count // group_count
    length = x_short.shape[0]
    group_scores = jnp.einsum("tgn,sgn->gts", c_short, b_short, preferred_element_type=jnp.float32)
    x_block = x_short.astype(jnp.float32)
    b_block = b_short.astype(jnp.float32)
    c_block = c_short.astype(jnp.float32)
    scores = jnp.repeat(group_scores, per_group, axis=0)
    b_head = jnp.repeat(b_block, per_group, axis=1)
    c_head = jnp.repeat(c_block, per_group, axis=1)
    forward = jnp.cumsum(log_f, axis=1)
    backward = jnp.flip(jnp.cumsum(jnp.flip(log_b, 1), axis=1), 1)
    row_index = lax.broadcasted_iota(jnp.int32, (length, length), 0)
    col_index = lax.broadcasted_iota(jnp.int32, (length, length), 1)
    lower_mask = (col_index <= row_index)[None]
    upper_mask = (col_index >= row_index)[None]
    decay_fwd = jnp.where(
        lower_mask, jnp.exp(jnp.minimum(forward[:, :, None] - forward[:, None, :], 0.0)), 0.0
    )
    decay_bwd = jnp.where(
        upper_mask, jnp.exp(jnp.minimum(backward[:, :, None] - backward[:, None, :], 0.0)), 0.0
    )
    mixing = scores * (decay_fwd * step_f[:, None, :] + decay_bwd * step_b[:, None, :])
    within = jnp.einsum("hts,shp->thp", mixing, x_block, precision=HIGHEST)
    weight_fwd = jnp.exp(forward[:, -1:] - forward) * step_f
    weight_bwd = jnp.exp(backward[:, :1] - backward) * step_b
    state_fwd = jnp.einsum("hs,shp,shn->hpn", weight_fwd, x_block, b_head, precision=HIGHEST)
    state_bwd = jnp.einsum("hs,shp,shn->hpn", weight_bwd, x_block, b_head, precision=HIGHEST)
    return (
        within,
        state_fwd,
        state_bwd,
        forward[:, -1],
        backward[:, 0],
        jnp.exp(forward),
        jnp.exp(backward),
        c_head,
    )


def read_state(c_head, factor, state):
    return (
        jnp.einsum("thn,hpn->thp", c_head, state, precision=HIGHEST)
        * jnp.transpose(factor)[:, :, None]
    )


def compose(earlier, later):
    return (earlier[0] + later[0], earlier[1] * jnp.exp(later[0])[:, None, None] + later[1])


def body(
    skip_stream_entering,
    unfiltered_channel_feed,
    unfiltered_state_entry,
    unfiltered_state_exit,
    final_valve_preactivation,
    increment_preactivation,
    summed_attenuation_both_ways,
    channel_fading_speed,
    channel_feed_filter,
    state_entry_filter,
    state_exit_filter,
    clustered_rescale_factor,
    final_projection_weights,
    specialist_rescale_factor,
    item_specialist_couple,
    selected_cluster_likelihood,
    selected_twin_scores_raw,
    specialist_gating_weights,
    specialist_raising_weights,
    specialist_lowering_weights,
):
    tokens_here = skip_stream_entering.shape[0]
    heads_here = increment_preactivation.shape[1]
    x_width = unfiltered_channel_feed.shape[1]
    b_width = unfiltered_state_entry.shape[1]
    groups_here = b_width // NS
    joined = jnp.concatenate(
        [unfiltered_channel_feed, unfiltered_state_entry, unfiltered_state_exit], axis=1
    )
    padded = extended(joined, ((SP, 0),), CONV // 2)
    kernel = jnp.concatenate([channel_feed_filter, state_entry_filter, state_exit_filter], axis=1)
    summed = jnp.zeros(joined.shape, jnp.float32)
    for offset in range(CONV):
        summed = summed + kernel[offset] * padded[offset : offset + tokens_here].astype(jnp.float32)
    conv_out = jax.nn.silu(summed).astype(jnp.bfloat16)
    x_conv = conv_out[:, :x_width].reshape(tokens_here, heads_here, HD)
    b_conv = conv_out[:, x_width : x_width + b_width].reshape(tokens_here, groups_here, NS)
    c_conv = conv_out[:, x_width + b_width :].reshape(tokens_here, groups_here, NS)
    whole_increment_list = jax.nn.softplus(increment_preactivation)
    whole_attenuation_list = (
        -whole_increment_list * channel_fading_speed[:, :, None] + summed_attenuation_both_ways
    )
    within, state_fwd, state_bwd, total_fwd, total_bwd, factor_fwd, factor_bwd, c_head = (
        block_parts(
            x_conv,
            b_conv,
            c_conv,
            whole_increment_list[0],
            whole_increment_list[1],
            whole_attenuation_list[0],
            whole_attenuation_list[1],
        )
    )
    empty = (jnp.zeros_like(total_fwd), jnp.zeros_like(state_fwd))
    incoming_fwd = carried_in((total_fwd, state_fwd), SP, compose, empty, False)[1]
    incoming_bwd = carried_in((total_bwd, state_bwd), SP, compose, empty, True)[1]
    mixer_out = (
        within
        + read_state(c_head, factor_fwd, incoming_fwd)
        + read_state(c_head, factor_bwd, incoming_bwd)
    )
    gated = mixer_out.reshape(tokens_here, x_width) * jax.nn.silu(
        final_valve_preactivation.astype(jnp.float32)
    )
    grouped = gated.reshape(tokens_here, groups_here, -1)
    grouped = grouped * lax.rsqrt(jnp.mean(grouped * grouped, axis=-1, keepdims=True) + group_eps)
    mixed = (grouped.reshape(tokens_here, x_width) * clustered_rescale_factor).astype(jnp.bfloat16)
    projected = jnp.dot(
        lax.all_gather(mixed, "tp", axis=1, tiled=True),
        final_projection_weights,
        preferred_element_type=jnp.float32,
    )
    stream = (skip_stream_entering.astype(jnp.float32) + projected).astype(jnp.bfloat16)
    stream_f = stream.astype(jnp.float32)
    col_count = skip_stream_entering.shape[1]
    whole_rows = lax.all_gather(stream, "tp", axis=1, tiled=True).astype(jnp.float32)
    normal_rows = (
        whole_rows
        * lax.rsqrt(jnp.mean(whole_rows * whole_rows, axis=-1, keepdims=True) + stream_eps)
        * specialist_rescale_factor
    ).astype(jnp.bfloat16)
    expert_total = lax.axis_size(SP)
    capacity = 4 * tokens_here // expert_total
    flat_ids = item_specialist_couple.reshape(-1)
    assignments = flat_ids.shape[0]
    expert_iota = lax.broadcasted_iota(jnp.int32, (assignments, expert_total), 1)
    one_hot = (flat_ids[:, None] == expert_iota).astype(jnp.int32)
    ranking = jnp.sum((jnp.cumsum(one_hot, axis=0) - 1) * one_hot, axis=1)
    slot_index = flat_ids * capacity + ranking
    slot_iota = lax.broadcasted_iota(jnp.int32, (expert_total * capacity, assignments), 0)
    selector = (slot_index[None, :] == slot_iota).astype(jnp.bfloat16)
    selector = jnp.sum(selector.reshape(expert_total * capacity, tokens_here, -1), axis=2)
    weight_gate = specialist_gating_weights[0]
    weight_up = specialist_raising_weights[0]
    weight_down = specialist_lowering_weights[0]
    outgoing = jnp.dot(selector, normal_rows, preferred_element_type=jnp.float32).astype(
        jnp.bfloat16
    )
    outgoing = outgoing.reshape(expert_total, capacity, D)
    arrived = lax.all_to_all(outgoing, SP, split_axis=0, concat_axis=0, tiled=True)
    sources = arrived.shape[0]
    slot_count = arrived.shape[1]
    rows = arrived.reshape(sources * slot_count, arrived.shape[2])
    gate = jnp.dot(rows, weight_gate, preferred_element_type=jnp.float32)
    upward = jnp.dot(rows, weight_up, preferred_element_type=jnp.float32)
    hidden = (jax.nn.silu(gate) * upward).astype(jnp.bfloat16)
    partial_out = jnp.dot(hidden, weight_down, preferred_element_type=jnp.float32).astype(
        jnp.bfloat16
    )
    partial_out = partial_out.reshape(sources, slot_count, partial_out.shape[1])
    expert_cols = sum_at_owner(partial_out, "tp", 2).astype(jnp.bfloat16)
    returned = lax.all_to_all(expert_cols, SP, split_axis=0, concat_axis=0, tiled=True)
    flat_back = returned.reshape(expert_total * capacity, col_count)
    picked = (
        jnp.take(flat_back, slot_index, axis=0)
        .astype(jnp.float32)
        .reshape(tokens_here, -1, col_count)
    )
    first = jax.nn.sigmoid(selected_twin_scores_raw[:, 0] - selected_twin_scores_raw[:, 1])
    route_weight = selected_cluster_likelihood[:, None] * jnp.stack([first, 1.0 - first], axis=1)
    experts_sum = jnp.sum(route_weight[:, :, None] * picked, axis=1)
    return (stream_f + experts_sum).astype(jnp.bfloat16)


def solution(mesh):
    torus = Mesh(mesh.devices.reshape(8, 4, mesh.shape["tp"]), ("sp_0", "sp_1", "tp"))
    return jax.shard_map(
        body,
        mesh=torus,
        in_specs=(
            P(SP, "tp"),
            P(SP, "tp"),
            P(SP, "tp"),
            P(SP, "tp"),
            P(SP, "tp"),
            P(None, "tp", SP),
            P(None, "tp", SP),
            P(None, "tp"),
            P(None, "tp"),
            P(None, "tp"),
            P(None, "tp"),
            P("tp"),
            P(None, "tp"),
            P(),
            P(SP, None),
            P(SP),
            P(SP, None),
            P(SP, None, "tp"),
            P(SP, None, "tp"),
            P(SP, "tp", None),
        ),
        out_specs=P(SP, "tp"),
        check_vma=False,
    )
```

profile of v0, /device:TPU:1, one launch (start us, length us, event | category | flops | bytes accessed | tf_op | source)
XLA Modules:
  0.0 280.2 jit_solution(5651927392031734438)
XLA Ops:
  0.0 0.9 constant_dynamic-update-slice_fusion.5
  0.9 0.8 constant_dynamic-update-slice_fusion.4
  1.6 0.8 constant_dynamic-update-slice_fusion.3
  2.4 3.9 %collective-permute-start = (bf16[2,384]{1,0:T(2,128)(2,1)S(1)}, bf16[2,384]{1,0:T(2,128)(2,1)S(1)}, u32[]{:S(2)}, u32[]{:S(2)}) collective-permute-start(bf16[2,384]{1,0:T(2,128)(2,1)S(1)} %get-tuple-element.47), channel_id=1, source_target_pairs={{0,16},{16,32},{32,48},{48,64},{64,80},{80,96},{96,112},{112,128},... | collective-permute-start | bytes 4616 | tf_op jit(solution)/shard_map/ppermute | solution.py:27
  6.3 1.3 collective-permute-start.1
  7.7 0.8 copy.71
  8.6 0.1 reshape.638
  8.8 0.8 multiply_add_fusion
  9.6 0.3 reduce_window_sum.30
  9.9 0.3 reduce_window_sum.31
  10.3 0.2 slice_reduce_fusion.6
  10.7 0.7 constant_dynamic-update-slice_fusion.2
  11.4 0.7 constant_dynamic-update-slice_fusion.1
  12.1 0.7 constant_dynamic-update-slice_fusion
  12.8 0.6 reduce-window.6
  13.4 0.2 slice_reduce_fusion
  13.7 0.1 reduce_sum.66
  14.0 0.7 compare_and_fusion
  14.8 0.2 multiply_convert_fusion
  15.1 0.2 convolution_convert_fusion.2
  15.4 10.4 %all-gather.6 = bf16[4,129,128]{2,1,0:T(8,128)(2,1)S(1)} all-gather(bf16[1,129,128]{2,1,0:T(8,128)(2,1)S(1)} %maximum_bitcast_fusion.2), channel_id=4, replica_groups=mesh['sp_0'=8,'sp_1'=4,'tp'=16] {'sp_1'}, dimensions={0}, use_global_device_ids=true | all-gather | bytes 165120 | tf_op jit(solution)/shard_map/all_gather | solution.py:50
  26.6 27.4 %all-gather.7 = bf16[8,129,128]{2,1,0:T(8,128)(2,1)S(1)} all-gather(bf16[1,129,128]{2,1,0:T(8,128)(2,1)S(1)} %maximum_bitcast_fusion.3), channel_id=5, replica_groups=mesh['sp_0'=8,'sp_1'=4,'tp'=16] {'sp_0'}, dimensions={0}, use_global_device_ids=true | all-gather | bytes 297216 | tf_op jit(solution)/shard_map/all_gather | solution.py:50
  54.0 0.2 convolution_convert_fusion.3
  54.2 9.1 %all-gather.4 = bf16[4,129,128]{2,1,0:T(8,128)(2,1)S(1)} all-gather(bf16[1,129,128]{2,1,0:T(8,128)(2,1)S(1)} %maximum_bitcast_fusion), channel_id=2, replica_groups=mesh['sp_0'=8,'sp_1'=4,'tp'=16] {'sp_1'}, dimensions={0}, use_global_device_ids=true | all-gather | bytes 165120 | tf_op jit(solution)/shard_map/all_gather | solution.py:50
  64.2 18.5 %all-gather.5 = bf16[8,129,128]{2,1,0:T(8,128)(2,1)S(1)} all-gather(bf16[1,129,128]{2,1,0:T(8,128)(2,1)S(1)} %maximum_bitcast_fusion.1), channel_id=3, replica_groups=mesh['sp_0'=8,'sp_1'=4,'tp'=16] {'sp_0'}, dimensions={0}, use_global_device_ids=true | all-gather | bytes 297216 | tf_op jit(solution)/shard_map/all_gather | solution.py:50
  83.0 0.4 convolution_bitcast_fusion.2
  83.4 0.5 fusion.5
  83.9 0.5 fusion.3
  84.8 37.9 %all_gather.38 = bf16[128,2048]{1,0:T(8,128)(2,1)S(1)} all-gather(bf16[128,128]{1,0:T(8,128)(2,1)S(1)} %multiply_convert_fusion.1), channel_id=1, replica_groups=mesh['sp_0'=8,'sp_1'=4,'tp'=16] {'tp'}, dimensions={1}, use_global_device_ids=true | all-gather | bytes 557056 | tf_op jit(solution)/shard_map/all_gather | solution.py:215
  122.7 0.3 fusion.6
  123.0 16.4 %all_gather.39 = bf16[128,2048]{1,0:T(8,128)(2,1)S(1)} all-gather(bf16[128,128]{1,0:T(8,128)(2,1)S(1)} %fusion.6), channel_id=1, replica_groups=mesh['sp_0'=8,'sp_1'=4,'tp'=16] {'tp'}, dimensions={1}, use_global_device_ids=true | all-gather | bytes 557056 | tf_op jit(solution)/shard_map/all_gather | solution.py:222
  139.4 0.2 fusion.7
  139.6 0.8 convolution_convert_fusion.1
  140.4 55.6 %all_to_all.15 = bf16[32,16,2048]{2,1,0:T(8,128)(2,1)S(1)} all-to-all(bf16[32,16,2048]{2,1,0:T(8,128)(2,1)S(1)} %bitcast.252), channel_id=1, replica_groups=mesh['sp_0'=8,'sp_1'=4,'tp'=16] {'sp_0','sp_1'}, dimensions={0} | all-to-all | bytes 4194304 | tf_op jit(solution)/shard_map/all_to_all | solution.py:246
  196.0 1.5 fusion.12
  197.5 5.0 %fusion = bf16[64,8,16,128]{3,1,2,0:T(8,128)(2,1)} fusion(bf16[1,256,2048]{2,1,0:T(8,128)(2,1)S(1)} %copy-done, bf16[512,2048]{1,0:T(8,128)(2,1)S(1)} %bitcast.256, bf16[1,2048,256]{2,1,0:T(8,128)(2,1)} %param.38, f32[512,256]{1,0:T(8,128)} %fusion.12), kind=kOutput, calls=%fused_computation.4 | convolution fusion | flops 1075576832 | bytes 6815744 | tf_op jit(solution)/shard_map/dot_general | solution.py:253
  202.6 2.2 copy.83
  204.8 1.9 copy.90
  206.7 6.9 %all-to-all-start.1 = ((bf16[16,32,16,128]{3,2,1,0:T(8,128)(2,1)}), bf16[16,32,16,128]{3,2,1,0:T(8,128)(2,1)S(1)}, u32[]{:S(2)}, u32[]{:S(2)}) async-start(bf16[16,32,16,128]{3,2,1,0:T(8,128)(2,1)} %bitcast.251), calls=%async_computation.1 | async-start | bytes 4194304 | tf_op jit(solution)/shard_map/all_to_all | solution.py:89
  213.7 0.1 mul.604
  213.9 0.1 copy.75
  214.2 48.5 %all-to-all-done.1 = bf16[16,32,16,128]{3,2,1,0:T(8,128)(2,1)S(1)} async-done(((bf16[16,32,16,128]{3,2,1,0:T(8,128)(2,1)}), bf16[16,32,16,128]{3,2,1,0:T(8,128)(2,1)S(1)}, u32[]{:S(2)}, u32[]{:S(2)}) %all-to-all-start.1) | async-done | bytes 2097184 | tf_op jit(solution)/shard_map/all_to_all | solution.py:89
  262.6 0.9 reduce_sum.69
  263.6 5.3 %all-to-all-start.2 = ((bf16[32,16,128]{2,1,0:T(8,128)(2,1)}), bf16[32,16,128]{2,1,0:T(8,128)(2,1)S(1)}, u32[]{:S(2)}, u32[]{:S(2)}) async-start(bf16[32,16,128]{2,1,0:T(8,128)(2,1)} %reduce_sum.69), calls=%async_computation.2 | async-start | bytes 262144 | tf_op jit(solution)/shard_map/all_to_all | solution.py:258
  268.9 9.4 %all-to-all-done.2 = bf16[32,16,128]{2,1,0:T(8,128)(2,1)S(1)} async-done(((bf16[32,16,128]{2,1,0:T(8,128)(2,1)}), bf16[32,16,128]{2,1,0:T(8,128)(2,1)S(1)}, u32[]{:S(2)}, u32[]{:S(2)}) %all-to-all-start.2) | async-done | bytes 131104 | tf_op jit(solution)/shard_map/all_to_all | solution.py:258
  278.3 0.9 gather_fusion
  279.2 0.3 multiply_reduce_fusion
  279.6 0.6 add_convert_fusion
  (98 shorter events, 3.4 us)
Async XLA Ops:
  0.0 197.5 %copy-start = (bf16[1,256,2048]{2,1,0:T(8,128)(2,1)S(1)}, bf16[1,256,2048]{2,1,0:T(8,128)(2,1)}, u32[]{:S(2)}) copy-start(bf16[1,256,2048]{2,1,0:T(8,128)(2,1)} %param.39) | copy-start | bytes 3145732
  2.4 12.4 %collective-permute-start = (bf16[2,384]{1,0:T(2,128)(2,1)S(1)}, bf16[2,384]{1,0:T(2,128)(2,1)S(1)}, u32[]{:S(2)}, u32[]{:S(2)}) collective-permute-start(bf16[2,384]{1,0:T(2,128)(2,1)S(1)} %get-tuple-element.47), channel_id=1, source_target_pairs={{0,16},{16,32},{32,48},{48,64},{64,80},{80,96},{96,112},{112,128},... | collective-permute-start | bytes 4616 | tf_op jit(solution)/shard_map/ppermute | solution.py:27
  6.3 8.4 %collective-permute-start.1 = (bf16[2,384]{1,0:T(2,128)(2,1)S(1)}, bf16[2,384]{1,0:T(2,128)(2,1)S(1)}, u32[]{:S(2)}, u32[]{:S(2)}) collective-permute-start(bf16[2,384]{1,0:T(2,128)(2,1)S(1)} %get-tuple-element.48), channel_id=1, source_target_pairs={{16,0},{32,16},{48,32},{64,48},{80,64},{96,80},{112,96},{128,112},... | collective-permute-start | bytes 4616 | tf_op jit(solution)/shard_map/ppermute | solution.py:29
  82.7 1.9 copy-start.2
  82.7 2.0 copy-start.7
  82.7 40.0 %copy-start.1 = (bf16[2048,128]{1,0:T(8,128)(2,1)S(1)}, bf16[2048,128]{1,0:T(8,128)(2,1)}, u32[]{:S(2)}) copy-start(bf16[2048,128]{1,0:T(8,128)(2,1)} %param.32) | copy-start | bytes 1572868
  82.7 40.0 %copy-start.3 = (bf16[128,128]{1,0:T(8,128)(2,1)S(1)}, bf16[128,128]{1,0:T(8,128)(2,1)}, u32[]{:S(2)}) copy-start(bf16[128,128]{1,0:T(8,128)(2,1)} %param.20) | copy-start | bytes 98308
  83.9 55.7 %copy-start.5 = (f32[2048]{0:T(1024)S(1)}, f32[2048]{0:T(1024)}, u32[]{:S(2)}) copy-start(f32[2048]{0:T(1024)} %param.33) | copy-start | bytes 24580
  140.4 55.6 %copy-start.9 = (bf16[1,2048,256]{2,1,0:T(8,128)(2,1)S(1)}, bf16[1,2048,256]{2,1,0:T(8,128)(2,1)}, u32[]{:S(2)}) copy-start(bf16[1,2048,256]{2,1,0:T(8,128)(2,1)} %param.37) | copy-start | bytes 3145732
  206.7 6.9 %copy-start.4 = (s32[128,2]{0,1:T(2,128)S(1)}, s32[128,2]{0,1:T(2,128)}, u32[]{:S(2)}) copy-start(s32[128,2]{0,1:T(2,128)} %param.34) | copy-start | bytes 3076
  206.7 7.3 %copy-start.6 = (f32[128,2]{0,1:T(2,128)S(1)}, f32[128,2]{0,1:T(2,128)}, u32[]{:S(2)}) copy-start(f32[128,2]{0,1:T(2,128)} %param.36) | copy-start | bytes 3076
  206.7 7.4 %copy-start.8 = (f32[128]{0:T(128)S(1)}, f32[128]{0:T(128)}, u32[]{:S(2)}) copy-start(f32[128]{0:T(128)} %param.35) | copy-start | bytes 1540
  206.7 56.0 %all-to-all-start.1 = ((bf16[16,32,16,128]{3,2,1,0:T(8,128)(2,1)}), bf16[16,32,16,128]{3,2,1,0:T(8,128)(2,1)S(1)}, u32[]{:S(2)}, u32[]{:S(2)}) async-start(bf16[16,32,16,128]{3,2,1,0:T(8,128)(2,1)} %bitcast.251), calls=%async_computation.1 | async-start | bytes 4194304 | tf_op jit(solution)/shard_map/all_to_all | solution.py:89
  263.6 14.8 %all-to-all-start.2 = ((bf16[32,16,128]{2,1,0:T(8,128)(2,1)}), bf16[32,16,128]{2,1,0:T(8,128)(2,1)S(1)}, u32[]{:S(2)}, u32[]{:S(2)}) async-start(bf16[32,16,128]{2,1,0:T(8,128)(2,1)} %reduce_sum.69), calls=%async_computation.2 | async-start | bytes 262144 | tf_op jit(solution)/shard_map/all_to_all | solution.py:258
where the time goes:
time: 281 us; the launch traced here: 280 us
  blocking collectives  175 us (62%)
  waiting for transfers between devices  57.9 us (21%)
  starting transfers between devices  17.4 us (6%)
  local copies, waits for them, and re-layouts  13.4 us (5%)
  matrix products  9.61 us (3%)
  other arithmetic  6.01 us (2%)
    all_gather x4, blocking collectives, all_in_one(): both, at, found = (lax.all_gather(jnp.concatenate(lines), axis), 0, {})  65.3 us
    all_to_all x1, blocking collectives, body(): lax.all_to_all(outgoing, SP, split_axis=0, concat_axis=0, tiled=True)  55.6 us
    all_to_all x1, waiting for transfers between devices, sum_at_owner(): parts = lax.all_to_all(in_blocks(shard, dim, peers), axis, 0, 0, tiled=True)  48.5 us
    all_gather x1, blocking collectives, body(): lax.all_gather(mixed, 'tp', axis=1, tiled=True)  37.9 us
    all_gather x1, blocking collectives, body(): lax.all_gather(stream, 'tp', axis=1, tiled=True).astype(jnp.float32)  16.4 us
    all_to_all x1, waiting for transfers between devices, body(): lax.all_to_all(expert_cols, SP, split_axis=0, concat_axis=0, tiled=True)  9.43 us
    all_to_all x1, starting transfers between devices, sum_at_owner(): parts = lax.all_to_all(in_blocks(shard, dim, peers), axis, 0, 0, tiled=True)  6.91 us
    unnamed x30, local copies, waits for them, and re-layouts  6.06 us
  transfers between devices with their start and end apart: 4, of which 2 were waited for; matrix products, arithmetic and copies ran while one was open for 3% of the time, Pallas kernels for 0%

commit v1 on v0

v1 whole, which is shorter than its diff:
```python
import functools

import jax
import jax.numpy as jnp
from jax import lax
from jax.experimental import pallas as pl
from jax.experimental.pallas import tpu as pltpu
from jax.sharding import Mesh
from jax.sharding import PartitionSpec as P

D = 2048
HD = 64
NS = 128
CONV = 5
SP = ("z", "x")
TP = ("y", "c")

HIGHEST = lax.Precision.HIGHEST
group_eps = 1e-05
stream_eps = 1e-06


def extended(cells, width):
    count = lax.axis_size(SP)
    head = cells[:width]
    tail = cells[-width:]
    return jnp.concatenate(
        [
            lax.ppermute(tail, SP, [(i, i + 1) for i in range(count - 1)]),
            cells,
            lax.ppermute(head, SP, [(i + 1, i) for i in range(count - 1)]),
        ],
        axis=0,
    )


def to_all(shard, axis):
    peers = lax.axis_size(axis)
    copies = jnp.broadcast_to(shard[None], (peers, *shard.shape))
    return lax.all_to_all(copies, axis, 0, 0, tiled=True)


def split_pair(value):
    high = value.astype(jnp.bfloat16)
    low = (value - high.astype(jnp.float32)).astype(jnp.bfloat16)
    return high, low


def log_rows(logs):
    high, low = split_pair(logs)
    both = jnp.stack([high, low])[:, :, None]
    rows = jnp.broadcast_to(both, (*both.shape[:2], NS)).reshape(-1, NS)
    return jnp.pad(rows, ((0, 16 - rows.shape[0]), (0, 0)))


def logs_of(rows, heads):
    values = rows[..., : 2 * heads, 0].astype(jnp.float32)
    return values[..., :heads] + values[..., heads:]


def block_parts(x_short, b_short, c_short, step_f, step_b, log_f, log_b):
    head_count = x_short.shape[1]
    length = x_short.shape[0]
    scores = jnp.einsum("tn,sn->ts", c_short, b_short, preferred_element_type=jnp.float32)
    x_block = x_short.astype(jnp.float32)
    b_block = b_short.astype(jnp.float32)
    forward = jnp.cumsum(log_f, axis=1)
    backward = jnp.flip(jnp.cumsum(jnp.flip(log_b, 1), axis=1), 1)
    row_index = lax.broadcasted_iota(jnp.int32, (length, length), 0)
    col_index = lax.broadcasted_iota(jnp.int32, (length, length), 1)
    lower_mask = (col_index <= row_index)[None]
    upper_mask = (col_index >= row_index)[None]
    decay_fwd = jnp.where(
        lower_mask, jnp.exp(jnp.minimum(forward[:, :, None] - forward[:, None, :], 0.0)), 0.0
    )
    decay_bwd = jnp.where(
        upper_mask, jnp.exp(jnp.minimum(backward[:, :, None] - backward[:, None, :], 0.0)), 0.0
    )
    mixing = scores[None] * (decay_fwd * step_f[:, None, :] + decay_bwd * step_b[:, None, :])
    within = jnp.einsum("hts,shp->thp", mixing, x_block, precision=HIGHEST)
    weight_fwd = jnp.exp(forward[:, -1:] - forward) * step_f
    weight_bwd = jnp.exp(backward[:, :1] - backward) * step_b
    state_fwd = jnp.einsum("hs,shp,sn->hpn", weight_fwd, x_block, b_block, precision=HIGHEST)
    state_bwd = jnp.einsum("hs,shp,sn->hpn", weight_bwd, x_block, b_block, precision=HIGHEST)
    return (
        within,
        state_fwd,
        state_bwd,
        forward[:, -1],
        backward[:, 0],
        jnp.exp(forward),
        jnp.exp(backward),
    )


def read_state(c_block, factor, state):
    return (
        jnp.einsum("tn,hpn->thp", c_block, state, precision=HIGHEST)
        * jnp.transpose(factor)[:, :, None]
    )


def shares(logs, place, reverse):
    count = logs.shape[0]
    spot = lax.broadcasted_iota(jnp.int32, (count, 1), 0)
    later = lax.broadcasted_iota(jnp.int32, (count, count), 1)
    each = lax.broadcasted_iota(jnp.int32, (count, count), 0)
    if reverse:
        between = (later < each) & (later > place)
        counts = spot > place
    else:
        between = (later > each) & (later < place)
        counts = spot < place
    passed = jnp.sum(jnp.where(between[:, :, None], logs[None], 0.0), axis=1)
    return jnp.where(counts, jnp.exp(passed), 0.0)


def weighted(factors, states):
    heads = factors.shape[1]
    parts = states.reshape(states.shape[0], heads, HD, NS).astype(jnp.float32)
    return jnp.sum(jnp.where(factors[:, :, None, None] > 0, parts, 0.0) * factors[:, :, None, None], axis=0)


def carried_in(state_fwd, state_bwd, total_fwd, total_bwd):
    heads = total_fwd.shape[0]
    rows = heads * HD
    my_x, my_z = lax.axis_index("x"), lax.axis_index("z")
    count_x, count_z = lax.axis_size("x"), lax.axis_size("z")
    message = jnp.concatenate(
        [
            state_fwd.reshape(rows, NS).astype(jnp.bfloat16),
            state_bwd.reshape(rows, NS).astype(jnp.bfloat16),
            log_rows(total_fwd),
            log_rows(total_bwd),
        ],
        axis=0,
    )
    seen = to_all(message, "x")
    logs_f = logs_of(seen[:, 2 * rows : 2 * rows + 16], heads)
    logs_b = logs_of(seen[:, 2 * rows + 16 : 2 * rows + 32], heads)
    states_f, states_b = seen[:, :rows], seen[:, rows : 2 * rows]
    near_f = weighted(shares(logs_f, my_x, False), states_f)
    near_b = weighted(shares(logs_b, my_x, True), states_b)
    row_f = weighted(shares(logs_f, count_x, False), states_f)
    row_b = weighted(shares(logs_b, -1, True), states_b)
    spot = lax.broadcasted_iota(jnp.int32, (count_x, 1), 0)
    ahead_f = jnp.sum(jnp.where(spot < my_x, logs_f, 0.0), axis=0)
    ahead_b = jnp.sum(jnp.where(spot > my_x, logs_b, 0.0), axis=0)
    out_f = jnp.concatenate(
        [row_f.reshape(rows, NS).astype(jnp.bfloat16), log_rows(jnp.sum(logs_f, axis=0))], axis=0
    )
    out_b = jnp.concatenate(
        [row_b.reshape(rows, NS).astype(jnp.bfloat16), log_rows(jnp.sum(logs_b, axis=0))], axis=0
    )
    far = lax.broadcasted_iota(jnp.int32, (count_z, 1, 1), 0)
    got = lax.all_to_all(jnp.where(far > my_z, out_f[None], out_b[None]), "z", 0, 0, tiled=True)
    logs = logs_of(got[:, rows : rows + 16], heads)
    far_f = weighted(shares(logs, my_z, False), got[:, :rows])
    far_b = weighted(shares(logs, my_z, True), got[:, :rows])
    incoming_f = far_f * jnp.exp(ahead_f)[:, None, None] + near_f
    incoming_b = far_b * jnp.exp(ahead_b)[:, None, None] + near_b
    return incoming_f, incoming_b


def expert_kernel(chunk, rows_ref, gain_ref, gate_ref, up_ref, down_ref, out_ref, normal):
    cores, places = rows_ref.shape[0], rows_ref.shape[1]

    def step(i, carry):
        at = pl.ds(pl.multiple_of(i * chunk, chunk), chunk)
        squares = jnp.zeros((chunk, 128), jnp.float32)
        for y in range(places):
            for c in range(cores):
                part = rows_ref[c, y, at, :].astype(jnp.float32)
                squares = squares + part * part
        scale = lax.rsqrt(jnp.sum(squares, axis=1, keepdims=True) / D + stream_eps)
        for y in range(places):
            for c in range(cores):
                k = y * cores + c
                part = rows_ref[c, y, at, :].astype(jnp.float32)
                normal[:, k * 128 : (k + 1) * 128] = (
                    part * scale * gain_ref[:, k * 128 : (k + 1) * 128]
                ).astype(jnp.bfloat16)
        whole = normal[...]
        gate = jnp.dot(whole, gate_ref[...], preferred_element_type=jnp.float32)
        upward = jnp.dot(whole, up_ref[...], preferred_element_type=jnp.float32)
        hidden = (jax.nn.silu(gate) * upward).astype(jnp.bfloat16)
        for y in range(places):
            k = y * cores
            part = jnp.dot(
                hidden,
                down_ref[:, k * 128 : (k + cores) * 128],
                preferred_element_type=jnp.float32,
            ).astype(jnp.bfloat16)
            for c in range(cores):
                out_ref[c, y, at, :] = part[:, c * 128 : (c + 1) * 128]
        return carry

    lax.fori_loop(0, rows_ref.shape[2] // chunk, step, 0)


def expert(rows, gain, weight_gate, weight_up, weight_down):
    chunk = 256
    full = pl.BlockSpec(memory_space=pltpu.VMEM)
    return pl.pallas_call(
        functools.partial(expert_kernel, chunk),
        out_shape=jax.ShapeDtypeStruct(rows.shape, jnp.bfloat16),
        in_specs=[full] * 5,
        out_specs=full,
        scratch_shapes=[pltpu.VMEM((chunk, D), jnp.bfloat16)],
        name="expert",
    )(rows, gain, weight_gate, weight_up, weight_down)


def body(
    skip_stream_entering,
    unfiltered_channel_feed,
    unfiltered_state_entry,
    unfiltered_state_exit,
    final_valve_preactivation,
    increment_preactivation,
    summed_attenuation_both_ways,
    channel_fading_speed,
    channel_feed_filter,
    state_entry_filter,
    state_exit_filter,
    clustered_rescale_factor,
    final_projection_weights,
    specialist_rescale_factor,
    item_specialist_couple,
    selected_cluster_likelihood,
    selected_twin_scores_raw,
    specialist_gating_weights,
    specialist_raising_weights,
    specialist_lowering_weights,
):
    tokens_here = skip_stream_entering.shape[0]
    heads_here = increment_preactivation.shape[1]
    width = unfiltered_channel_feed.shape[1]
    joined = jnp.concatenate(
        [unfiltered_channel_feed, unfiltered_state_entry, unfiltered_state_exit], axis=1
    )
    padded = extended(joined, CONV // 2)
    kernel = jnp.concatenate([channel_feed_filter, state_entry_filter, state_exit_filter], axis=1)
    summed = jnp.zeros(joined.shape, jnp.float32)
    for offset in range(CONV):
        summed = summed + kernel[offset] * padded[offset : offset + tokens_here].astype(jnp.float32)
    conv_out = jax.nn.silu(summed).astype(jnp.bfloat16)
    x_conv = conv_out[:, :width].reshape(tokens_here, heads_here, HD)
    b_conv = conv_out[:, width : 2 * width]
    c_conv = conv_out[:, 2 * width :]
    steps = jax.nn.softplus(increment_preactivation)
    logs = -steps * channel_fading_speed[:, :, None] + summed_attenuation_both_ways
    within, state_fwd, state_bwd, total_fwd, total_bwd, factor_fwd, factor_bwd = block_parts(
        x_conv, b_conv, c_conv, steps[0], steps[1], logs[0], logs[1]
    )
    incoming_fwd, incoming_bwd = carried_in(state_fwd, state_bwd, total_fwd, total_bwd)
    c_block = c_conv.astype(jnp.float32)
    mixer_out = (
        within
        + read_state(c_block, factor_fwd, incoming_fwd)
        + read_state(c_block, factor_bwd, incoming_bwd)
    )
    gated = mixer_out.reshape(tokens_here, width) * jax.nn.silu(
        final_valve_preactivation.astype(jnp.float32)
    )
    gated = gated * lax.rsqrt(jnp.mean(gated * gated, axis=-1, keepdims=True) + group_eps)
    mixed = (gated * clustered_rescale_factor).astype(jnp.bfloat16)

    peers_y, peers_c = lax.axis_size("y"), lax.axis_size("c")
    gathered = lax.all_gather(to_all(mixed, "y"), "c", axis=1)
    projected = jnp.einsum(
        "kti,kij->tj",
        gathered.reshape(peers_y * peers_c, tokens_here, width),
        final_projection_weights.reshape(peers_y * peers_c, width, width),
        preferred_element_type=jnp.float32,
    )
    stream = (skip_stream_entering.astype(jnp.float32) + projected).astype(jnp.bfloat16)

    expert_total = lax.axis_size(SP)
    capacity = 4 * tokens_here // expert_total
    slots = expert_total * capacity
    named = lax.broadcasted_iota(jnp.int32, (tokens_here, expert_total), 1)
    hit = [item_specialist_couple[:, k : k + 1] == named for k in range(2)]
    earlier = lax.broadcasted_iota(jnp.int32, (tokens_here, tokens_here), 0) > (
        lax.broadcasted_iota(jnp.int32, (tokens_here, tokens_here), 1)
    )
    ranking = jnp.dot(
        earlier.astype(jnp.bfloat16),
        (hit[0] | hit[1]).astype(jnp.bfloat16),
        preferred_element_type=jnp.float32,
    )
    slot_iota = lax.broadcasted_iota(jnp.int32, (tokens_here, slots), 1)
    chosen = []
    for k in range(2):
        rank = jnp.sum(jnp.where(hit[k], ranking, 0.0), axis=1, keepdims=True).astype(jnp.int32)
        chosen.append(item_specialist_couple[:, k : k + 1] * capacity + rank == slot_iota)
    outgoing = lax.dot_general(
        (chosen[0] | chosen[1]).astype(jnp.bfloat16),
        stream,
        (((0,), (0,)), ((), ())),
        preferred_element_type=jnp.float32,
    ).astype(jnp.bfloat16)
    arrived = lax.all_to_all(
        outgoing.reshape(expert_total, capacity, width), SP, 0, 0, tiled=True
    ).reshape(slots, width)
    rows = to_all(to_all(arrived, "y"), "c")
    partial_out = expert(
        rows,
        specialist_rescale_factor.reshape(1, D),
        specialist_gating_weights[0],
        specialist_raising_weights[0],
        specialist_lowering_weights[0],
    )
    pair = lax.all_to_all(partial_out, "c", 0, 0, tiled=True)
    pair = jnp.sum(pair.astype(jnp.float32), axis=0).astype(jnp.bfloat16)
    whole = lax.all_to_all(pair, "y", 0, 0, tiled=True)
    answer = jnp.sum(whole.astype(jnp.float32), axis=0).astype(jnp.bfloat16)
    returned = lax.all_to_all(
        answer.reshape(expert_total, capacity, width), SP, 0, 0, tiled=True
    ).reshape(slots, width)
    first = jax.nn.sigmoid(selected_twin_scores_raw[:, :1] - selected_twin_scores_raw[:, 1:])
    likelihood = selected_cluster_likelihood[:, None]
    total = stream.astype(jnp.float32)
    for k, weight in enumerate((likelihood * first, likelihood * (1.0 - first))):
        picked = jnp.dot(
            chosen[k].astype(jnp.bfloat16), returned, preferred_element_type=jnp.float32
        )
        total = total + weight * picked
    return total.astype(jnp.bfloat16)


def solution(mesh):
    sizes = dict(mesh.shape)
    torus = Mesh(mesh.devices.reshape(8, 4, sizes["tp"] // 2, 2), ("z", "x", "y", "c"))
    return jax.shard_map(
        body,
        mesh=torus,
        in_specs=(
            P(SP, TP),
            P(SP, TP),
            P(SP, TP),
            P(SP, TP),
            P(SP, TP),
            P(None, TP, SP),
            P(None, TP, SP),
            P(None, TP),
            P(None, TP),
            P(None, TP),
            P(None, TP),
            P(TP),
            P(None, TP),
            P(),
            P(SP, None),
            P(SP),
            P(SP, None),
            P(SP, None, TP),
            P(SP, None, TP),
            P(SP, TP, None),
        ),
        out_specs=P(SP, TP),
        check_vma=False,
    )
```

time: 281 us -> 194 us (0.69)
  blocking collectives: 175 us -> 97.1 us
  waiting for transfers between devices: 57.9 us -> 33.5 us
  starting transfers between devices: 17.4 us -> 33.7 us
  Pallas kernels: 0 us -> 6.37 us
  matrix products: 9.61 us -> 3.24 us
    all_gather x6 -> x1, blocking collectives: 120 us -> 6.89 us  [body(): gathered = lax.all_gather(to_all(mixed, 'y'), 'c', axis=1)]
    all_to_all x1 -> x5, blocking collectives: 55.6 us -> 90.2 us  [the longest x2 38 us: to_all(): return lax.all_to_all(copies, axis, 0, 0, tiled=True)]
    all_to_all x2 -> x4, waiting for transfers between devices: 57.9 us -> 33.5 us  [the longest x2 14.9 us: to_all(): return lax.all_to_all(copies, axis, 0, 0, tiled=True)]
    all_to_all x2 -> x4, starting transfers between devices: 12.2 us -> 28.4 us  [the longest x1 12.5 us: carried_in(): lax.all_to_all(jnp.where(far > my_z, out_f[None], out_b[None]), 'z', 0, 0...]
    dot_general x9 -> x10, matrix products: 9.24 us -> 2.84 us  [the longest x2 1.08 us: body(): jnp.dot(chosen[k].astype(jnp.bfloat16), returned, preferred_element_type=...]
    pallas_call x0 -> x1, Pallas kernels: none -> 6.37 us  [expert(): pl.pallas_call(functools.partial(expert_kernel, chunk), out_shape=jax.Sha...]
    broadcast_in_dim x0 -> x20, local copies, waits for them, and re-layouts: none -> 3.35 us  [the longest x4 2.01 us: to_all(): copies = jnp.broadcast_to(shard[None], (peers, *shard.shape))]
    unnamed x30 -> x19, local copies, waits for them, and re-layouts: 6.06 us -> 3.12 us
  transfers between devices with their start and end apart: 4 -> 6, of which waited for: 2 -> 4; matrix products, arithmetic and copies ran while one was open for 3% -> 3% of each run, Pallas kernels for 0% -> 0%
where the time goes in v1:
time: 194 us; the launch traced here: 193 us
  blocking collectives  97.1 us (50%)
  starting transfers between devices  33.7 us (17%)
  waiting for transfers between devices  33.5 us (17%)
  local copies, waits for them, and re-layouts  11.1 us (6%)
  other arithmetic  7.66 us (4%)
  Pallas kernels  6.37 us (3%)
  matrix products  3.24 us (2%)
    all_to_all x2, blocking collectives, to_all(): return lax.all_to_all(copies, axis, 0, 0, tiled=True)  38 us
    all_to_all x1, blocking collectives, body(): whole = lax.all_to_all(pair, 'y', 0, 0, tiled=True)  32.8 us
    all_to_all x2, waiting for transfers between devices, to_all(): return lax.all_to_all(copies, axis, 0, 0, tiled=True)  14.9 us
    all_to_all x1, blocking collectives, body(): lax.all_to_all(outgoing.reshape(expert_total, capacity, width), SP, 0, 0,...  12.7 us
    all_to_all x1, starting transfers between devices, carried_in(): lax.all_to_all(jnp.where(far > my_z, out_f[None], out_b[None]), 'z', 0, 0...  12.5 us
    all_to_all x2, starting transfers between devices, to_all(): return lax.all_to_all(copies, axis, 0, 0, tiled=True)  12.1 us
    all_to_all x1, waiting for transfers between devices, body(): lax.all_to_all(answer.reshape(expert_total, capacity, width), SP, 0, 0, t...  9.4 us
    all_to_all x1, waiting for transfers between devices, carried_in(): lax.all_to_all(jnp.where(far > my_z, out_f[None], out_b[None]), 'z', 0, 0...  9.26 us
  transfers between devices with their start and end apart: 6, of which 4 were waited for; matrix products, arithmetic and copies ran while one was open for 3% of the time, Pallas kernels for 0%

profile of v1, /device:TPU:1, one launch (start us, length us, event | category | flops | bytes accessed | tf_op | source)
XLA Modules:
  0.0 193.1 jit_solution(8810928779054232238)
XLA Ops:
  0.0 0.8 constant_dynamic-update-slice_fusion.5
  0.8 0.8 constant_dynamic-update-slice_fusion.4
  1.6 0.8 constant_dynamic-update-slice_fusion.3
  2.4 3.9 %collective-permute-start = (bf16[2,384]{1,0:T(2,128)(2,1)S(1)}, bf16[2,384]{1,0:T(2,128)(2,1)S(1)}, u32[]{:S(2)}, u32[]{:S(2)}) collective-permute-start(bf16[2,384]{1,0:T(2,128)(2,1)S(1)} %get-tuple-element.48), channel_id=1, source_target_pairs={{0,16},{16,32},{32,48},{48,64},{64,80},{80,96},{96,112},{112,128},... | collective-permute-start | bytes 4616 | tf_op jit(solution)/shard_map/ppermute | solution.py:29
  6.3 1.3 collective-permute-start.1
  7.6 0.8 multiply_add_fusion
  8.5 0.3 reduce_window_sum.18
  8.8 0.2 slice_reduce_fusion.5
  9.1 0.3 reduce_window_sum.17
  9.4 0.2 slice_reduce_fusion.6
  9.7 0.7 constant_dynamic-update-slice_fusion.2
  10.4 0.7 constant_dynamic-update-slice_fusion.1
  11.1 0.7 constant_dynamic-update-slice_fusion
  12.2 0.2 multiply_convert_fusion
  12.5 0.2 convolution_convert_fusion.2
  12.7 0.2 convolution_convert_fusion.1
  13.1 0.7 broadcast_in_dim.354
  13.8 5.3 %all-to-all-start = ((bf16[4,288,128]{2,1,0:T(8,128)(2,1)}), bf16[4,288,128]{2,1,0:T(8,128)(2,1)S(1)}, u32[]{:S(2)}, u32[]{:S(2)}) async-start(bf16[4,288,128]{2,1,0:T(8,128)(2,1)} %broadcast_in_dim.354), calls=%async_computation | async-start | bytes 589824 | tf_op jit(solution)/shard_map/all_to_all | solution.py:40
  19.1 5.7 %all-to-all-done = bf16[4,288,128]{2,1,0:T(8,128)(2,1)S(1)} async-done(((bf16[4,288,128]{2,1,0:T(8,128)(2,1)}), bf16[4,288,128]{2,1,0:T(8,128)(2,1)S(1)}, u32[]{:S(2)}, u32[]{:S(2)}) %all-to-all-start) | async-done | bytes 294944 | tf_op jit(solution)/shard_map/all_to_all | solution.py:40
  25.1 0.2 select_reduce_fusion.8
  27.8 0.7 fusion.18
  28.8 0.8 broadcast_select_fusion
  29.6 12.5 %all-to-all-start.1 = ((bf16[8,144,128]{2,1,0:T(8,128)(2,1)}), bf16[8,144,128]{2,1,0:T(8,128)(2,1)S(1)}, u32[]{:S(2)}, u32[]{:S(2)}) async-start(bf16[8,144,128]{2,1,0:T(8,128)(2,1)} %broadcast_select_fusion), calls=%async_computation.1 | async-start | bytes 589824 | tf_op jit(solution)/shard_map/all_to_all | solution.py:156
  42.2 0.4 convolution_bitcast_fusion.1
  42.6 9.3 %all-to-all-done.1 = bf16[8,144,128]{2,1,0:T(8,128)(2,1)S(1)} async-done(((bf16[8,144,128]{2,1,0:T(8,128)(2,1)}), bf16[8,144,128]{2,1,0:T(8,128)(2,1)S(1)}, u32[]{:S(2)}, u32[]{:S(2)}) %all-to-all-start.1) | async-done | bytes 294944 | tf_op jit(solution)/shard_map/all_to_all | solution.py:156
  53.1 0.7 fusion.10
  53.9 0.3 fusion.3
  54.1 0.3 fusion.2
  54.7 0.7 broadcast_in_dim.394
  55.5 6.8 %all-to-all-start.2 = ((bf16[8,128,128]{2,1,0:T(8,128)(2,1)}), bf16[8,128,128]{2,1,0:T(8,128)(2,1)S(1)}, u32[]{:S(2)}, u32[]{:S(2)}) async-start(bf16[8,128,128]{2,1,0:T(8,128)(2,1)} %broadcast_in_dim.394), calls=%async_computation.2 | async-start | bytes 524288 | tf_op jit(solution)/shard_map/all_to_all | solution.py:40
  62.3 0.2 select_reduce_fusion.1
  62.5 9.2 %all-to-all-done.2 = bf16[8,128,128]{2,1,0:T(8,128)(2,1)S(1)} async-done(((bf16[8,128,128]{2,1,0:T(8,128)(2,1)}), bf16[8,128,128]{2,1,0:T(8,128)(2,1)S(1)}, u32[]{:S(2)}, u32[]{:S(2)}) %all-to-all-start.2) | async-done | bytes 262176 | tf_op jit(solution)/shard_map/all_to_all | solution.py:40
  71.6 6.9 %all-gather = bf16[8,256,128]{2,1,0:T(8,128)(2,1)S(1)} all-gather(bf16[8,128,128]{2,1,0:T(8,128)(2,1)S(1)} %all-to-all-done.2), channel_id=2, replica_groups=mesh['z'=8,'x'=4,'y'=8,'c'=2] {'c'}, dimensions={1}, use_global_device_ids=true | all-gather | bytes 786432 | tf_op jit(solution)/shard_map/all_gather | solution.py:270
  78.5 0.3 fusion.5
  78.8 0.3 convolution_convert_fusion
  79.2 12.7 %all_to_all.45 = bf16[32,16,128]{2,1,0:T(8,128)(2,1)S(1)} all-to-all(bf16[32,16,128]{2,1,0:T(8,128)(2,1)S(1)} %bitcast.140), channel_id=1, replica_groups=mesh['z'=8,'x'=4,'y'=8,'c'=2] {'z','x'}, dimensions={0} | all-to-all | bytes 262144 | tf_op jit(solution)/shard_map/all_to_all | solution.py:303
  92.0 28.8 %all_to_all.46 = bf16[8,512,128]{2,1,0:T(8,128)(2,1)S(1)} all-to-all(bf16[8,512,128]{2,1,0:T(8,128)(2,1)S(1)} %broadcast_in_dim.398), channel_id=1, replica_groups=mesh['z'=8,'x'=4,'y'=8,'c'=2] {'y'}, dimensions={0} | all-to-all | bytes 2097152 | tf_op jit(solution)/shard_map/all_to_all | solution.py:40
  120.8 0.4 broadcast_in_dim.399
  121.2 9.3 %all_to_all.47.rows_ref = bf16[2,8,512,128]{3,2,1,0:T(8,128)(2,1)} all-to-all(bf16[2,8,512,128]{3,2,1,0:T(8,128)(2,1)S(1)} %broadcast_in_dim.399), channel_id=1, replica_groups=mesh['z'=8,'x'=4,'y'=8,'c'=2] {'c'}, dimensions={0} | all-to-all | bytes 4194304 | tf_op jit(solution)/shard_map/all_to_all | solution.py:40
  130.5 6.4 %expert.1 = bf16[2,8,512,128]{3,2,1,0:T(8,128)(2,1)} custom-call(bf16[2,8,512,128]{3,2,1,0:T(8,128)(2,1)} %all_to_all.47.rows_ref, f32[1,2048]{1,0:T(1,128)} %bitcast.143, bf16[2048,256]{1,0:T(8,128)(2,1)} %bitcast.124, bf16[2048,256]{1,0:T(8,128)(2,1)} %bitcast.125, bf16[256,2048]{1,0:T(8,128)(2,1)} %bitcast.126), custom_call_target="tpu_custom_call" | custom-call | tf_op jit(solution)/shard_map/expert/pallas_call | solution.py:204
  136.9 6.6 %all_to_all.48 = bf16[2,8,512,128]{3,2,1,0:T(8,128)(2,1)S(1)} all-to-all(bf16[2,8,512,128]{3,2,1,0:T(8,128)(2,1)} %expert.1), channel_id=1, replica_groups=mesh['z'=8,'x'=4,'y'=8,'c'=2] {'c'}, dimensions={0} | all-to-all | bytes 4194304 | tf_op jit(solution)/shard_map/all_to_all | solution.py:314
  143.5 1.6 reduce_sum.232
  145.1 32.8 %all_to_all.49 = bf16[8,512,128]{2,1,0:T(8,128)(2,1)S(1)} all-to-all(bf16[8,512,128]{2,1,0:T(8,128)(2,1)} %reduce_sum.232), channel_id=1, replica_groups=mesh['z'=8,'x'=4,'y'=8,'c'=2] {'y'}, dimensions={0} | all-to-all | bytes 2097152 | tf_op jit(solution)/shard_map/all_to_all | solution.py:316
  177.9 0.8 reduce_sum.233
  178.7 3.9 %all-to-all-start.8 = ((bf16[32,16,128]{2,1,0:T(8,128)(2,1)}), bf16[32,16,128]{2,1,0:T(8,128)(2,1)S(1)}, u32[]{:S(2)}, u32[]{:S(2)}) async-start(bf16[32,16,128]{2,1,0:T(8,128)(2,1)} %bitcast.40), calls=%async_computation.8 | async-start | bytes 262144 | tf_op jit(solution)/shard_map/all_to_all | solution.py:318
  182.6 9.4 %all-to-all-done.8 = bf16[32,16,128]{2,1,0:T(8,128)(2,1)S(1)} async-done(((bf16[32,16,128]{2,1,0:T(8,128)(2,1)}), bf16[32,16,128]{2,1,0:T(8,128)(2,1)S(1)}, u32[]{:S(2)}, u32[]{:S(2)}) %all-to-all-start.8) | async-done | bytes 131104 | tf_op jit(solution)/shard_map/all_to_all | solution.py:318
  192.0 0.2 fusion.1
  192.2 0.8 fusion.6
  (122 shorter events, 5.8 us)
Async XLA Ops:
  0.0 78.5 %copy-start = (bf16[2048,128]{1,0:T(8,128)(2,1)S(1)}, bf16[2048,128]{1,0:T(8,128)(2,1)}, u32[]{:S(2)}) copy-start(bf16[2048,128]{1,0:T(8,128)(2,1)} %param.32) | copy-start | bytes 1572868
  2.4 9.8 %collective-permute-start = (bf16[2,384]{1,0:T(2,128)(2,1)S(1)}, bf16[2,384]{1,0:T(2,128)(2,1)S(1)}, u32[]{:S(2)}, u32[]{:S(2)}) collective-permute-start(bf16[2,384]{1,0:T(2,128)(2,1)S(1)} %get-tuple-element.48), channel_id=1, source_target_pairs={{0,16},{16,32},{32,48},{48,64},{64,80},{80,96},{96,112},{112,128},... | collective-permute-start | bytes 4616 | tf_op jit(solution)/shard_map/ppermute | solution.py:29
  6.3 5.9 %collective-permute-start.1 = (bf16[2,384]{1,0:T(2,128)(2,1)S(1)}, bf16[2,384]{1,0:T(2,128)(2,1)S(1)}, u32[]{:S(2)}, u32[]{:S(2)}) collective-permute-start(bf16[2,384]{1,0:T(2,128)(2,1)S(1)} %get-tuple-element.49), channel_id=1, source_target_pairs={{16,0},{32,16},{48,32},{64,48},{80,64},{96,80},{112,96},{128,112},... | collective-permute-start | bytes 4616 | tf_op jit(solution)/shard_map/ppermute | solution.py:31
  13.8 40.7 %copy-start.1 = (bf16[128,128]{1,0:T(8,128)(2,1)S(1)}, bf16[128,128]{1,0:T(8,128)(2,1)}, u32[]{:S(2)}) copy-start(bf16[128,128]{1,0:T(8,128)(2,1)} %param.24) | copy-start | bytes 98308
  13.8 11.0 %all-to-all-start = ((bf16[4,288,128]{2,1,0:T(8,128)(2,1)}), bf16[4,288,128]{2,1,0:T(8,128)(2,1)S(1)}, u32[]{:S(2)}, u32[]{:S(2)}) async-start(bf16[4,288,128]{2,1,0:T(8,128)(2,1)} %broadcast_in_dim.354), calls=%async_computation | async-start | bytes 589824 | tf_op jit(solution)/shard_map/all_to_all | solution.py:40
  19.1 35.5 %copy-start.5 = (f32[128]{0:T(128)S(1)}, f32[128]{0:T(128)}, u32[]{:S(2)}) copy-start(f32[128]{0:T(128)} %param.31) | copy-start | bytes 1540
  28.6 33.7 %copy-start.3 = (s32[128,2]{0,1:T(2,128)S(1)}, s32[128,2]{0,1:T(2,128)}, u32[]{:S(2)}) copy-start(s32[128,2]{0,1:T(2,128)} %param.34) | copy-start | bytes 3076
  29.6 22.3 %all-to-all-start.1 = ((bf16[8,144,128]{2,1,0:T(8,128)(2,1)}), bf16[8,144,128]{2,1,0:T(8,128)(2,1)S(1)}, u32[]{:S(2)}, u32[]{:S(2)}) async-start(bf16[8,144,128]{2,1,0:T(8,128)(2,1)} %broadcast_select_fusion), calls=%async_computation.1 | async-start | bytes 589824 | tf_op jit(solution)/shard_map/all_to_all | solution.py:156
  42.0 36.5 %copy-start.2 = (bf16[128,128]{1,0:T(8,128)(2,1)S(1)}, bf16[128,128]{1,0:T(8,128)(2,1)}, u32[]{:S(2)}) copy-start(bf16[128,128]{1,0:T(8,128)(2,1)} %param.20) | copy-start | bytes 98308
  55.5 16.2 %all-to-all-start.2 = ((bf16[8,128,128]{2,1,0:T(8,128)(2,1)}), bf16[8,128,128]{2,1,0:T(8,128)(2,1)S(1)}, u32[]{:S(2)}, u32[]{:S(2)}) async-start(bf16[8,128,128]{2,1,0:T(8,128)(2,1)} %broadcast_in_dim.394), calls=%async_computation.2 | async-start | bytes 524288 | tf_op jit(solution)/shard_map/all_to_all | solution.py:40
  145.1 37.4 %copy-start.4 = (f32[128,2]{0,1:T(2,128)S(1)}, f32[128,2]{0,1:T(2,128)}, u32[]{:S(2)}) copy-start(f32[128,2]{0,1:T(2,128)} %param.36) | copy-start | bytes 3076
  145.1 37.4 %copy-start.6 = (f32[128]{0:T(128)S(1)}, f32[128]{0:T(128)}, u32[]{:S(2)}) copy-start(f32[128]{0:T(128)} %param.35) | copy-start | bytes 1540
  178.7 13.3 %all-to-all-start.8 = ((bf16[32,16,128]{2,1,0:T(8,128)(2,1)}), bf16[32,16,128]{2,1,0:T(8,128)(2,1)S(1)}, u32[]{:S(2)}, u32[]{:S(2)}) async-start(bf16[32,16,128]{2,1,0:T(8,128)(2,1)} %bitcast.40), calls=%async_computation.8 | async-start | bytes 262144 | tf_op jit(solution)/shard_map/all_to_all | solution.py:318

commit v2 on v1

v2 whole, which is shorter than its diff:
```python
import functools

import jax
import jax.numpy as jnp
from jax import lax
from jax.experimental import pallas as pl
from jax.experimental.pallas import tpu as pltpu
from jax.sharding import Mesh
from jax.sharding import PartitionSpec as P

D = 2048
HD = 64
NS = 128
CONV = 5
SP = ("z", "x")
TP = ("y", "c")

HIGHEST = lax.Precision.HIGHEST
group_eps = 1e-05
stream_eps = 1e-06

VMEM = pl.BlockSpec(memory_space=pltpu.VMEM)
SMEM = pl.BlockSpec(memory_space=pltpu.SMEM)
MIB = 1 << 20


def call(kernel, name, outs, args, flops=1000, scratch=(), room=8, smem=0):
    shapes = [jax.ShapeDtypeStruct(shape, dtype) for shape, dtype in outs]
    moved = sum(a.size * a.dtype.itemsize for a in args) + sum(
        o.size * o.dtype.itemsize for o in shapes
    )
    return pl.pallas_call(
        kernel,
        out_shape=shapes,
        in_specs=[SMEM] * smem + [VMEM] * (len(args) - smem),
        out_specs=[VMEM] * len(shapes),
        scratch_shapes=list(scratch),
        compiler_params=pltpu.CompilerParams(vmem_limit_bytes=room * MIB),
        cost_estimate=pl.CostEstimate(flops=flops, bytes_accessed=moved, transcendentals=0),
        name=name,
    )(*args)


def exact_dot(a, b):
    return jnp.dot(a, b, precision=HIGHEST, preferred_element_type=jnp.float32)


def dot_rows(a, b, precision=None):
    return lax.dot_general(
        a,
        b,
        (((1,), (1,)), ((), ())),
        precision=precision,
        preferred_element_type=jnp.float32,
    )


def iota(shape, dim):
    return lax.broadcasted_iota(jnp.int32, shape, dim)


def table_kernel(capacity, step_ref, fade_ref, speed_ref, named_ref, like_ref, score_ref, row_ref, col_ref):
    length = row_ref.shape[1]
    for d in range(2):
        raw = step_ref[d]
        step = jnp.maximum(raw, 0.0) + jnp.log1p(jnp.exp(-jnp.abs(raw)))
        row_ref[2 * d : 2 * d + 2, :] = -step * speed_ref[d] + fade_ref[d]
        row_ref[4 + 2 * d : 6 + 2 * d, :] = step
    whole = row_ref[0:8, :]
    lane, line = iota(whole.shape, 1), iota(whole.shape, 0)
    ahead = behind = whole
    reach = 1
    while reach < length:
        ahead = ahead + jnp.where(lane >= reach, pltpu.roll(ahead, reach, 1), 0.0)
        behind = behind + jnp.where(lane < length - reach, pltpu.roll(behind, length - reach, 1), 0.0)
        reach *= 2
    row_ref[0:8, :] = jnp.where(line < 2, ahead, jnp.where(line < 4, behind, whole))
    experts = 32
    expert = iota((experts, length), 0)
    hit = [named_ref[k : k + 1, :] == expert for k in range(2)]
    earlier = iota((length, length), 0) < iota((length, length), 1)
    ranking = jnp.dot(
        jnp.where(hit[0] | hit[1], 1.0, 0.0).astype(jnp.bfloat16),
        jnp.where(earlier, 1.0, 0.0).astype(jnp.bfloat16),
        preferred_element_type=jnp.float32,
    )
    place = ranking + expert.astype(jnp.float32) * capacity
    for k in range(2):
        row_ref[8 + k : 9 + k, :] = jnp.sum(jnp.where(hit[k], place, 0.0), axis=0, keepdims=True)
    first = jax.nn.sigmoid(score_ref[0:1, :] - score_ref[1:2, :])
    row_ref[10:11, :] = like_ref[...] * first
    row_ref[11:12, :] = like_ref[...] * (1.0 - first)
    row_ref[12:16, :] = jnp.zeros((4, length), jnp.float32)
    col_ref[...] = jnp.zeros_like(col_ref)
    col_ref[0:16, :] = row_ref[...]
    col_ref[...] = jnp.transpose(col_ref[...])


def conv_kernel(
    x_ref, b_ref, c_ref, before_ref, after_ref, kx_ref, kb_ref, kc_ref, col_ref,
    message_ref, xs_ref, bs_ref, cs_ref, padded,
):
    length, width = x_ref.shape
    parts = []
    for n, (ref, taps) in enumerate(((x_ref, kx_ref), (b_ref, kb_ref), (c_ref, kc_ref))):
        lanes = slice(n * width, (n + 1) * width)
        padded[8 : 8 + length, :] = ref[...].astype(jnp.float32)
        padded[6:8, :] = before_ref[:, lanes]
        padded[8 + length : 10 + length, :] = after_ref[:, lanes]
        total = jnp.zeros((length, width), jnp.float32)
        for k in range(CONV):
            total = total + taps[k : k + 1, :] * padded[6 + k : 6 + k + length, :]
        parts.append(jax.nn.silu(total).astype(jnp.bfloat16))
    xs_ref[...], bs_ref[...], cs_ref[...] = parts
    x_block = parts[0].astype(jnp.float32)
    b_block = parts[1].astype(jnp.float32)
    left = iota((length, width), 1) < HD
    logs = jnp.zeros((16, width), jnp.float32)
    line = iota((16, width), 0)
    for d, last in ((0, length - 1), (1, 0)):
        weight = []
        for h in range(2):
            k = 2 * d + h
            end = col_ref[last : last + 1, k : k + 1]
            weight.append(jnp.exp(end - col_ref[:, k : k + 1]) * col_ref[:, 4 + k : 5 + k])
            high = end.astype(jnp.bfloat16).astype(jnp.float32)
            logs = jnp.where(line == 4 * d + h, high, logs)
            logs = jnp.where(line == 4 * d + 2 + h, end - high, logs)
        scaled = x_block * jnp.where(left, weight[0], weight[1])
        state = exact_dot(jnp.transpose(scaled), b_block).astype(jnp.bfloat16)
        for peer in range(message_ref.shape[0]):
            message_ref[peer, d * width : (d + 1) * width, :] = state
    for peer in range(message_ref.shape[0]):
        message_ref[peer, 2 * width :, :] = logs.astype(jnp.bfloat16)


def within_kernel(xs_ref, bs_ref, cs_ref, row_ref, col_ref, out_ref):
    length, width = xs_ref.shape
    scores = dot_rows(cs_ref[...], bs_ref[...])
    x_block = xs_ref[...].astype(jnp.float32)
    to, since = iota((length, length), 0), iota((length, length), 1)
    sides = []
    for h in range(2):
        both = jnp.zeros((length, length), jnp.float32)
        for d in range(2):
            k = 2 * d + h
            seen = since <= to if d == 0 else since >= to
            passed = col_ref[:, k : k + 1] - row_ref[k : k + 1, :]
            decay = jnp.where(seen, jnp.exp(jnp.minimum(passed, 0.0)), 0.0)
            both = both + decay * row_ref[4 + k : 5 + k, :]
        sides.append(exact_dot(scores * both, x_block))
    out_ref[...] = jnp.where(iota((length, width), 1) < HD, sides[0], sides[1])


def log_pair(tile, d):
    return [tile[4 * d + h : 4 * d + h + 1, :] + tile[4 * d + 2 + h : 4 * d + 3 + h, :] for h in range(2)]


def by_head(pair, rows):
    return jnp.where(iota((rows, 128), 0) < HD, pair[0], pair[1])


def row_kernel(place_ref, seen_ref, message_ref, near_ref, ahead_ref):
    my_x, my_z = place_ref[0], place_ref[1]
    peers, rows = seen_ref.shape[0], near_ref.shape[1]
    line = iota((16, 128), 0)
    out = []
    ahead_ref[...] = jnp.zeros_like(ahead_ref)
    for d in range(2):
        total = near = jnp.zeros((rows, 128), jnp.float32)
        far = [jnp.zeros((1, 128), jnp.float32)] * 2
        ahead = list(far)
        for k in range(peers) if d == 0 else reversed(range(peers)):
            logs = log_pair(seen_ref[k, 2 * rows :, :].astype(jnp.float32), d)
            near = jnp.where(k == my_x, total, near)
            passed = k < my_x if d == 0 else k > my_x
            state = seen_ref[k, d * rows : (d + 1) * rows, :].astype(jnp.float32)
            total = total * jnp.exp(by_head(logs, rows)) + state
            for h in range(2):
                far[h] = far[h] + logs[h]
                ahead[h] = ahead[h] + jnp.where(passed, logs[h], 0.0)
        near_ref[d] = near
        tile = jnp.zeros((16, 128), jnp.float32)
        for h in range(2):
            ahead_ref[2 * d + h : 2 * d + h + 1, :] = ahead[h]
            high = far[h].astype(jnp.bfloat16).astype(jnp.float32)
            tile = jnp.where(line == h, high, tile)
            tile = jnp.where(line == 2 + h, far[h] - high, tile)
        out.append((total, tile))
    for k in range(message_ref.shape[0]):
        onward = k > my_z
        message_ref[k, :rows, :] = jnp.where(onward, out[0][0], out[1][0]).astype(jnp.bfloat16)
        message_ref[k, rows:, :] = jnp.where(onward, out[0][1], out[1][1]).astype(jnp.bfloat16)


def mixed_kernel(
    place_ref, got_ref, near_ref, ahead_ref, cs_ref, within_ref, col_ref, valve_ref, gain_ref, out_ref
):
    my_z = place_ref[1]
    peers, rows = got_ref.shape[0], near_ref.shape[1]
    length = cs_ref.shape[0]
    c_block = cs_ref[...].astype(jnp.float32)
    left = iota((length, rows), 1) < HD
    mixer = within_ref[...]
    for d in range(2):
        state = jnp.zeros((rows, 128), jnp.float32)
        for k in range(peers) if d == 0 else reversed(range(peers)):
            passed = k < my_z if d == 0 else k > my_z
            logs = log_pair(got_ref[k, rows:, :].astype(jnp.float32), 0)
            onto = state * jnp.exp(by_head(logs, rows)) + got_ref[k, :rows, :].astype(jnp.float32)
            state = jnp.where(passed, onto, state)
        ahead = [ahead_ref[2 * d + h : 2 * d + h + 1, :] for h in range(2)]
        state = state * jnp.exp(by_head(ahead, rows)) + near_ref[d]
        factor = jnp.exp(
            jnp.where(left, col_ref[:, 2 * d : 2 * d + 1], col_ref[:, 2 * d + 1 : 2 * d + 2])
        )
        mixer = mixer + dot_rows(c_block, state, HIGHEST) * factor
    gated = mixer * jax.nn.silu(valve_ref[...].astype(jnp.float32))
    gated = gated * lax.rsqrt(jnp.mean(gated * gated, axis=-1, keepdims=True) + group_eps)
    mixed = (gated * gain_ref[...]).astype(jnp.bfloat16)
    for k in range(out_ref.shape[0]):
        out_ref[k] = mixed


def stream_kernel(mixed_ref, weight_ref, skip_ref, row_ref, stream_ref, out_ref):
    length, width = skip_ref.shape
    places = mixed_ref.shape[0]
    total = skip_ref[...].astype(jnp.float32)
    product = jnp.zeros((length, width), jnp.float32)
    for y in range(places):
        both = jnp.concatenate([mixed_ref[y, :length, :], mixed_ref[y, length:, :]], axis=1)
        product = product + jnp.dot(
            both, weight_ref[2 * y * width : 2 * (y + 1) * width, :], preferred_element_type=jnp.float32
        )
    stream = (total + product).astype(jnp.bfloat16)
    stream_ref[...] = stream
    slot = iota((out_ref.shape[0], length), 0).astype(jnp.float32)
    chosen = (row_ref[8:9, :] == slot) | (row_ref[9:10, :] == slot)
    out_ref[...] = jnp.dot(
        jnp.where(chosen, 1.0, 0.0).astype(jnp.bfloat16), stream, preferred_element_type=jnp.float32
    ).astype(jnp.bfloat16)


def half_products(rows_ref, gain_ref, gate_ref, up_ref, core, at, scaled):
    places = rows_ref.shape[0]
    squares = jnp.zeros((at.size, 128), jnp.float32)
    for y in range(places):
        part = rows_ref[y, at, :].astype(jnp.float32)
        squares = squares + part * part
        scaled[:, y * 128 : (y + 1) * 128] = (part * gain_ref[y, pl.ds(core, 1), :]).astype(
            jnp.bfloat16
        )
    whole = scaled[...]
    gate = jnp.dot(whole, gate_ref[...], preferred_element_type=jnp.float32)
    upward = jnp.dot(whole, up_ref[...], preferred_element_type=jnp.float32)
    return jnp.sum(squares, axis=1, keepdims=True), gate, upward


def pick_half(core, weight_ref, half):
    for y in range(half.shape[0] // 128):
        half[y * 128 : (y + 1) * 128, :] = weight_ref[y, core]


def first_half_kernel(
    chunk, place_ref, rows_ref, gain_ref, gate_ref, up_ref, squares_ref, gate_out, up_out, scaled, gate_half, up_half
):
    core = place_ref[2]
    pick_half(core, gate_ref, gate_half)
    pick_half(core, up_ref, up_half)

    def step(i, carry):
        at = pl.ds(pl.multiple_of(i * chunk, chunk), chunk)
        squares, gate, upward = half_products(
            rows_ref, gain_ref, gate_half, up_half, core, at, scaled
        )
        squares_ref[at, :] = jnp.broadcast_to(squares, (chunk, 128))
        gate_out[at, :] = gate
        up_out[at, :] = upward
        return carry

    lax.fori_loop(0, rows_ref.shape[1] // chunk, step, 0)


def second_half_kernel(
    chunk, place_ref, rows_ref, gain_ref, gate_ref, up_ref, down_ref, squares_ref, gate_in, up_in,
    hidden_ref, out_ref, scaled, gate_half, up_half, down_half,
):
    other = 1 - place_ref[2]
    pick_half(other, gate_ref, gate_half)
    pick_half(other, up_ref, up_half)
    for y in range(rows_ref.shape[0]):
        at = pl.ds(pl.multiple_of((2 * y + other) * 128, 128), 128)
        down_half[:, y * 128 : (y + 1) * 128] = down_ref[:, at]

    def step(i, carry):
        at = pl.ds(pl.multiple_of(i * chunk, chunk), chunk)
        squares, gate, upward = half_products(
            rows_ref, gain_ref, gate_half, up_half, other, at, scaled
        )
        squares = squares + squares_ref[at, 0:1]
        scale = lax.rsqrt(squares / D + stream_eps)
        gate = (gate + gate_in[at, :]) * scale
        upward = (upward + up_in[at, :]) * scale
        hidden = (jax.nn.silu(gate) * upward).astype(jnp.bfloat16)
        hidden_ref[at, :] = hidden
        part = jnp.dot(hidden, down_half[...], preferred_element_type=jnp.float32)
        for y in range(rows_ref.shape[0]):
            out_ref[y, at, :] = part[:, y * 128 : (y + 1) * 128].astype(jnp.bfloat16)
        return carry

    lax.fori_loop(0, rows_ref.shape[1] // chunk, step, 0)


def own_half_kernel(chunk, place_ref, hidden_ref, down_ref, out_ref, down_half):
    core = place_ref[2]
    for y in range(out_ref.shape[0]):
        at = pl.ds(pl.multiple_of((2 * y + core) * 128, 128), 128)
        down_half[:, y * 128 : (y + 1) * 128] = down_ref[:, at]

    def step(i, carry):
        at = pl.ds(pl.multiple_of(i * chunk, chunk), chunk)
        part = jnp.dot(hidden_ref[at, :], down_half[...], preferred_element_type=jnp.float32)
        for y in range(out_ref.shape[0]):
            out_ref[y, at, :] = part[:, y * 128 : (y + 1) * 128].astype(jnp.bfloat16)
        return carry

    lax.fori_loop(0, hidden_ref.shape[0] // chunk, step, 0)


def final_kernel(returned_ref, stream_ref, col_ref, out_ref):
    length = stream_ref.shape[0]
    slot = iota((length, returned_ref.shape[0]), 1).astype(jnp.float32)
    returned = returned_ref[...]
    total = stream_ref[...].astype(jnp.float32)
    for k in range(2):
        chosen = jnp.where(col_ref[:, 8 + k : 9 + k] == slot, 1.0, 0.0).astype(jnp.bfloat16)
        picked = jnp.dot(chosen, returned, preferred_element_type=jnp.float32)
        total = total + col_ref[:, 10 + k : 11 + k] * picked
    out_ref[...] = total.astype(jnp.bfloat16)


def swapped(value):
    return lax.ppermute(value, "c", [(0, 1), (1, 0)])


def to_all(shard, axis):
    peers = lax.axis_size(axis)
    copies = jnp.broadcast_to(shard[None], (peers, *shard.shape))
    return lax.all_to_all(copies, axis, 0, 0, tiled=True)


def body(
    skip_stream_entering,
    unfiltered_channel_feed,
    unfiltered_state_entry,
    unfiltered_state_exit,
    final_valve_preactivation,
    increment_preactivation,
    summed_attenuation_both_ways,
    channel_fading_speed,
    channel_feed_filter,
    state_entry_filter,
    state_exit_filter,
    clustered_rescale_factor,
    final_projection_weights,
    specialist_rescale_factor,
    item_specialist_couple,
    selected_cluster_likelihood,
    selected_twin_scores_raw,
    specialist_gating_weights,
    specialist_raising_weights,
    specialist_lowering_weights,
):
    f32, bf16 = jnp.float32, jnp.bfloat16
    length, width = unfiltered_channel_feed.shape
    blocks = lax.axis_size(SP)
    peers_x, peers_y, peers_z = (lax.axis_size(a) for a in ("x", "y", "z"))
    capacity = 4 * length // blocks
    slots = blocks * capacity
    place = jnp.stack([lax.axis_index("x"), lax.axis_index("z"), lax.axis_index("c")]).astype(jnp.int32)

    rim = CONV // 2
    feeds = (unfiltered_channel_feed, unfiltered_state_entry, unfiltered_state_exit)
    tail = jnp.concatenate([a[-rim:] for a in feeds], axis=1).astype(f32)
    top = jnp.concatenate([a[:rim] for a in feeds], axis=1).astype(f32)
    before = lax.ppermute(tail, SP, [(i, i + 1) for i in range(blocks - 1)])
    after = lax.ppermute(top, SP, [(i + 1, i) for i in range(blocks - 1)])

    rows, cols = call(
        functools.partial(table_kernel, capacity),
        "table",
        [((16, length), f32), ((length, length), f32)],
        (
            increment_preactivation,
            summed_attenuation_both_ways,
            channel_fading_speed[:, :, None],
            item_specialist_couple.T,
            selected_cluster_likelihood[None],
            selected_twin_scores_raw.T,
        ),
        flops=4_000_000,
    )
    message, x_conv, b_conv, c_conv = call(
        conv_kernel,
        "conv",
        [((peers_x, 2 * width + 16, NS), bf16)] + [((length, width), bf16)] * 3,
        (*feeds, before, after, channel_feed_filter, state_entry_filter, state_exit_filter, cols),
        flops=4_000_000,
        scratch=[pltpu.VMEM((length + 16, width), f32)],
    )
    seen = lax.all_to_all(message, "x", 0, 0, tiled=True)
    (within,) = call(
        within_kernel,
        "within",
        [((length, width), f32)],
        (x_conv, b_conv, c_conv, rows, cols),
        flops=40_000_000,
    )
    onward, near, ahead = call(
        row_kernel,
        "row",
        [((peers_z, width + 16, NS), bf16), ((2, width, NS), f32), ((8, NS), f32)],
        (place, seen),
        smem=1,
    )
    got = lax.all_to_all(onward, "z", 0, 0, tiled=True)
    (copies,) = call(
        mixed_kernel,
        "mixed",
        [((peers_y, length, width), bf16)],
        (
            place, got, near, ahead, c_conv, within, cols,
            final_valve_preactivation, clustered_rescale_factor[None],
        ),
        smem=1,
    )
    gathered = lax.all_gather(
        lax.all_to_all(copies, "y", 0, 0, tiled=True), "c", axis=1, tiled=True
    )
    stream, outgoing = call(
        stream_kernel,
        "stream",
        [((length, width), bf16), ((slots, width), bf16)],
        (gathered, final_projection_weights, skip_stream_entering, rows),
    )
    arrived = lax.all_to_all(
        outgoing.reshape(blocks, capacity, width), SP, 0, 0, tiled=True
    ).reshape(slots, width)
    own = to_all(arrived, "y")
    theirs = swapped(own)
    chunk = 256
    wide = (peers_y, 2, 128)
    gain = specialist_rescale_factor.reshape(wide)
    weight_gate = specialist_gating_weights.reshape(*wide, -1)
    weight_up = specialist_raising_weights.reshape(*wide, -1)
    weight_down = specialist_lowering_weights[0]
    units = weight_down.shape[0]
    half = pltpu.VMEM((D // 2, units), bf16)
    down_half = pltpu.VMEM((units, D // 2), bf16)
    scaled = pltpu.VMEM((chunk, D // 2), bf16)
    squares, gate, upward = call(
        functools.partial(first_half_kernel, chunk),
        "first_half",
        [((slots, 128), f32), ((slots, units), f32), ((slots, units), f32)],
        (place, own, gain, weight_gate, weight_up),
        flops=4 * slots * units * D // 2,
        scratch=[scaled, half, half],
        smem=1,
        room=16,
    )
    hidden, sent = call(
        functools.partial(second_half_kernel, chunk),
        "second_half",
        [((slots, units), bf16), ((peers_y, slots, width), bf16)],
        (place, theirs, gain, weight_gate, weight_up, weight_down, squares, gate, upward),
        flops=6 * slots * units * D // 2,
        scratch=[scaled, half, half, down_half],
        smem=1,
        room=20,
    )
    partner = swapped(sent)
    (kept,) = call(
        functools.partial(own_half_kernel, chunk),
        "own_half",
        [((peers_y, slots, width), bf16)],
        (place, hidden, weight_down),
        flops=2 * slots * units * D // 2,
        scratch=[down_half],
        smem=1,
        room=12,
    )
    pair = (kept.astype(f32) + partner.astype(f32)).astype(bf16)
    whole = lax.all_to_all(pair, "y", 0, 0, tiled=True)
    answer = jnp.sum(whole.astype(f32), axis=0).astype(bf16)
    returned = lax.all_to_all(
        answer.reshape(blocks, capacity, width), SP, 0, 0, tiled=True
    ).reshape(slots, width)
    (out,) = call(final_kernel, "final", [((length, width), bf16)], (returned, stream, cols))
    return out


def solution(mesh):
    sizes = dict(mesh.shape)
    torus = Mesh(mesh.devices.reshape(8, 4, sizes["tp"] // 2, 2), ("z", "x", "y", "c"))
    return jax.shard_map(
        body,
        mesh=torus,
        in_specs=(
            P(SP, TP),
            P(SP, TP),
            P(SP, TP),
            P(SP, TP),
            P(SP, TP),
            P(None, TP, SP),
            P(None, TP, SP),
            P(None, TP),
            P(None, TP),
            P(None, TP),
            P(None, TP),
            P(TP),
            P(None, TP),
            P(),
            P(SP, None),
            P(SP),
            P(SP, None),
            P(SP, None, TP),
            P(SP, None, TP),
            P(SP, TP, None),
        ),
        out_specs=P(SP, TP),
        check_vma=False,
    )
```

time: 194 us -> 179 us (0.923)
  waiting for transfers between devices: 33.5 us -> 16.6 us
  blocking collectives: 97.1 us -> 109 us
  other arithmetic: 7.66 us -> 0.51 us
  Pallas kernels: 6.37 us -> 11.4 us
  starting transfers between devices: 33.7 us -> 30.4 us
  matrix products: 3.24 us -> 0 us
    all_to_all x2 -> x3, blocking collectives: 19.4 us -> 41.4 us  [the longest x1 16 us: body(): lax.all_to_all(copies, 'y', 0, 0, tiled=True)]
    all_to_all x4 -> x2, waiting for transfers between devices: 33.5 us -> 15 us  [the longest x1 9.42 us: body(): got = lax.all_to_all(onward, 'z', 0, 0, tiled=True)]
    all_to_all x4 -> x2, starting transfers between devices: 28.4 us -> 17.6 us  [the longest x1 12.4 us: body(): got = lax.all_to_all(onward, 'z', 0, 0, tiled=True)]
    all_to_all x2 -> x1, blocking collectives: 38 us -> 28.9 us  [to_all(): return lax.all_to_all(copies, axis, 0, 0, tiled=True)]
    ppermute x2 -> x4, starting transfers between devices: 5.23 us -> 12.7 us  [the longest x2 7.51 us: swapped(): return lax.ppermute(value, 'c', [(0, 1), (1, 0)])]
    pallas_call x1 -> x10, Pallas kernels: 6.37 us -> 11.4 us  [call(): pl.pallas_call(kernel, out_shape=shapes, in_specs=[SMEM] * smem + [VMEM]...]
    unnamed x19 -> x38, local copies, waits for them, and re-layouts: 3.12 us -> 7.74 us
    reduce_sum x9 -> x1, other arithmetic: 4.44 us -> 0.15 us  [body(): answer = jnp.sum(whole.astype(f32), axis=0).astype(bf16)]
  transfers between devices with their start and end apart: 6 -> 6, of which waited for: 4 -> 4; matrix products, arithmetic and copies ran while one was open for 3% -> 0% of each run, Pallas kernels for 0% -> 2%
where the time goes in v2:
time: 179 us; the launch traced here: 178 us
  blocking collectives  109 us (61%)
  starting transfers between devices  30.4 us (17%)
  waiting for transfers between devices  16.6 us (9%)
  Pallas kernels  11.4 us (6%)
  local copies, waits for them, and re-layouts  10.1 us (6%)
    all_to_all x1, blocking collectives, body(): whole = lax.all_to_all(pair, 'y', 0, 0, tiled=True)  31.6 us
    all_to_all x1, blocking collectives, to_all(): return lax.all_to_all(copies, axis, 0, 0, tiled=True)  28.9 us
    all_to_all x1, blocking collectives, body(): lax.all_to_all(copies, 'y', 0, 0, tiled=True)  16 us
    all_to_all x1, blocking collectives, body(): lax.all_to_all(outgoing.reshape(blocks, capacity, width), SP, 0, 0, tiled...  12.7 us
    all_to_all x1, blocking collectives, body(): lax.all_to_all(answer.reshape(blocks, capacity, width), SP, 0, 0, tiled=T...  12.7 us
    all_to_all x1, starting transfers between devices, body(): got = lax.all_to_all(onward, 'z', 0, 0, tiled=True)  12.4 us
    pallas_call x10, Pallas kernels, call(): pl.pallas_call(kernel, out_shape=shapes, in_specs=[SMEM] * smem + [VMEM]...  11.4 us
    all_to_all x1, waiting for transfers between devices, body(): got = lax.all_to_all(onward, 'z', 0, 0, tiled=True)  9.42 us
  transfers between devices with their start and end apart: 6, of which 4 were waited for; matrix products, arithmetic and copies ran while one was open for 0% of the time, Pallas kernels for 2%

profile of v2, /device:TPU:1, one launch (start us, length us, event | category | flops | bytes accessed | tf_op | source)
XLA Modules:
  0.0 178.0 jit_solution(8580434038335439916)
XLA Ops:
  0.0 0.7 fusion.2
  0.7 0.7 fusion
  1.5 3.9 %collective-permute-start = (f32[2,384]{1,0:T(2,128)S(1)}, f32[2,384]{1,0:T(2,128)S(1)}, u32[]{:S(2)}, u32[]{:S(2)}) collective-permute-start(f32[2,384]{1,0:T(2,128)S(1)} %maximum_convert_fusion), channel_id=1, source_target_pairs={{0,16},{16,32},{32,48},{48,64},{64,80},{80,96},{96,112},{112,128},... | collective-permute-start | bytes 9224 | tf_op jit(solution)/shard_map/ppermute | solution.py:386
  5.4 1.3 collective-permute-start.1
  6.7 0.8 copy.21.speed_ref
  7.5 0.7 copy-done.14
  8.2 0.7 copy-done.15
  8.9 0.7 copy-done.16
  9.5 0.7 copy-done.17
  10.2 0.7 copy-done.18
  10.9 0.6 table.1
  11.6 0.0 copy-start.4
  11.6 0.7 copy-done.4
  12.3 0.8 copy-done.5
  13.1 0.8 copy-done.6
  13.8 0.7 copy-done.10
  14.5 0.7 copy-done.11
  15.2 0.7 copy-done.12
  15.9 1.3 conv.1
  17.2 5.2 %all-to-all-start = ((bf16[4,272,128]{2,1,0:T(8,128)(2,1)}), bf16[4,272,128]{2,1,0:T(8,128)(2,1)S(1)}, u32[]{:S(2)}, u32[]{:S(2)}) async-start(bf16[4,272,128]{2,1,0:T(8,128)(2,1)} %get-tuple-element.22), calls=%async_computation | async-start | bytes 557056 | tf_op jit(solution)/shard_map/all_to_all | solution.py:411
  22.3 0.1 pad_add_fusion.place_ref
  22.4 5.5 %all-to-all-done.seen_ref = bf16[4,272,128]{2,1,0:T(8,128)(2,1)S(1)} async-done(((bf16[4,272,128]{2,1,0:T(8,128)(2,1)}), bf16[4,272,128]{2,1,0:T(8,128)(2,1)S(1)}, u32[]{:S(2)}, u32[]{:S(2)}) %all-to-all-start) | async-done | bytes 278560 | tf_op jit(solution)/shard_map/all_to_all | solution.py:411
  27.9 1.3 row.1
  29.3 12.4 %all-to-all-start.1 = ((bf16[8,144,128]{2,1,0:T(8,128)(2,1)}), bf16[8,144,128]{2,1,0:T(8,128)(2,1)S(1)}, u32[]{:S(2)}, u32[]{:S(2)}) async-start(bf16[8,144,128]{2,1,0:T(8,128)(2,1)} %get-tuple-element.23), calls=%async_computation.1 | async-start | bytes 589824 | tf_op jit(solution)/shard_map/all_to_all | solution.py:426
  41.7 0.4 within.1.within_ref
  42.2 9.4 %all-to-all-done.1.got_ref = bf16[8,144,128]{2,1,0:T(8,128)(2,1)S(1)} async-done(((bf16[8,144,128]{2,1,0:T(8,128)(2,1)}), bf16[8,144,128]{2,1,0:T(8,128)(2,1)S(1)}, u32[]{:S(2)}, u32[]{:S(2)}) %all-to-all-start.1) | async-done | bytes 294944 | tf_op jit(solution)/shard_map/all_to_all | solution.py:426
  51.6 1.1 mixed.1
  52.7 16.0 %all_to_all.35 = bf16[8,128,128]{2,1,0:T(8,128)(2,1)S(1)} all-to-all(bf16[8,128,128]{2,1,0:T(8,128)(2,1)S(1)} %mixed.1), channel_id=1, replica_groups=mesh['z'=8,'x'=4,'y'=8,'c'=2] {'y'}, dimensions={0} | all-to-all | bytes 524288 | tf_op jit(solution)/shard_map/all_to_all | solution.py:438
  68.7 6.9 %all_gather.3.mixed_ref = bf16[8,256,128]{2,1,0:T(8,128)(2,1)S(1)} all-gather(bf16[8,128,128]{2,1,0:T(8,128)(2,1)S(1)} %all_to_all.35), channel_id=1, replica_groups=mesh['z'=8,'x'=4,'y'=8,'c'=2] {'c'}, dimensions={1}, use_global_device_ids=true | all-gather | bytes 786432 | tf_op jit(solution)/shard_map/all_gather | solution.py:437
  75.6 0.5 stream.1
  76.1 12.7 %all_to_all.36 = bf16[32,16,128]{2,1,0:T(8,128)(2,1)S(1)} all-to-all(bf16[32,16,128]{2,1,0:T(8,128)(2,1)S(1)} %bitcast.23), channel_id=1, replica_groups=mesh['z'=8,'x'=4,'y'=8,'c'=2] {'z','x'}, dimensions={0} | all-to-all | bytes 262144 | tf_op jit(solution)/shard_map/all_to_all | solution.py:446
  88.9 0.1 broadcast_in_dim.20
  89.0 0.0 copy-start.1
  89.0 0.0 copy-start.2
  89.0 28.9 %all_to_all.37.rows_ref = bf16[8,512,128]{2,1,0:T(8,128)(2,1)S(1)} all-to-all(bf16[8,512,128]{2,1,0:T(8,128)(2,1)S(1)} %broadcast_in_dim.20), channel_id=1, replica_groups=mesh['z'=8,'x'=4,'y'=8,'c'=2] {'y'}, dimensions={0} | all-to-all | bytes 2097152 | tf_op jit(solution)/shard_map/all_to_all | solution.py:349
  117.9 5.2 %collective-permute-start.2 = (bf16[8,512,128]{2,1,0:T(8,128)(2,1)S(1)}, bf16[8,512,128]{2,1,0:T(8,128)(2,1)S(1)}, u32[]{:S(2)}, u32[]{:S(2)}) collective-permute-start(bf16[8,512,128]{2,1,0:T(8,128)(2,1)S(1)} %all_to_all.37.rows_ref), channel_id=1, source_target_pairs={{0,1},{1,0},{2,3},{3,2},{4,5},{5,4},{6,7},{7,6},{8,9},{9,8},{10,11... | collective-permute-start | bytes 3145736 | tf_op jit(solution)/shard_map/ppermute | solution.py:343
  123.2 0.0 copy-start
  123.2 1.6 first_half.1
  124.8 0.6 collective-permute-done.2.rows_ref
  125.4 2.4 %second_half.1 = (bf16[512,256]{1,0:T(8,128)(2,1)S(1)}, bf16[8,512,128]{2,1,0:T(8,128)(2,1)S(1)}) custom-call(s32[3]{0:T(128)S(1)} %pad_add_fusion.place_ref, bf16[8,512,128]{2,1,0:T(8,128)(2,1)S(1)} %collective-permute-done.2.rows_ref, f32[8,2,128]{2,1,0:T(2,128)S(1)} %bitcast.25, bf16[8,2,128,256]{3,2,1,0:T(8,128)(2,1)S(1)} %bitcast.19, ...), custom_call_target="tpu_custom_call" | custom-call | flops 805306368 | bytes 6823948 | tf_op jit(solution)/shard_map/second_half/pallas_call | solution.py:32
  127.8 2.3 %collective-permute-start.3 = (bf16[8,512,128]{2,1,0:T(8,128)(2,1)S(1)}, bf16[8,512,128]{2,1,0:T(8,128)(2,1)S(1)}, u32[]{:S(2)}, u32[]{:S(2)}) collective-permute-start(bf16[8,512,128]{2,1,0:T(8,128)(2,1)S(1)} %get-tuple-element.35), channel_id=1, source_target_pairs={{0,1},{1,0},{2,3},{3,2},{4,5},{5,4},{6,7},{7,6},{8,9},{9,8},{10,11... | collective-permute-start | bytes 3145736 | tf_op jit(solution)/shard_map/ppermute | solution.py:343
  130.1 1.3 own_half.1
  131.4 1.0 collective-permute-done.3
  132.4 0.3 add_convert_fusion
  132.7 31.6 %all_to_all.38 = bf16[8,512,128]{2,1,0:T(8,128)(2,1)S(1)} all-to-all(bf16[8,512,128]{2,1,0:T(8,128)(2,1)S(1)} %add_convert_fusion), channel_id=1, replica_groups=mesh['z'=8,'x'=4,'y'=8,'c'=2] {'y'}, dimensions={0} | all-to-all | bytes 2097152 | tf_op jit(solution)/shard_map/all_to_all | solution.py:493
  164.3 0.1 reduce_sum.12
  164.4 12.7 %all_to_all.39 = bf16[32,16,128]{2,1,0:T(8,128)(2,1)S(1)} all-to-all(bf16[32,16,128]{2,1,0:T(8,128)(2,1)S(1)} %bitcast.30), channel_id=1, replica_groups=mesh['z'=8,'x'=4,'y'=8,'c'=2] {'z','x'}, dimensions={0} | all-to-all | bytes 262144 | tf_op jit(solution)/shard_map/all_to_all | solution.py:495
  177.1 0.9 final.1
  (27 shorter events, 0.1 us)
Async XLA Ops:
  0.0 51.6 %copy-start.13 = (f32[128]{0:T(128)S(1)}, f32[128]{0:T(128)}, u32[]{:S(2)}) copy-start(f32[128]{0:T(128)} %param.31) | copy-start | bytes 1540
  0.0 51.6 %copy-start.8 = (bf16[128,128]{1,0:T(8,128)(2,1)S(1)}, bf16[128,128]{1,0:T(8,128)(2,1)}, u32[]{:S(2)}) copy-start(bf16[128,128]{1,0:T(8,128)(2,1)} %valve_ref.1) | copy-start | bytes 98308
  1.5 10.1 %collective-permute-start = (f32[2,384]{1,0:T(2,128)S(1)}, f32[2,384]{1,0:T(2,128)S(1)}, u32[]{:S(2)}, u32[]{:S(2)}) collective-permute-start(f32[2,384]{1,0:T(2,128)S(1)} %maximum_convert_fusion), channel_id=1, source_target_pairs={{0,16},{16,32},{32,48},{48,64},{64,80},{80,96},{96,112},{112,128},... | collective-permute-start | bytes 9224 | tf_op jit(solution)/shard_map/ppermute | solution.py:386
  5.4 6.1 %collective-permute-start.1 = (f32[2,384]{1,0:T(2,128)S(1)}, f32[2,384]{1,0:T(2,128)S(1)}, u32[]{:S(2)}, u32[]{:S(2)}) collective-permute-start(f32[2,384]{1,0:T(2,128)S(1)} %maximum_convert_fusion.1), channel_id=1, source_target_pairs={{16,0},{32,16},{48,32},{64,48},{80,64},{96,80},{112,96},{128,112},... | collective-permute-start | bytes 9224 | tf_op jit(solution)/shard_map/ppermute | solution.py:387
  7.5 0.7 copy-start.14
  8.2 0.7 copy-start.15
  8.9 0.7 copy-start.16
  9.5 0.7 copy-start.17
  10.2 0.7 copy-start.18
  11.6 0.8 copy-start.4
  12.3 0.8 copy-start.5
  13.1 0.8 copy-start.6
  13.8 0.7 copy-start.10
  14.5 0.7 copy-start.11
  15.2 0.7 copy-start.12
  17.2 10.8 %all-to-all-start = ((bf16[4,272,128]{2,1,0:T(8,128)(2,1)}), bf16[4,272,128]{2,1,0:T(8,128)(2,1)S(1)}, u32[]{:S(2)}, u32[]{:S(2)}) async-start(bf16[4,272,128]{2,1,0:T(8,128)(2,1)} %get-tuple-element.22), calls=%async_computation | async-start | bytes 557056 | tf_op jit(solution)/shard_map/all_to_all | solution.py:411
  29.3 22.3 %all-to-all-start.1 = ((bf16[8,144,128]{2,1,0:T(8,128)(2,1)}), bf16[8,144,128]{2,1,0:T(8,128)(2,1)S(1)}, u32[]{:S(2)}, u32[]{:S(2)}) async-start(bf16[8,144,128]{2,1,0:T(8,128)(2,1)} %get-tuple-element.23), calls=%async_computation.1 | async-start | bytes 589824 | tf_op jit(solution)/shard_map/all_to_all | solution.py:426
  51.6 24.0 %copy-start.3 = (bf16[2048,128]{1,0:T(8,128)(2,1)S(1)}, bf16[2048,128]{1,0:T(8,128)(2,1)}, u32[]{:S(2)}) copy-start(bf16[2048,128]{1,0:T(8,128)(2,1)} %weight_ref.1) | copy-start | bytes 1572868
  51.6 24.0 %copy-start.9 = (bf16[128,128]{1,0:T(8,128)(2,1)S(1)}, bf16[128,128]{1,0:T(8,128)(2,1)}, u32[]{:S(2)}) copy-start(bf16[128,128]{1,0:T(8,128)(2,1)} %skip_ref.1) | copy-start | bytes 98308
  88.9 34.3 %copy-start.7 = (f32[2048]{0:T(1024)S(1)}, f32[2048]{0:T(1024)}, u32[]{:S(2)}) copy-start(f32[2048]{0:T(1024)} %param.33) | copy-start | bytes 24580
  89.0 34.2 %copy-start.1 = (bf16[1,2048,256]{2,1,0:T(8,128)(2,1)S(1)}, bf16[1,2048,256]{2,1,0:T(8,128)(2,1)}, u32[]{:S(2)}) copy-start(bf16[1,2048,256]{2,1,0:T(8,128)(2,1)} %param.37) | copy-start | bytes 3145732
  89.0 34.2 %copy-start.2 = (bf16[1,2048,256]{2,1,0:T(8,128)(2,1)S(1)}, bf16[1,2048,256]{2,1,0:T(8,128)(2,1)}, u32[]{:S(2)}) copy-start(bf16[1,2048,256]{2,1,0:T(8,128)(2,1)} %param.38) | copy-start | bytes 3145732
  117.9 7.5 %collective-permute-start.2 = (bf16[8,512,128]{2,1,0:T(8,128)(2,1)S(1)}, bf16[8,512,128]{2,1,0:T(8,128)(2,1)S(1)}, u32[]{:S(2)}, u32[]{:S(2)}) collective-permute-start(bf16[8,512,128]{2,1,0:T(8,128)(2,1)S(1)} %all_to_all.37.rows_ref), channel_id=1, source_target_pairs={{0,1},{1,0},{2,3},{3,2},{4,5},{5,4},{6,7},{7,6},{8,9},{9,8},{10,11... | collective-permute-start | bytes 3145736 | tf_op jit(solution)/shard_map/ppermute | solution.py:343
  123.2 2.2 %copy-start = (bf16[1,256,2048]{2,1,0:T(8,128)(2,1)S(1)}, bf16[1,256,2048]{2,1,0:T(8,128)(2,1)}, u32[]{:S(2)}) copy-start(bf16[1,256,2048]{2,1,0:T(8,128)(2,1)} %param.39) | copy-start | bytes 3145732
  127.8 4.6 %collective-permute-start.3 = (bf16[8,512,128]{2,1,0:T(8,128)(2,1)S(1)}, bf16[8,512,128]{2,1,0:T(8,128)(2,1)S(1)}, u32[]{:S(2)}, u32[]{:S(2)}) collective-permute-start(bf16[8,512,128]{2,1,0:T(8,128)(2,1)S(1)} %get-tuple-element.35), channel_id=1, source_target_pairs={{0,1},{1,0},{2,3},{3,2},{4,5},{5,4},{6,7},{7,6},{8,9},{9,8},{10,11... | collective-permute-start | bytes 3145736 | tf_op jit(solution)/shard_map/ppermute | solution.py:343

commit v3 on v2

--- a/solution.py
+++ b/solution.py
@@ -21,18 +21,22 @@
 
 VMEM = pl.BlockSpec(memory_space=pltpu.VMEM)
 SMEM = pl.BlockSpec(memory_space=pltpu.SMEM)
+HBM = pl.BlockSpec(memory_space=pltpu.HBM)
 MIB = 1 << 20
 
 
-def call(kernel, name, outs, args, flops=1000, scratch=(), room=8, smem=0):
+def call(kernel, name, outs, args, flops=1000, scratch=(), room=8, smem=0, hbm=0):
     shapes = [jax.ShapeDtypeStruct(shape, dtype) for shape, dtype in outs]
     moved = sum(a.size * a.dtype.itemsize for a in args) + sum(
         o.size * o.dtype.itemsize for o in shapes
     )
+    args = list(args)
+    for n in range(smem, smem + hbm):
+        args[n] = pltpu.with_memory_space_constraint(args[n], pltpu.HBM)
     return pl.pallas_call(
         kernel,
         out_shape=shapes,
-        in_specs=[SMEM] * smem + [VMEM] * (len(args) - smem),
+        in_specs=[SMEM] * smem + [HBM] * hbm + [VMEM] * (len(args) - smem - hbm),
         out_specs=[VMEM] * len(shapes),
         scratch_shapes=list(scratch),
         compiler_params=pltpu.CompilerParams(vmem_limit_bytes=room * MIB),
@@ -59,13 +63,48 @@
     return lax.broadcasted_iota(jnp.int32, shape, dim)
 
 
-def table_kernel(capacity, step_ref, fade_ref, speed_ref, named_ref, like_ref, score_ref, row_ref, col_ref):
+def fetch(pairs, done):
+    copies = [pltpu.make_async_copy(a, b, done.at[n]) for n, (a, b) in enumerate(pairs)]
+    for copy in copies:
+        copy.start()
+    for copy in copies:
+        copy.wait()
+
+
+def rim_kernel(place_ref, x_in, b_in, c_in, even_ref, odd_ref, x_ref, b_ref, c_ref, done):
+    fetch(((x_in, x_ref), (b_in, b_ref), (c_in, c_ref)), done)
+    even = place_ref[3] == 0
+    length, width = x_ref.shape
+    for n, ref in enumerate((x_ref, b_ref, c_ref)):
+        lanes = slice(n * width, (n + 1) * width)
+        top = ref[0:16, :].astype(jnp.float32)[0:2]
+        tail = ref[length - 16 : length, :].astype(jnp.float32)[14:16]
+        even_ref[:, lanes] = jnp.where(even, tail, top)
+        odd_ref[:, lanes] = jnp.where(even, top, tail)
+
+
+def table_kernel(
+    capacity, step_in, fade_in, speed_in, named_in, like_in, score_in, kx_in, kb_in, kc_in,
+    row_ref, col_ref, kx_ref, kb_ref, kc_ref,
+    step_ref, fade_ref, speed_ref, named_ref, like_ref, score_ref, done,
+):
+    fetch(
+        (
+            (step_in, step_ref), (fade_in, fade_ref), (speed_in, speed_ref), (named_in, named_ref),
+            (like_in, like_ref), (score_in, score_ref), (kx_in, kx_ref), (kb_in, kb_ref), (kc_in, kc_ref),
+        ),
+        done,
+    )
     length = row_ref.shape[1]
     for d in range(2):
         raw = step_ref[d]
         step = jnp.maximum(raw, 0.0) + jnp.log1p(jnp.exp(-jnp.abs(raw)))
-        row_ref[2 * d : 2 * d + 2, :] = -step * speed_ref[d] + fade_ref[d]
         row_ref[4 + 2 * d : 6 + 2 * d, :] = step
+        for h in range(2):
+            k = 2 * d + h
+            row_ref[k : k + 1, :] = (
+                -step[h : h + 1] * speed_ref[d : d + 1, h : h + 1] + fade_ref[d][h : h + 1]
+            )
     whole = row_ref[0:8, :]
     lane, line = iota(whole.shape, 1), iota(whole.shape, 0)
     ahead = behind = whole
@@ -97,16 +136,19 @@
 
 
 def conv_kernel(
-    x_ref, b_ref, c_ref, before_ref, after_ref, kx_ref, kb_ref, kc_ref, col_ref,
+    place_ref, x_ref, b_ref, c_ref, even_ref, odd_ref, kx_ref, kb_ref, kc_ref, col_ref,
     message_ref, xs_ref, bs_ref, cs_ref, padded,
 ):
     length, width = x_ref.shape
+    even = place_ref[3] == 0
+    before = jnp.where(even, odd_ref[...], even_ref[...])
+    after = jnp.where(even, even_ref[...], odd_ref[...])
     parts = []
     for n, (ref, taps) in enumerate(((x_ref, kx_ref), (b_ref, kb_ref), (c_ref, kc_ref))):
         lanes = slice(n * width, (n + 1) * width)
         padded[8 : 8 + length, :] = ref[...].astype(jnp.float32)
-        padded[6:8, :] = before_ref[:, lanes]
-        padded[8 + length : 10 + length, :] = after_ref[:, lanes]
+        padded[6:8, :] = before[:, lanes]
+        padded[8 + length : 10 + length, :] = after[:, lanes]
         total = jnp.zeros((length, width), jnp.float32)
         for k in range(CONV):
             total = total + taps[k : k + 1, :] * padded[6 + k : 6 + k + length, :]
@@ -134,7 +176,7 @@
         message_ref[peer, 2 * width :, :] = logs.astype(jnp.bfloat16)
 
 
-def within_kernel(xs_ref, bs_ref, cs_ref, row_ref, col_ref, out_ref):
+def within(xs_ref, bs_ref, cs_ref, row_ref, col_ref):
     length, width = xs_ref.shape
     scores = dot_rows(cs_ref[...], bs_ref[...])
     x_block = xs_ref[...].astype(jnp.float32)
@@ -149,7 +191,7 @@
             decay = jnp.where(seen, jnp.exp(jnp.minimum(passed, 0.0)), 0.0)
             both = both + decay * row_ref[4 + k : 5 + k, :]
         sides.append(exact_dot(scores * both, x_block))
-    out_ref[...] = jnp.where(iota((length, width), 1) < HD, sides[0], sides[1])
+    return jnp.where(iota((length, width), 1) < HD, sides[0], sides[1])
 
 
 def log_pair(tile, d):
@@ -194,14 +236,15 @@
 
 
 def mixed_kernel(
-    place_ref, got_ref, near_ref, ahead_ref, cs_ref, within_ref, col_ref, valve_ref, gain_ref, out_ref
+    place_ref, got_ref, near_ref, ahead_ref, xs_ref, bs_ref, cs_ref, row_ref, col_ref, valve_ref, gain_ref,
+    out_ref,
 ):
     my_z = place_ref[1]
     peers, rows = got_ref.shape[0], near_ref.shape[1]
     length = cs_ref.shape[0]
     c_block = cs_ref[...].astype(jnp.float32)
     left = iota((length, rows), 1) < HD
-    mixer = within_ref[...]
+    mixer = within(xs_ref, bs_ref, cs_ref, row_ref, col_ref)
     for d in range(2):
         state = jnp.zeros((rows, 128), jnp.float32)
         for k in range(peers) if d == 0 else reversed(range(peers)):
@@ -377,45 +420,60 @@
     peers_x, peers_y, peers_z = (lax.axis_size(a) for a in ("x", "y", "z"))
     capacity = 4 * length // blocks
     slots = blocks * capacity
-    place = jnp.stack([lax.axis_index("x"), lax.axis_index("z"), lax.axis_index("c")]).astype(jnp.int32)
+    axes = [lax.axis_index(a) for a in ("x", "z", "c")]
+    place = jnp.stack([*axes, axes[0] % 2]).astype(jnp.int32)
 
     rim = CONV // 2
-    feeds = (unfiltered_channel_feed, unfiltered_state_entry, unfiltered_state_exit)
-    tail = jnp.concatenate([a[-rim:] for a in feeds], axis=1).astype(f32)
-    top = jnp.concatenate([a[:rim] for a in feeds], axis=1).astype(f32)
-    before = lax.ppermute(tail, SP, [(i, i + 1) for i in range(blocks - 1)])
-    after = lax.ppermute(top, SP, [(i + 1, i) for i in range(blocks - 1)])
-
-    rows, cols = call(
+    even_rim, odd_rim, *feeds = call(
+        rim_kernel,
+        "rim",
+        [((rim, 3 * width), f32)] * 2 + [((length, width), bf16)] * 3,
+        (place, unfiltered_channel_feed, unfiltered_state_entry, unfiltered_state_exit),
+        flops=100_000,
+        scratch=[pltpu.SemaphoreType.DMA((3,))],
+        smem=1,
+        hbm=3,
+    )
+    pairs = [(i, i + 1) for i in range(blocks - 1)]
+    even_rim = lax.ppermute(even_rim, SP, [p for a, b in pairs[0::2] for p in ((a, b), (b, a))])
+    odd_rim = lax.ppermute(odd_rim, SP, [p for a, b in pairs[1::2] for p in ((a, b), (b, a))])
+    filters = (channel_feed_filter, state_entry_filter, state_exit_filter)
+    heads = increment_preactivation.shape[1]
+    rows, cols, *filters = call(
         functools.partial(table_kernel, capacity),
         "table",
-        [((16, length), f32), ((length, length), f32)],
+        [((16, length), f32), ((length, length), f32)] + [((CONV, width), f32)] * 3,
         (
             increment_preactivation,
             summed_attenuation_both_ways,
-            channel_fading_speed[:, :, None],
+            channel_fading_speed,
             item_specialist_couple.T,
             selected_cluster_likelihood[None],
             selected_twin_scores_raw.T,
+            *filters,
         ),
         flops=4_000_000,
+        scratch=[
+            pltpu.VMEM((2, heads, length), f32),
+            pltpu.VMEM((2, heads, length), f32),
+            pltpu.VMEM((2, heads), f32),
+            pltpu.VMEM((2, length), jnp.int32),
+            pltpu.VMEM((1, length), f32),
+            pltpu.VMEM((2, length), f32),
+            pltpu.SemaphoreType.DMA((9,)),
+        ],
+        hbm=9,
     )
     message, x_conv, b_conv, c_conv = call(
         conv_kernel,
         "conv",
         [((peers_x, 2 * width + 16, NS), bf16)] + [((length, width), bf16)] * 3,
-        (*feeds, before, after, channel_feed_filter, state_entry_filter, state_exit_filter, cols),
+        (place, *feeds, even_rim, odd_rim, *filters, cols),
         flops=4_000_000,
         scratch=[pltpu.VMEM((length + 16, width), f32)],
+        smem=1,
     )
     seen = lax.all_to_all(message, "x", 0, 0, tiled=True)
-    (within,) = call(
-        within_kernel,
-        "within",
-        [((length, width), f32)],
-        (x_conv, b_conv, c_conv, rows, cols),
-        flops=40_000_000,
-    )
     onward, near, ahead = call(
         row_kernel,
         "row",
@@ -429,7 +487,7 @@
         "mixed",
         [((peers_y, length, width), bf16)],
         (
-            place, got, near, ahead, c_conv, within, cols,
+            place, got, near, ahead, x_conv, b_conv, c_conv, rows, cols,
             final_valve_preactivation, clustered_rescale_factor[None],
         ),
         smem=1,

time: 179 us -> 170 us (0.950)
  blocking collectives: 109 us -> 143 us
  starting transfers between devices: 30.4 us -> 12.1 us
  waiting for transfers between devices: 16.6 us -> 1.61 us
  local copies, waits for them, and re-layouts: 10.1 us -> 0.17 us
    all_to_all x0 -> x2, blocking collectives: none -> 32.9 us  [the longest x1 20.2 us: body(): got = lax.all_to_all(onward, 'z', 0, 0, tiled=True)]
    all_to_all x2 -> x0, starting transfers between devices: 17.6 us -> none  [the longest x1 12.4 us: body(): got = lax.all_to_all(onward, 'z', 0, 0, tiled=True)]
    all_to_all x2 -> x0, waiting for transfers between devices: 15 us -> none  [the longest x1 9.42 us: body(): got = lax.all_to_all(onward, 'z', 0, 0, tiled=True)]
    unnamed x38 -> x16, local copies, waits for them, and re-layouts: 7.74 us -> 0.04 us
  transfers between devices with their start and end apart: 6 -> 4, of which waited for: 4 -> 2; matrix products, arithmetic and copies ran while one was open for 0% -> 0% of each run, Pallas kernels for 2% -> 3%
where the time goes in v3:
time: 170 us
  blocking collectives  143 us (84%)
  Pallas kernels  12.7 us (7%)
  starting transfers between devices  12.1 us (7%)
    all_to_all x1, blocking collectives, body(): whole = lax.all_to_all(pair, 'y', 0, 0, tiled=True)  31.6 us
    all_to_all x1, blocking collectives, to_all(): return lax.all_to_all(copies, axis, 0, 0, tiled=True)  28.9 us
    all_to_all x1, blocking collectives, body(): got = lax.all_to_all(onward, 'z', 0, 0, tiled=True)  20.2 us
    all_to_all x1, blocking collectives, body(): lax.all_to_all(copies, 'y', 0, 0, tiled=True)  16 us
    all_to_all x1, blocking collectives, body(): lax.all_to_all(outgoing.reshape(blocks, capacity, width), SP, 0, 0, tiled...  12.7 us
    pallas_call x10, Pallas kernels, call(): pl.pallas_call(kernel, out_shape=shapes, in_specs=[SMEM] * smem + [HBM] *...  12.7 us
    all_to_all x1, blocking collectives, body(): seen = lax.all_to_all(message, 'x', 0, 0, tiled=True)  12.7 us
    all_to_all x1, blocking collectives, body(): lax.all_to_all(answer.reshape(blocks, capacity, width), SP, 0, 0, tiled=T...  12.7 us
  transfers between devices with their start and end apart: 4, of which 2 were waited for; matrix products, arithmetic and copies ran while one was open for 0% of the time, Pallas kernels for 3%

profile of v3, /device:TPU:1, one launch (start us, length us, event | category | flops | bytes accessed | tf_op | source)
XLA Modules:
  0.0 169.9 jit_solution(11452084065646743434)
XLA Ops:
  0.0 0.0 copy-start.7
  0.0 0.0 copy-start.5
  0.0 0.1 pad_add_fusion.place_ref
  0.1 1.4 rim.1
  1.5 3.9 %collective-permute-start = (f32[2,384]{1,0:T(2,128)S(1)}, f32[2,384]{1,0:T(2,128)S(1)}, u32[]{:S(2)}, u32[]{:S(2)}) collective-permute-start(f32[2,384]{1,0:T(2,128)S(1)} %get-tuple-element.32), channel_id=1, source_target_pairs={{0,16},{16,0},{32,48},{48,32},{64,80},{80,64},{96,112},{112,96},{1... | collective-permute-start | bytes 9224 | tf_op jit(solution)/shard_map/ppermute | solution.py:438
  5.4 0.7 collective-permute-start.1
  6.1 1.6 table.1
  7.6 0.0 collective-permute-done.even_ref
  7.6 0.0 collective-permute-done.1.odd_ref
  7.7 1.1 conv.1
  8.8 12.7 %all_to_all.35.seen_ref = bf16[4,272,128]{2,1,0:T(8,128)(2,1)S(1)} all-to-all(bf16[4,272,128]{2,1,0:T(8,128)(2,1)S(1)} %get-tuple-element.38), channel_id=1, replica_groups=mesh['z'=8,'x'=4,'y'=8,'c'=2] {'x'}, dimensions={0} | all-to-all | bytes 557056 | tf_op jit(solution)/shard_map/all_to_all | solution.py:476
  21.5 0.7 row.1
  22.1 20.2 %all_to_all.36.got_ref = bf16[8,144,128]{2,1,0:T(8,128)(2,1)S(1)} all-to-all(bf16[8,144,128]{2,1,0:T(8,128)(2,1)S(1)} %get-tuple-element.39), channel_id=1, replica_groups=mesh['z'=8,'x'=4,'y'=8,'c'=2] {'z'}, dimensions={0} | all-to-all | bytes 589824 | tf_op jit(solution)/shard_map/all_to_all | solution.py:484
  42.3 0.0 copy-done.7
  42.3 0.0 copy-done.5
  42.3 0.0 copy-start.3
  42.3 0.0 copy-start.6
  42.3 1.4 mixed.1
  43.7 16.0 %all_to_all.37 = bf16[8,128,128]{2,1,0:T(8,128)(2,1)S(1)} all-to-all(bf16[8,128,128]{2,1,0:T(8,128)(2,1)S(1)} %mixed.1), channel_id=1, replica_groups=mesh['z'=8,'x'=4,'y'=8,'c'=2] {'y'}, dimensions={0} | all-to-all | bytes 524288 | tf_op jit(solution)/shard_map/all_to_all | solution.py:496
  59.6 7.9 %all_gather.3.mixed_ref = bf16[8,256,128]{2,1,0:T(8,128)(2,1)S(1)} all-gather(bf16[8,128,128]{2,1,0:T(8,128)(2,1)S(1)} %all_to_all.37), channel_id=1, replica_groups=mesh['z'=8,'x'=4,'y'=8,'c'=2] {'c'}, dimensions={1}, use_global_device_ids=true | all-gather | bytes 786432 | tf_op jit(solution)/shard_map/all_gather | solution.py:495
  67.5 0.0 copy-done.3
  67.5 0.0 copy-done.6
  67.5 0.5 stream.1
  68.0 12.7 %all_to_all.38 = bf16[32,16,128]{2,1,0:T(8,128)(2,1)S(1)} all-to-all(bf16[32,16,128]{2,1,0:T(8,128)(2,1)S(1)} %bitcast.23), channel_id=1, replica_groups=mesh['z'=8,'x'=4,'y'=8,'c'=2] {'z','x'}, dimensions={0} | all-to-all | bytes 262144 | tf_op jit(solution)/shard_map/all_to_all | solution.py:504
  80.8 0.0 copy-start.4
  80.8 0.1 broadcast_in_dim.16
  80.9 0.0 copy-start.1
  81.0 0.0 copy-start.2
  81.0 28.9 %all_to_all.39.rows_ref = bf16[8,512,128]{2,1,0:T(8,128)(2,1)S(1)} all-to-all(bf16[8,512,128]{2,1,0:T(8,128)(2,1)S(1)} %broadcast_in_dim.16), channel_id=1, replica_groups=mesh['z'=8,'x'=4,'y'=8,'c'=2] {'y'}, dimensions={0} | all-to-all | bytes 2097152 | tf_op jit(solution)/shard_map/all_to_all | solution.py:392
  109.9 5.2 %collective-permute-start.2 = (bf16[8,512,128]{2,1,0:T(8,128)(2,1)S(1)}, bf16[8,512,128]{2,1,0:T(8,128)(2,1)S(1)}, u32[]{:S(2)}, u32[]{:S(2)}) collective-permute-start(bf16[8,512,128]{2,1,0:T(8,128)(2,1)S(1)} %all_to_all.39.rows_ref), channel_id=1, source_target_pairs={{0,1},{1,0},{2,3},{3,2},{4,5},{5,4},{6,7},{7,6},{8,9},{9,8},{10,11... | collective-permute-start | bytes 3145736 | tf_op jit(solution)/shard_map/ppermute | solution.py:386
  115.1 0.0 copy-done.4
  115.1 0.0 copy-done.1
  115.1 0.0 copy-done.2
  115.1 0.0 copy-start
  115.1 1.6 first_half.1
  116.7 0.6 collective-permute-done.2.rows_ref
  117.4 0.0 copy-done
  117.4 2.4 %second_half.1 = (bf16[512,256]{1,0:T(8,128)(2,1)S(1)}, bf16[8,512,128]{2,1,0:T(8,128)(2,1)S(1)}) custom-call(s32[4]{0:T(128)S(1)} %pad_add_fusion.place_ref, bf16[8,512,128]{2,1,0:T(8,128)(2,1)S(1)} %collective-permute-done.2.rows_ref, f32[8,2,128]{2,1,0:T(2,128)S(1)} %bitcast.25, bf16[8,2,128,256]{3,2,1,0:T(8,128)(2,1)S(1)} %bitcast.19, ...), custom_call_target="tpu_custom_call" | custom-call | flops 805306368 | bytes 6823952 | tf_op jit(solution)/shard_map/second_half/pallas_call | solution.py:36
  119.8 2.3 %collective-permute-start.3 = (bf16[8,512,128]{2,1,0:T(8,128)(2,1)S(1)}, bf16[8,512,128]{2,1,0:T(8,128)(2,1)S(1)}, u32[]{:S(2)}, u32[]{:S(2)}) collective-permute-start(bf16[8,512,128]{2,1,0:T(8,128)(2,1)S(1)} %get-tuple-element.51), channel_id=1, source_target_pairs={{0,1},{1,0},{2,3},{3,2},{4,5},{5,4},{6,7},{7,6},{8,9},{9,8},{10,11... | collective-permute-start | bytes 3145736 | tf_op jit(solution)/shard_map/ppermute | solution.py:386
  122.1 1.3 own_half.1
  123.4 1.0 collective-permute-done.3
  124.3 0.3 add_convert_fusion
  124.6 31.6 %all_to_all.40 = bf16[8,512,128]{2,1,0:T(8,128)(2,1)S(1)} all-to-all(bf16[8,512,128]{2,1,0:T(8,128)(2,1)S(1)} %add_convert_fusion), channel_id=1, replica_groups=mesh['z'=8,'x'=4,'y'=8,'c'=2] {'y'}, dimensions={0} | all-to-all | bytes 2097152 | tf_op jit(solution)/shard_map/all_to_all | solution.py:551
  156.2 0.1 reduce_sum.12
  156.3 12.7 %all_to_all.41 = bf16[32,16,128]{2,1,0:T(8,128)(2,1)S(1)} all-to-all(bf16[32,16,128]{2,1,0:T(8,128)(2,1)S(1)} %bitcast.27), channel_id=1, replica_groups=mesh['z'=8,'x'=4,'y'=8,'c'=2] {'z','x'}, dimensions={0} | all-to-all | bytes 262144 | tf_op jit(solution)/shard_map/all_to_all | solution.py:553
  169.0 0.9 final.1
Async XLA Ops:
  0.0 42.3 %copy-start.7 = (f32[128]{0:T(128)S(1)}, f32[128]{0:T(128)}, u32[]{:S(2)}) copy-start(f32[128]{0:T(128)} %param.31) | copy-start | bytes 1540
  0.0 42.3 %copy-start.5 = (bf16[128,128]{1,0:T(8,128)(2,1)S(1)}, bf16[128,128]{1,0:T(8,128)(2,1)}, u32[]{:S(2)}) copy-start(bf16[128,128]{1,0:T(8,128)(2,1)} %valve_ref.1) | copy-start | bytes 98308
  1.5 6.2 %collective-permute-start = (f32[2,384]{1,0:T(2,128)S(1)}, f32[2,384]{1,0:T(2,128)S(1)}, u32[]{:S(2)}, u32[]{:S(2)}) collective-permute-start(f32[2,384]{1,0:T(2,128)S(1)} %get-tuple-element.32), channel_id=1, source_target_pairs={{0,16},{16,0},{32,48},{48,32},{64,80},{80,64},{96,112},{112,96},{1... | collective-permute-start | bytes 9224 | tf_op jit(solution)/shard_map/ppermute | solution.py:438
  5.4 2.3 %collective-permute-start.1 = (f32[2,384]{1,0:T(2,128)S(1)}, f32[2,384]{1,0:T(2,128)S(1)}, u32[]{:S(2)}, u32[]{:S(2)}) collective-permute-start(f32[2,384]{1,0:T(2,128)S(1)} %get-tuple-element.33), channel_id=1, source_target_pairs={{16,32},{32,16},{48,64},{64,48},{80,96},{96,80},{112,128},{128,112... | collective-permute-start | bytes 9224 | tf_op jit(solution)/shard_map/ppermute | solution.py:439
  42.3 25.2 %copy-start.3 = (bf16[2048,128]{1,0:T(8,128)(2,1)S(1)}, bf16[2048,128]{1,0:T(8,128)(2,1)}, u32[]{:S(2)}) copy-start(bf16[2048,128]{1,0:T(8,128)(2,1)} %weight_ref.1) | copy-start | bytes 1572868
  42.3 25.2 %copy-start.6 = (bf16[128,128]{1,0:T(8,128)(2,1)S(1)}, bf16[128,128]{1,0:T(8,128)(2,1)}, u32[]{:S(2)}) copy-start(bf16[128,128]{1,0:T(8,128)(2,1)} %skip_ref.1) | copy-start | bytes 98308
  80.8 34.3 %copy-start.4 = (f32[2048]{0:T(1024)S(1)}, f32[2048]{0:T(1024)}, u32[]{:S(2)}) copy-start(f32[2048]{0:T(1024)} %param.33) | copy-start | bytes 24580
  80.9 34.2 %copy-start.1 = (bf16[1,2048,256]{2,1,0:T(8,128)(2,1)S(1)}, bf16[1,2048,256]{2,1,0:T(8,128)(2,1)}, u32[]{:S(2)}) copy-start(bf16[1,2048,256]{2,1,0:T(8,128)(2,1)} %param.37) | copy-start | bytes 3145732
  81.0 34.2 %copy-start.2 = (bf16[1,2048,256]{2,1,0:T(8,128)(2,1)S(1)}, bf16[1,2048,256]{2,1,0:T(8,128)(2,1)}, u32[]{:S(2)}) copy-start(bf16[1,2048,256]{2,1,0:T(8,128)(2,1)} %param.38) | copy-start | bytes 3145732
  109.9 7.5 %collective-permute-start.2 = (bf16[8,512,128]{2,1,0:T(8,128)(2,1)S(1)}, bf16[8,512,128]{2,1,0:T(8,128)(2,1)S(1)}, u32[]{:S(2)}, u32[]{:S(2)}) collective-permute-start(bf16[8,512,128]{2,1,0:T(8,128)(2,1)S(1)} %all_to_all.39.rows_ref), channel_id=1, source_target_pairs={{0,1},{1,0},{2,3},{3,2},{4,5},{5,4},{6,7},{7,6},{8,9},{9,8},{10,11... | collective-permute-start | bytes 3145736 | tf_op jit(solution)/shard_map/ppermute | solution.py:386
  115.1 2.2 %copy-start = (bf16[1,256,2048]{2,1,0:T(8,128)(2,1)S(1)}, bf16[1,256,2048]{2,1,0:T(8,128)(2,1)}, u32[]{:S(2)}) copy-start(bf16[1,256,2048]{2,1,0:T(8,128)(2,1)} %param.39) | copy-start | bytes 3145732
  119.8 4.6 %collective-permute-start.3 = (bf16[8,512,128]{2,1,0:T(8,128)(2,1)S(1)}, bf16[8,512,128]{2,1,0:T(8,128)(2,1)S(1)}, u32[]{:S(2)}, u32[]{:S(2)}) collective-permute-start(bf16[8,512,128]{2,1,0:T(8,128)(2,1)S(1)} %get-tuple-element.51), channel_id=1, source_target_pairs={{0,1},{1,0},{2,3},{3,2},{4,5},{5,4},{6,7},{7,6},{8,9},{9,8},{10,11... | collective-permute-start | bytes 3145736 | tf_op jit(solution)/shard_map/ppermute | solution.py:386

commit v4 on v3

--- a/solution.py
+++ b/solution.py
@@ -277,103 +277,54 @@
         )
     stream = (total + product).astype(jnp.bfloat16)
     stream_ref[...] = stream
-    slot = iota((out_ref.shape[0], length), 0).astype(jnp.float32)
+    blocks, places, cores, half, _ = out_ref.shape
+    slot = iota((blocks * cores * half, length), 0).astype(jnp.float32)
     chosen = (row_ref[8:9, :] == slot) | (row_ref[9:10, :] == slot)
-    out_ref[...] = jnp.dot(
+    picked = jnp.dot(
         jnp.where(chosen, 1.0, 0.0).astype(jnp.bfloat16), stream, preferred_element_type=jnp.float32
-    ).astype(jnp.bfloat16)
-
-
-def half_products(rows_ref, gain_ref, gate_ref, up_ref, core, at, scaled):
-    places = rows_ref.shape[0]
-    squares = jnp.zeros((at.size, 128), jnp.float32)
+    )
+    picked = picked.reshape(blocks, cores, half, width).astype(jnp.bfloat16)
     for y in range(places):
-        part = rows_ref[y, at, :].astype(jnp.float32)
+        out_ref[:, y] = picked
+
+
+def expert_kernel(
+    rows_ref, gain_ref, gate_own, gate_other, up_own, up_other, down_own, down_other, out_ref, scaled
+):
+    blocks, features, half, lanes = rows_ref.shape
+    count = blocks * half
+    squares = jnp.zeros((count, lanes), jnp.float32)
+    for k in range(features):
+        part = rows_ref[:, k].astype(jnp.float32).reshape(count, lanes)
         squares = squares + part * part
-        scaled[:, y * 128 : (y + 1) * 128] = (part * gain_ref[y, pl.ds(core, 1), :]).astype(
-            jnp.bfloat16
-        )
+        at = slice(k * lanes, (k + 1) * lanes)
+        scaled[:, at] = (part * gain_ref[:, at]).astype(jnp.bfloat16)
+    scale = lax.rsqrt(jnp.sum(squares, axis=1, keepdims=True) / D + stream_eps)
     whole = scaled[...]
-    gate = jnp.dot(whole, gate_ref[...], preferred_element_type=jnp.float32)
-    upward = jnp.dot(whole, up_ref[...], preferred_element_type=jnp.float32)
-    return jnp.sum(squares, axis=1, keepdims=True), gate, upward
-
-
-def pick_half(core, weight_ref, half):
-    for y in range(half.shape[0] // 128):
-        half[y * 128 : (y + 1) * 128, :] = weight_ref[y, core]
-
-
-def first_half_kernel(
-    chunk, place_ref, rows_ref, gain_ref, gate_ref, up_ref, squares_ref, gate_out, up_out, scaled, gate_half, up_half
-):
-    core = place_ref[2]
-    pick_half(core, gate_ref, gate_half)
-    pick_half(core, up_ref, up_half)
-
-    def step(i, carry):
-        at = pl.ds(pl.multiple_of(i * chunk, chunk), chunk)
-        squares, gate, upward = half_products(
-            rows_ref, gain_ref, gate_half, up_half, core, at, scaled
-        )
-        squares_ref[at, :] = jnp.broadcast_to(squares, (chunk, 128))
-        gate_out[at, :] = gate
-        up_out[at, :] = upward
-        return carry
-
-    lax.fori_loop(0, rows_ref.shape[1] // chunk, step, 0)
-
-
-def second_half_kernel(
-    chunk, place_ref, rows_ref, gain_ref, gate_ref, up_ref, down_ref, squares_ref, gate_in, up_in,
-    hidden_ref, out_ref, scaled, gate_half, up_half, down_half,
-):
-    other = 1 - place_ref[2]
-    pick_half(other, gate_ref, gate_half)
-    pick_half(other, up_ref, up_half)
-    for y in range(rows_ref.shape[0]):
-        at = pl.ds(pl.multiple_of((2 * y + other) * 128, 128), 128)
-        down_half[:, y * 128 : (y + 1) * 128] = down_ref[:, at]
-
-    def step(i, carry):
-        at = pl.ds(pl.multiple_of(i * chunk, chunk), chunk)
-        squares, gate, upward = half_products(
-            rows_ref, gain_ref, gate_half, up_half, other, at, scaled
-        )
-        squares = squares + squares_ref[at, 0:1]
-        scale = lax.rsqrt(squares / D + stream_eps)
-        gate = (gate + gate_in[at, :]) * scale
-        upward = (upward + up_in[at, :]) * scale
-        hidden = (jax.nn.silu(gate) * upward).astype(jnp.bfloat16)
-        hidden_ref[at, :] = hidden
-        part = jnp.dot(hidden, down_half[...], preferred_element_type=jnp.float32)
-        for y in range(rows_ref.shape[0]):
-            out_ref[y, at, :] = part[:, y * 128 : (y + 1) * 128].astype(jnp.bfloat16)
-        return carry
-
-    lax.fori_loop(0, rows_ref.shape[1] // chunk, step, 0)
-
-
-def own_half_kernel(chunk, place_ref, hidden_ref, down_ref, out_ref, down_half):
-    core = place_ref[2]
-    for y in range(out_ref.shape[0]):
-        at = pl.ds(pl.multiple_of((2 * y + core) * 128, 128), 128)
-        down_half[:, y * 128 : (y + 1) * 128] = down_ref[:, at]
-
-    def step(i, carry):
-        at = pl.ds(pl.multiple_of(i * chunk, chunk), chunk)
-        part = jnp.dot(hidden_ref[at, :], down_half[...], preferred_element_type=jnp.float32)
-        for y in range(out_ref.shape[0]):
-            out_ref[y, at, :] = part[:, y * 128 : (y + 1) * 128].astype(jnp.bfloat16)
-        return carry
-
-    lax.fori_loop(0, hidden_ref.shape[0] // chunk, step, 0)
+    hidden = []
+    for gate_ref, up_ref in ((gate_own, up_own), (gate_other, up_other)):
+        gate = jnp.dot(whole, gate_ref[...], preferred_element_type=jnp.float32) * scale
+        upward = jnp.dot(whole, up_ref[...], preferred_element_type=jnp.float32) * scale
+        hidden.append((jax.nn.silu(gate) * upward).astype(jnp.bfloat16))
+    step = 2 * lanes
+    for j in range(features // 2):
+        at = slice(j * step, (j + 1) * step)
+        part = jnp.dot(hidden[0], down_own[:, at], preferred_element_type=jnp.float32)
+        part = part + jnp.dot(hidden[1], down_other[:, at], preferred_element_type=jnp.float32)
+        for n in range(2):
+            tile = part[:, n * lanes : (n + 1) * lanes].reshape(blocks, half, lanes)
+            out_ref[:, 2 * j + n] = tile.astype(jnp.bfloat16)
 
 
 def final_kernel(returned_ref, stream_ref, col_ref, out_ref):
-    length = stream_ref.shape[0]
-    slot = iota((length, returned_ref.shape[0]), 1).astype(jnp.float32)
-    returned = returned_ref[...]
+    length, width = stream_ref.shape
+    blocks, places, cores, half, _ = returned_ref.shape
+    slots = blocks * cores * half
+    slot = iota((length, slots), 1).astype(jnp.float32)
+    answer = returned_ref[:, 0].astype(jnp.float32)
+    for y in range(1, places):
+        answer = answer + returned_ref[:, y].astype(jnp.float32)
+    returned = answer.reshape(slots, width).astype(jnp.bfloat16)
     total = stream_ref[...].astype(jnp.float32)
     for k in range(2):
         chosen = jnp.where(col_ref[:, 8 + k : 9 + k] == slot, 1.0, 0.0).astype(jnp.bfloat16)
@@ -384,12 +335,6 @@
 
 def swapped(value):
     return lax.ppermute(value, "c", [(0, 1), (1, 0)])
-
-
-def to_all(shard, axis):
-    peers = lax.axis_size(axis)
-    copies = jnp.broadcast_to(shard[None], (peers, *shard.shape))
-    return lax.all_to_all(copies, axis, 0, 0, tiled=True)
 
 
 def body(
@@ -464,6 +409,15 @@
         ],
         hbm=9,
     )
+    rows, gate_own, up_own, down_own = lax.optimization_barrier(
+        (
+            rows,
+            specialist_gating_weights[0],
+            specialist_raising_weights[0],
+            specialist_lowering_weights[0],
+        )
+    )
+    gate_other, up_other, down_other = swapped(gate_own), swapped(up_own), swapped(down_own)
     message, x_conv, b_conv, c_conv = call(
         conv_kernel,
         "conv",
@@ -495,64 +449,33 @@
     gathered = lax.all_gather(
         lax.all_to_all(copies, "y", 0, 0, tiled=True), "c", axis=1, tiled=True
     )
+    half = capacity // 2
+    spread = (blocks, peers_y, 2, half, width)
+    everyone = (*SP, *TP)
     stream, outgoing = call(
         stream_kernel,
         "stream",
-        [((length, width), bf16), ((slots, width), bf16)],
+        [((length, width), bf16), (spread, bf16)],
         (gathered, final_projection_weights, skip_stream_entering, rows),
     )
     arrived = lax.all_to_all(
-        outgoing.reshape(blocks, capacity, width), SP, 0, 0, tiled=True
-    ).reshape(slots, width)
-    own = to_all(arrived, "y")
-    theirs = swapped(own)
-    chunk = 256
-    wide = (peers_y, 2, 128)
-    gain = specialist_rescale_factor.reshape(wide)
-    weight_gate = specialist_gating_weights.reshape(*wide, -1)
-    weight_up = specialist_raising_weights.reshape(*wide, -1)
-    weight_down = specialist_lowering_weights[0]
-    units = weight_down.shape[0]
-    half = pltpu.VMEM((D // 2, units), bf16)
-    down_half = pltpu.VMEM((units, D // 2), bf16)
-    scaled = pltpu.VMEM((chunk, D // 2), bf16)
-    squares, gate, upward = call(
-        functools.partial(first_half_kernel, chunk),
-        "first_half",
-        [((slots, 128), f32), ((slots, units), f32), ((slots, units), f32)],
-        (place, own, gain, weight_gate, weight_up),
-        flops=4 * slots * units * D // 2,
-        scratch=[scaled, half, half],
-        smem=1,
-        room=16,
-    )
-    hidden, sent = call(
-        functools.partial(second_half_kernel, chunk),
-        "second_half",
-        [((slots, units), bf16), ((peers_y, slots, width), bf16)],
-        (place, theirs, gain, weight_gate, weight_up, weight_down, squares, gate, upward),
-        flops=6 * slots * units * D // 2,
-        scratch=[scaled, half, half, down_half],
-        smem=1,
-        room=20,
-    )
-    partner = swapped(sent)
-    (kept,) = call(
-        functools.partial(own_half_kernel, chunk),
-        "own_half",
-        [((peers_y, slots, width), bf16)],
-        (place, hidden, weight_down),
-        flops=2 * slots * units * D // 2,
-        scratch=[down_half],
-        smem=1,
-        room=12,
-    )
-    pair = (kept.astype(f32) + partner.astype(f32)).astype(bf16)
-    whole = lax.all_to_all(pair, "y", 0, 0, tiled=True)
-    answer = jnp.sum(whole.astype(f32), axis=0).astype(bf16)
+        outgoing.reshape(-1, half, width), everyone, 0, 0, tiled=True
+    ).reshape(blocks, 2 * peers_y, half, width)
+    (partial_out,) = call(
+        expert_kernel,
+        "expert",
+        [(arrived.shape, bf16)],
+        (
+            arrived, specialist_rescale_factor[None], gate_own, gate_other, up_own, up_other,
+            down_own, down_other,
+        ),
+        flops=6 * slots * gate_own.shape[1] * D,
+        scratch=[pltpu.VMEM((slots // 2, D), bf16)],
+        room=24,
+    )
     returned = lax.all_to_all(
-        answer.reshape(blocks, capacity, width), SP, 0, 0, tiled=True
-    ).reshape(slots, width)
+        partial_out.reshape(-1, half, width), everyone, 0, 0, tiled=True
+    ).reshape(spread)
     (out,) = call(final_kernel, "final", [((length, width), bf16)], (returned, stream, cols))
     return out
 

time: 170 us -> 165 us (0.971)
  blocking collectives: 143 us -> 79.2 us
  waiting for transfers between devices: 1.61 us -> 29.9 us
  starting transfers between devices: 12.1 us -> 34.8 us
  local copies, waits for them, and re-layouts: 0.17 us -> 9.48 us
  Pallas kernels: 12.7 us -> 10.1 us
    all_to_all x5 -> x1, blocking collectives: 106 us -> 42.5 us  [body(): lax.all_to_all(partial_out.reshape(-1, half, width), everyone, 0, 0, tile...]
    all_to_all x0 -> x2, waiting for transfers between devices: none -> 29.4 us  [the longest x1 19.6 us: body(): lax.all_to_all(outgoing.reshape(-1, half, width), everyone, 0, 0, tiled=T...]
    all_to_all x0 -> x2, starting transfers between devices: none -> 19.6 us  [the longest x1 10.8 us: body(): got = lax.all_to_all(onward, 'z', 0, 0, tiled=True)]
    unnamed x16 -> x30, local copies, waits for them, and re-layouts: 0.04 us -> 9.48 us
    ppermute x2 -> x3, starting transfers between devices: 7.51 us -> 10.7 us  [swapped(): return lax.ppermute(value, 'c', [(0, 1), (1, 0)])]
    pallas_call x10 -> x8, Pallas kernels: 12.7 us -> 10.1 us  [call(): pl.pallas_call(kernel, out_shape=shapes, in_specs=[SMEM] * smem + [HBM] *...]
  transfers between devices with their start and end apart: 4 -> 7, of which waited for: 2 -> 3; matrix products, arithmetic and copies ran while one was open for 0% -> 0% of each run, Pallas kernels for 3% -> 1%
where the time goes in v4:
time: 165 us; the launch traced here: 164 us
  blocking collectives  79.2 us (48%)
  starting transfers between devices  34.8 us (21%)
  waiting for transfers between devices  29.9 us (18%)
  Pallas kernels  10.1 us (6%)
  local copies, waits for them, and re-layouts  9.48 us (6%)
    all_to_all x1, blocking collectives, body(): lax.all_to_all(partial_out.reshape(-1, half, width), everyone, 0, 0, tile...  42.5 us
    all_to_all x1, waiting for transfers between devices, body(): lax.all_to_all(outgoing.reshape(-1, half, width), everyone, 0, 0, tiled=T...  19.6 us
    all_to_all x1, blocking collectives, body(): lax.all_to_all(copies, 'y', 0, 0, tiled=True)  16.1 us
    all_to_all x1, blocking collectives, body(): seen = lax.all_to_all(message, 'x', 0, 0, tiled=True)  12.7 us
    all_to_all x1, starting transfers between devices, body(): got = lax.all_to_all(onward, 'z', 0, 0, tiled=True)  10.8 us
    ppermute x3, starting transfers between devices, swapped(): return lax.ppermute(value, 'c', [(0, 1), (1, 0)])  10.7 us
    pallas_call x8, Pallas kernels, call(): pl.pallas_call(kernel, out_shape=shapes, in_specs=[SMEM] * smem + [HBM] *...  10.1 us
    all_to_all x1, waiting for transfers between devices, body(): got = lax.all_to_all(onward, 'z', 0, 0, tiled=True)  9.79 us
  transfers between devices with their start and end apart: 7, of which 3 were waited for; matrix products, arithmetic and copies ran while one was open for 0% of the time, Pallas kernels for 1%

profile of v4, /device:TPU:1, one launch (start us, length us, event | category | flops | bytes accessed | tf_op | source)
XLA Modules:
  0.0 163.8 jit_solution(14747671377097050079)
XLA Ops:
  0.0 0.1 pad_add_fusion.place_ref
  0.1 1.4 rim.1
  1.5 3.9 %collective-permute-start = (f32[2,384]{1,0:T(2,128)S(1)}, f32[2,384]{1,0:T(2,128)S(1)}, u32[]{:S(2)}, u32[]{:S(2)}) collective-permute-start(f32[2,384]{1,0:T(2,128)S(1)} %get-tuple-element.31), channel_id=1, source_target_pairs={{0,16},{16,0},{32,48},{48,32},{64,80},{80,64},{96,112},{112,96},{1... | collective-permute-start | bytes 9224 | tf_op jit(solution)/shard_map/ppermute | solution.py:383
  5.4 0.7 collective-permute-start.1
  6.1 1.6 table.1
  7.6 0.0 collective-permute-done.even_ref
  7.6 0.0 collective-permute-done.1.odd_ref
  7.7 1.1 conv.1
  8.8 12.7 %all_to_all.25.seen_ref = bf16[4,272,128]{2,1,0:T(8,128)(2,1)S(1)} all-to-all(bf16[4,272,128]{2,1,0:T(8,128)(2,1)S(1)} %get-tuple-element.37), channel_id=1, replica_groups=mesh['z'=8,'x'=4,'y'=8,'c'=2] {'x'}, dimensions={0} | all-to-all | bytes 557056 | tf_op jit(solution)/shard_map/all_to_all | solution.py:430
  21.5 1.4 row.1
  22.8 0.0 copy-start.11
  22.8 10.8 %all-to-all-start.1 = ((bf16[8,144,128]{2,1,0:T(8,128)(2,1)}), bf16[8,144,128]{2,1,0:T(8,128)(2,1)S(1)}, u32[]{:S(2)}, u32[]{:S(2)}) async-start(bf16[8,144,128]{2,1,0:T(8,128)(2,1)} %get-tuple-element.38), calls=%async_computation.1 | async-start | bytes 589824 | tf_op jit(solution)/shard_map/all_to_all | solution.py:438
  33.6 9.8 %all-to-all-done.1.got_ref = bf16[8,144,128]{2,1,0:T(8,128)(2,1)S(1)} async-done(((bf16[8,144,128]{2,1,0:T(8,128)(2,1)}), bf16[8,144,128]{2,1,0:T(8,128)(2,1)S(1)}, u32[]{:S(2)}, u32[]{:S(2)}) %all-to-all-start.1) | async-done | bytes 294944 | tf_op jit(solution)/shard_map/all_to_all | solution.py:438
  43.4 0.0 copy-start.14
  43.4 0.0 copy-done.11
  43.4 0.7 copy-done.14
  44.1 1.4 mixed.1
  45.5 0.0 copy-start.10
  45.5 16.1 %all_to_all.26 = bf16[8,128,128]{2,1,0:T(8,128)(2,1)S(1)} all-to-all(bf16[8,128,128]{2,1,0:T(8,128)(2,1)S(1)} %mixed.1), channel_id=1, replica_groups=mesh['z'=8,'x'=4,'y'=8,'c'=2] {'y'}, dimensions={0} | all-to-all | bytes 524288 | tf_op jit(solution)/shard_map/all_to_all | solution.py:450
  61.6 0.0 copy-start.12
  61.6 7.9 %all_gather.3.mixed_ref = bf16[8,256,128]{2,1,0:T(8,128)(2,1)S(1)} all-gather(bf16[8,128,128]{2,1,0:T(8,128)(2,1)S(1)} %all_to_all.26), channel_id=1, replica_groups=mesh['z'=8,'x'=4,'y'=8,'c'=2] {'c'}, dimensions={1}, use_global_device_ids=true | all-gather | bytes 786432 | tf_op jit(solution)/shard_map/all_gather | solution.py:449
  69.5 0.0 copy-done.10
  69.5 0.0 copy-done.12
  69.5 0.5 stream.1
  70.0 0.0 copy-start.9
  70.0 1.0 copy-done.9
  71.0 8.7 %all-to-all-start.3 = ((bf16[512,8,128]{2,1,0:T(8,128)(2,1)}), bf16[512,8,128]{2,1,0:T(8,128)(2,1)S(1)}, u32[]{:S(2)}, u32[]{:S(2)}) async-start(bf16[512,8,128]{2,1,0:T(8,128)(2,1)} %bitcast.25), calls=%async_computation.3 | async-start | bytes 2097152 | tf_op jit(solution)/shard_map/all_to_all | solution.py:461
  79.8 0.0 copy-done
  79.8 6.3 %collective-permute-start.2 = (bf16[2048,256]{1,0:T(8,128)(2,1)S(1)}, bf16[2048,256]{1,0:T(8,128)(2,1)S(1)}, u32[]{:S(2)}, u32[]{:S(2)}) collective-permute-start(bf16[2048,256]{1,0:T(8,128)(2,1)S(1)} %bitcast.19), channel_id=1, source_target_pairs={{0,1},{1,0},{2,3},{3,2},{4,5},{5,4},{6,7},{7,6},{8,9},{9,8},{10,11... | collective-permute-start | bytes 3145736 | tf_op jit(solution)/shard_map/ppermute | solution.py:337
  86.1 0.0 copy-done.1
  86.1 1.9 %collective-permute-start.3 = (bf16[2048,256]{1,0:T(8,128)(2,1)S(1)}, bf16[2048,256]{1,0:T(8,128)(2,1)S(1)}, u32[]{:S(2)}, u32[]{:S(2)}) collective-permute-start(bf16[2048,256]{1,0:T(8,128)(2,1)S(1)} %bitcast.21), channel_id=1, source_target_pairs={{0,1},{1,0},{2,3},{3,2},{4,5},{5,4},{6,7},{7,6},{8,9},{9,8},{10,11... | collective-permute-start | bytes 3145736 | tf_op jit(solution)/shard_map/ppermute | solution.py:337
  88.1 2.4 %collective-permute-start.4 = (bf16[256,2048]{1,0:T(8,128)(2,1)}, bf16[256,2048]{1,0:T(8,128)(2,1)S(1)}, u32[]{:S(2)}, u32[]{:S(2)}) collective-permute-start(bf16[256,2048]{1,0:T(8,128)(2,1)} %bitcast.23), channel_id=1, source_target_pairs={{0,1},{1,0},{2,3},{3,2},{4,5},{5,4},{6,7},{7,6},{8,9},{9,8},{10,11... | collective-permute-start | bytes 3145736 | tf_op jit(solution)/shard_map/ppermute | solution.py:337
  90.5 0.0 collective-permute-done.2.gate_other
  90.5 0.0 copy-start.3
  90.5 0.9 copy-done.3
  91.5 0.0 collective-permute-done.3.up_other
  91.5 1.0 copy-done.5
  92.4 0.5 collective-permute-done.4.down_other
  93.0 1.0 copy-done.7
  93.9 19.6 %all-to-all-done.3 = bf16[512,8,128]{2,1,0:T(8,128)(2,1)S(1)} async-done(((bf16[512,8,128]{2,1,0:T(8,128)(2,1)}), bf16[512,8,128]{2,1,0:T(8,128)(2,1)S(1)}, u32[]{:S(2)}, u32[]{:S(2)}) %all-to-all-start.3) | async-done | bytes 1048608 | tf_op jit(solution)/shard_map/all_to_all | solution.py:461
  113.5 0.0 copy-done.13
  113.5 1.2 copy-done.2
  114.8 1.2 copy-done.4
  116.0 1.2 copy-done.6
  117.2 1.2 copy-done.8
  118.4 1.9 %expert.1 = bf16[32,16,8,128]{3,2,1,0:T(8,128)(2,1)S(1)} custom-call(bf16[32,16,8,128]{3,2,1,0:T(8,128)(2,1)S(1)} %bitcast.16, f32[1,2048]{1,0:T(1,128)S(1)} %bitcast.26, bf16[2048,256]{1,0:T(8,128)(2,1)S(1)} %bitcast.20, bf16[2048,256]{1,0:T(8,128)(2,1)S(1)} %copy-done.4, bf16[2048,256]{1,0:T(8,128)(2,1)S(1)} %bitcast.22, bf16[2048,256]{1,0:T(8,128)(2,1)S(1)} %copy-done.6, ...), custom_call_target="tpu_custom_call" | custom-call | flops 1610612736 | bytes 8396800 | tf_op jit(solution)/shard_map/expert/pallas_call | solution.py:36
  120.3 42.5 %all_to_all.27 = bf16[512,8,128]{2,1,0:T(8,128)(2,1)S(1)} all-to-all(bf16[512,8,128]{2,1,0:T(8,128)(2,1)S(1)} %bitcast.17), channel_id=1, replica_groups=mesh['z'=8,'x'=4,'y'=8,'c'=2] {'z','x','y','c'}, dimensions={0} | all-to-all | bytes 2097152 | tf_op jit(solution)/shard_map/all_to_all | solution.py:476
  162.9 1.0 final.1
  (9 shorter events, 0.0 us)
Async XLA Ops:
  1.5 6.2 %collective-permute-start = (f32[2,384]{1,0:T(2,128)S(1)}, f32[2,384]{1,0:T(2,128)S(1)}, u32[]{:S(2)}, u32[]{:S(2)}) collective-permute-start(f32[2,384]{1,0:T(2,128)S(1)} %get-tuple-element.31), channel_id=1, source_target_pairs={{0,16},{16,0},{32,48},{48,32},{64,80},{80,64},{96,112},{112,96},{1... | collective-permute-start | bytes 9224 | tf_op jit(solution)/shard_map/ppermute | solution.py:383
  5.4 2.3 %collective-permute-start.1 = (f32[2,384]{1,0:T(2,128)S(1)}, f32[2,384]{1,0:T(2,128)S(1)}, u32[]{:S(2)}, u32[]{:S(2)}) collective-permute-start(f32[2,384]{1,0:T(2,128)S(1)} %get-tuple-element.32), channel_id=1, source_target_pairs={{16,32},{32,16},{48,64},{64,48},{80,96},{96,80},{112,128},{128,112... | collective-permute-start | bytes 9224 | tf_op jit(solution)/shard_map/ppermute | solution.py:384
  22.8 20.6 %copy-start.11 = (bf16[128,128]{1,0:T(8,128)(2,1)S(1)}, bf16[128,128]{1,0:T(8,128)(2,1)}, u32[]{:S(2)}) copy-start(bf16[128,128]{1,0:T(8,128)(2,1)} %valve_ref.1) | copy-start | bytes 98308
  22.8 20.6 %all-to-all-start.1 = ((bf16[8,144,128]{2,1,0:T(8,128)(2,1)}), bf16[8,144,128]{2,1,0:T(8,128)(2,1)S(1)}, u32[]{:S(2)}, u32[]{:S(2)}) async-start(bf16[8,144,128]{2,1,0:T(8,128)(2,1)} %get-tuple-element.38), calls=%async_computation.1 | async-start | bytes 589824 | tf_op jit(solution)/shard_map/all_to_all | solution.py:438
  43.4 0.7 copy-start.14
  45.5 24.0 %copy-start.10 = (bf16[2048,128]{1,0:T(8,128)(2,1)S(1)}, bf16[2048,128]{1,0:T(8,128)(2,1)}, u32[]{:S(2)}) copy-start(bf16[2048,128]{1,0:T(8,128)(2,1)} %weight_ref.1) | copy-start | bytes 1572868
  61.6 7.9 %copy-start.12 = (bf16[128,128]{1,0:T(8,128)(2,1)S(1)}, bf16[128,128]{1,0:T(8,128)(2,1)}, u32[]{:S(2)}) copy-start(bf16[128,128]{1,0:T(8,128)(2,1)} %skip_ref.1) | copy-start | bytes 98308
  69.5 44.0 %copy-start.13 = (f32[2048]{0:T(1024)S(1)}, f32[2048]{0:T(1024)}, u32[]{:S(2)}) copy-start(f32[2048]{0:T(1024)} %param.33) | copy-start | bytes 24580
  70.0 1.0 copy-start.9
  71.0 8.8 %copy-start = (bf16[1,2048,256]{2,1,0:T(8,128)(2,1)S(1)}, bf16[1,2048,256]{2,1,0:T(8,128)(2,1)}, u32[]{:S(2)}) copy-start(bf16[1,2048,256]{2,1,0:T(8,128)(2,1)} %param.37) | copy-start | bytes 3145732
  71.0 15.1 %copy-start.1 = (bf16[1,2048,256]{2,1,0:T(8,128)(2,1)S(1)}, bf16[1,2048,256]{2,1,0:T(8,128)(2,1)}, u32[]{:S(2)}) copy-start(bf16[1,2048,256]{2,1,0:T(8,128)(2,1)} %param.38) | copy-start | bytes 3145732
  71.0 42.5 %all-to-all-start.3 = ((bf16[512,8,128]{2,1,0:T(8,128)(2,1)}), bf16[512,8,128]{2,1,0:T(8,128)(2,1)S(1)}, u32[]{:S(2)}, u32[]{:S(2)}) async-start(bf16[512,8,128]{2,1,0:T(8,128)(2,1)} %bitcast.25), calls=%async_computation.3 | async-start | bytes 2097152 | tf_op jit(solution)/shard_map/all_to_all | solution.py:461
  79.8 10.7 %collective-permute-start.2 = (bf16[2048,256]{1,0:T(8,128)(2,1)S(1)}, bf16[2048,256]{1,0:T(8,128)(2,1)S(1)}, u32[]{:S(2)}, u32[]{:S(2)}) collective-permute-start(bf16[2048,256]{1,0:T(8,128)(2,1)S(1)} %bitcast.19), channel_id=1, source_target_pairs={{0,1},{1,0},{2,3},{3,2},{4,5},{5,4},{6,7},{7,6},{8,9},{9,8},{10,11... | collective-permute-start | bytes 3145736 | tf_op jit(solution)/shard_map/ppermute | solution.py:337
  86.1 5.3 %collective-permute-start.3 = (bf16[2048,256]{1,0:T(8,128)(2,1)S(1)}, bf16[2048,256]{1,0:T(8,128)(2,1)S(1)}, u32[]{:S(2)}, u32[]{:S(2)}) collective-permute-start(bf16[2048,256]{1,0:T(8,128)(2,1)S(1)} %bitcast.21), channel_id=1, source_target_pairs={{0,1},{1,0},{2,3},{3,2},{4,5},{5,4},{6,7},{7,6},{8,9},{9,8},{10,11... | collective-permute-start | bytes 3145736 | tf_op jit(solution)/shard_map/ppermute | solution.py:337
  88.1 4.9 %collective-permute-start.4 = (bf16[256,2048]{1,0:T(8,128)(2,1)}, bf16[256,2048]{1,0:T(8,128)(2,1)S(1)}, u32[]{:S(2)}, u32[]{:S(2)}) collective-permute-start(bf16[256,2048]{1,0:T(8,128)(2,1)} %bitcast.23), channel_id=1, source_target_pairs={{0,1},{1,0},{2,3},{3,2},{4,5},{5,4},{6,7},{7,6},{8,9},{9,8},{10,11... | collective-permute-start | bytes 3145736 | tf_op jit(solution)/shard_map/ppermute | solution.py:337
  90.5 1.0 copy-start.3
  91.5 1.0 copy-start.5
  93.0 1.0 copy-start.7
  113.5 1.2 copy-start.2
  114.8 1.2 copy-start.4
  116.0 1.2 copy-start.6
  117.2 1.2 copy-start.8

commit v5 on v4

--- a/solution.py
+++ b/solution.py
@@ -8,6 +8,7 @@
 from jax.sharding import Mesh
 from jax.sharding import PartitionSpec as P
 
+
 D = 2048
 HD = 64
 NS = 128
@@ -25,7 +26,7 @@
 MIB = 1 << 20
 
 
-def call(kernel, name, outs, args, flops=1000, scratch=(), room=8, smem=0, hbm=0):
+def call(kernel, outs, args, flops=1000, scratch=(), room=8, smem=0, hbm=0):
     shapes = [jax.ShapeDtypeStruct(shape, dtype) for shape, dtype in outs]
     moved = sum(a.size * a.dtype.itemsize for a in args) + sum(
         o.size * o.dtype.itemsize for o in shapes
@@ -41,7 +42,6 @@
         scratch_shapes=list(scratch),
         compiler_params=pltpu.CompilerParams(vmem_limit_bytes=room * MIB),
         cost_estimate=pl.CostEstimate(flops=flops, bytes_accessed=moved, transcendentals=0),
-        name=name,
     )(*args)
 
 
@@ -371,7 +371,6 @@
     rim = CONV // 2
     even_rim, odd_rim, *feeds = call(
         rim_kernel,
-        "rim",
         [((rim, 3 * width), f32)] * 2 + [((length, width), bf16)] * 3,
         (place, unfiltered_channel_feed, unfiltered_state_entry, unfiltered_state_exit),
         flops=100_000,
@@ -386,7 +385,6 @@
     heads = increment_preactivation.shape[1]
     rows, cols, *filters = call(
         functools.partial(table_kernel, capacity),
-        "table",
         [((16, length), f32), ((length, length), f32)] + [((CONV, width), f32)] * 3,
         (
             increment_preactivation,
@@ -409,18 +407,8 @@
         ],
         hbm=9,
     )
-    rows, gate_own, up_own, down_own = lax.optimization_barrier(
-        (
-            rows,
-            specialist_gating_weights[0],
-            specialist_raising_weights[0],
-            specialist_lowering_weights[0],
-        )
-    )
-    gate_other, up_other, down_other = swapped(gate_own), swapped(up_own), swapped(down_own)
     message, x_conv, b_conv, c_conv = call(
         conv_kernel,
-        "conv",
         [((peers_x, 2 * width + 16, NS), bf16)] + [((length, width), bf16)] * 3,
         (place, *feeds, even_rim, odd_rim, *filters, cols),
         flops=4_000_000,
@@ -430,7 +418,6 @@
     seen = lax.all_to_all(message, "x", 0, 0, tiled=True)
     onward, near, ahead = call(
         row_kernel,
-        "row",
         [((peers_z, width + 16, NS), bf16), ((2, width, NS), f32), ((8, NS), f32)],
         (place, seen),
         smem=1,
@@ -438,7 +425,6 @@
     got = lax.all_to_all(onward, "z", 0, 0, tiled=True)
     (copies,) = call(
         mixed_kernel,
-        "mixed",
         [((peers_y, length, width), bf16)],
         (
             place, got, near, ahead, x_conv, b_conv, c_conv, rows, cols,
@@ -446,15 +432,28 @@
         ),
         smem=1,
     )
-    gathered = lax.all_gather(
-        lax.all_to_all(copies, "y", 0, 0, tiled=True), "c", axis=1, tiled=True
-    )
+    copies, gate_own, up_own, down_own = lax.optimization_barrier(
+        (
+            copies,
+            specialist_gating_weights[0],
+            specialist_raising_weights[0],
+            specialist_lowering_weights[0],
+        )
+    )
+    others = []
+    for weight in (gate_own, up_own, down_own):
+        others.append(swapped(weight))
+    gate_other, up_other, down_other = others
+    columns = lax.all_to_all(copies, "y", 0, 0, tiled=True)
+    columns, gate_other, up_other, down_other = lax.optimization_barrier(
+        (columns, gate_other, up_other, down_other)
+    )
+    gathered = lax.all_gather(columns, "c", axis=1, tiled=True)
     half = capacity // 2
     spread = (blocks, peers_y, 2, half, width)
     everyone = (*SP, *TP)
     stream, outgoing = call(
         stream_kernel,
-        "stream",
         [((length, width), bf16), (spread, bf16)],
         (gathered, final_projection_weights, skip_stream_entering, rows),
     )
@@ -463,7 +462,6 @@
     ).reshape(blocks, 2 * peers_y, half, width)
     (partial_out,) = call(
         expert_kernel,
-        "expert",
         [(arrived.shape, bf16)],
         (
             arrived, specialist_rescale_factor[None], gate_own, gate_other, up_own, up_other,
@@ -476,7 +474,7 @@
     returned = lax.all_to_all(
         partial_out.reshape(-1, half, width), everyone, 0, 0, tiled=True
     ).reshape(spread)
-    (out,) = call(final_kernel, "final", [((length, width), bf16)], (returned, stream, cols))
+    (out,) = call(final_kernel, [((length, width), bf16)], (returned, stream, cols))
     return out
 
 

time: 165 us -> 166 us (level)
  blocking collectives: 79.2 us -> 140 us
  waiting for transfers between devices: 29.9 us -> 0.01 us
  starting transfers between devices: 34.8 us -> 15.6 us
  local copies, waits for them, and re-layouts: 9.48 us -> 0.05 us
    all_to_all x1 -> x3, blocking collectives: 16.1 us -> 82 us  [the longest x1 42.8 us: body(): lax.all_to_all(outgoing.reshape(-1, half, width), everyone, 0, 0, tiled=T...]
    all_to_all x2 -> x0, waiting for transfers between devices: 29.4 us -> none  [the longest x1 19.6 us: body(): lax.all_to_all(outgoing.reshape(-1, half, width), everyone, 0, 0, tiled=T...]
    all_to_all x2 -> x0, starting transfers between devices: 19.6 us -> none  [the longest x1 10.8 us: body(): got = lax.all_to_all(onward, 'z', 0, 0, tiled=True)]
    unnamed x30 -> x16, local copies, waits for them, and re-layouts: 9.48 us -> 0.05 us
    all_gather x1, blocking collectives: 7.91 us -> 2.27 us  [body(): gathered = lax.all_gather(columns, 'c', axis=1, tiled=True)]
  transfers between devices with their start and end apart: 7 -> 5, of which waited for: 3 -> 0; matrix products, arithmetic and copies ran while one was open for 0% -> 0% of each run, Pallas kernels for 1% -> 1%
where the time goes in v5:
time: 166 us; the launch traced here: 165 us
  blocking collectives  140 us (84%)
  starting transfers between devices  15.6 us (9%)
  Pallas kernels  9.57 us (6%)
    all_to_all x1, blocking collectives, body(): lax.all_to_all(outgoing.reshape(-1, half, width), everyone, 0, 0, tiled=T...  42.8 us
    all_to_all x1, blocking collectives, body(): lax.all_to_all(partial_out.reshape(-1, half, width), everyone, 0, 0, tile...  42.5 us
    all_to_all x1, blocking collectives, body(): got = lax.all_to_all(onward, 'z', 0, 0, tiled=True)  20.2 us
    all_to_all x1, blocking collectives, body(): columns = lax.all_to_all(copies, 'y', 0, 0, tiled=True)  19 us
    all_to_all x1, blocking collectives, body(): seen = lax.all_to_all(message, 'x', 0, 0, tiled=True)  12.8 us
    ppermute x3, starting transfers between devices, swapped(): return lax.ppermute(value, 'c', [(0, 1), (1, 0)])  11 us
    pallas_call x8, Pallas kernels, call(): pl.pallas_call(kernel, out_shape=shapes, in_specs=[SMEM] * smem + [HBM] *...  9.57 us
    ppermute x1, starting transfers between devices, body(): lax.ppermute(even_rim, SP, [p for a, b in pairs[0::2] for p in ((a, b), (...  3.94 us
  transfers between devices with their start and end apart: 5, of which 0 were waited for; matrix products, arithmetic and copies ran while one was open for 0% of the time, Pallas kernels for 1%

profile of v5, /device:TPU:1, one launch (start us, length us, event | category | flops | bytes accessed | tf_op | source)
XLA Modules:
  0.0 165.1 jit_solution(8532693607891317434)
XLA Ops:
  0.0 0.1 pad_add_fusion.place_ref
  0.1 1.4 shard_map.190
  1.5 3.9 %collective-permute-start = (f32[2,384]{1,0:T(2,128)S(1)}, f32[2,384]{1,0:T(2,128)S(1)}, u32[]{:S(2)}, u32[]{:S(2)}) collective-permute-start(f32[2,384]{1,0:T(2,128)S(1)} %get-tuple-element.35), channel_id=1, source_target_pairs={{0,16},{16,0},{32,48},{48,32},{64,80},{80,64},{96,112},{112,96},{1... | collective-permute-start | bytes 9224 | tf_op jit(solution)/shard_map/ppermute | solution.py:382
  5.4 0.7 collective-permute-start.1
  6.1 1.6 shard_map.191
  7.6 0.0 collective-permute-done.even_ref
  7.6 0.0 collective-permute-done.1.odd_ref
  7.7 0.0 copy-start.4
  7.7 0.0 copy-start.7
  7.7 1.1 shard_map.192
  8.8 0.0 copy-start
  8.8 0.0 copy-start.1
  8.8 12.8 %all_to_all.25.seen_ref = bf16[4,272,128]{2,1,0:T(8,128)(2,1)S(1)} all-to-all(bf16[4,272,128]{2,1,0:T(8,128)(2,1)S(1)} %get-tuple-element.41), channel_id=1, replica_groups=mesh['z'=8,'x'=4,'y'=8,'c'=2] {'x'}, dimensions={0} | all-to-all | bytes 557056 | tf_op jit(solution)/shard_map/all_to_all | solution.py:418
  21.6 0.7 shard_map.193
  22.3 20.2 %all_to_all.26.got_ref = bf16[8,144,128]{2,1,0:T(8,128)(2,1)S(1)} all-to-all(bf16[8,144,128]{2,1,0:T(8,128)(2,1)S(1)} %get-tuple-element.42), channel_id=1, replica_groups=mesh['z'=8,'x'=4,'y'=8,'c'=2] {'z'}, dimensions={0} | all-to-all | bytes 589824 | tf_op jit(solution)/shard_map/all_to_all | solution.py:425
  42.5 0.0 copy-done.4
  42.5 0.0 copy-done.7
  42.5 1.4 shard_map.194
  43.8 0.0 copy-done
  43.8 0.0 copy-start.3
  43.8 6.7 %collective-permute-start.2 = (bf16[2048,256]{1,0:T(8,128)(2,1)S(1)}, bf16[2048,256]{1,0:T(8,128)(2,1)S(1)}, u32[]{:S(2)}, u32[]{:S(2)}) collective-permute-start(bf16[2048,256]{1,0:T(8,128)(2,1)S(1)} %bitcast.19), channel_id=1, source_target_pairs={{0,1},{1,0},{2,3},{3,2},{4,5},{5,4},{6,7},{7,6},{8,9},{9,8},{10,11... | collective-permute-start | bytes 3145736 | tf_op jit(solution)/shard_map/ppermute | solution.py:337
  50.6 0.0 copy-done.1
  50.6 1.9 %collective-permute-start.3 = (bf16[2048,256]{1,0:T(8,128)(2,1)S(1)}, bf16[2048,256]{1,0:T(8,128)(2,1)S(1)}, u32[]{:S(2)}, u32[]{:S(2)}) collective-permute-start(bf16[2048,256]{1,0:T(8,128)(2,1)S(1)} %bitcast.21), channel_id=1, source_target_pairs={{0,1},{1,0},{2,3},{3,2},{4,5},{5,4},{6,7},{7,6},{8,9},{9,8},{10,11... | collective-permute-start | bytes 3145736 | tf_op jit(solution)/shard_map/ppermute | solution.py:337
  52.5 2.4 %collective-permute-start.4 = (bf16[256,2048]{1,0:T(8,128)(2,1)}, bf16[256,2048]{1,0:T(8,128)(2,1)S(1)}, u32[]{:S(2)}, u32[]{:S(2)}) collective-permute-start(bf16[256,2048]{1,0:T(8,128)(2,1)} %bitcast.23), channel_id=1, source_target_pairs={{0,1},{1,0},{2,3},{3,2},{4,5},{5,4},{6,7},{7,6},{8,9},{9,8},{10,11... | collective-permute-start | bytes 3145736 | tf_op jit(solution)/shard_map/ppermute | solution.py:337
  54.9 19.0 %all_to_all.27 = bf16[8,128,128]{2,1,0:T(8,128)(2,1)S(1)} all-to-all(bf16[8,128,128]{2,1,0:T(8,128)(2,1)S(1)} %shard_map.194), channel_id=1, replica_groups=mesh['z'=8,'x'=4,'y'=8,'c'=2] {'y'}, dimensions={0} | all-to-all | bytes 524288 | tf_op jit(solution)/shard_map/all_to_all | solution.py:447
  73.9 0.0 copy-start.5
  73.9 0.0 collective-permute-done.2.gate_other
  73.9 0.0 collective-permute-done.3.up_other
  73.9 0.0 collective-permute-done.4.down_other
  73.9 2.3 %all_gather.3.mixed_ref = bf16[8,256,128]{2,1,0:T(8,128)(2,1)S(1)} all-gather(bf16[8,128,128]{2,1,0:T(8,128)(2,1)S(1)} %all_to_all.27), channel_id=1, replica_groups=mesh['z'=8,'x'=4,'y'=8,'c'=2] {'c'}, dimensions={1}, use_global_device_ids=true | all-gather | bytes 786432 | tf_op jit(solution)/shard_map/all_gather | solution.py:451
  76.2 0.0 copy-done.3
  76.2 0.0 copy-done.5
  76.2 0.5 shard_map.195
  76.7 0.0 copy-start.2
  76.7 0.0 copy-start.6
  76.8 42.8 %all_to_all.28 = bf16[512,8,128]{2,1,0:T(8,128)(2,1)S(1)} all-to-all(bf16[512,8,128]{2,1,0:T(8,128)(2,1)S(1)} %bitcast.25), channel_id=1, replica_groups=mesh['z'=8,'x'=4,'y'=8,'c'=2] {'z','x','y','c'}, dimensions={0} | all-to-all | bytes 2097152 | tf_op jit(solution)/shard_map/all_to_all | solution.py:460
  119.6 0.0 copy-done.2
  119.6 0.0 copy-done.6
  119.6 2.1 %shard_map.196 = bf16[32,16,8,128]{3,2,1,0:T(8,128)(2,1)S(1)} custom-call(bf16[32,16,8,128]{3,2,1,0:T(8,128)(2,1)S(1)} %bitcast.16, f32[1,2048]{1,0:T(1,128)S(1)} %bitcast.26, bf16[2048,256]{1,0:T(8,128)(2,1)S(1)} %bitcast.20, bf16[2048,256]{1,0:T(8,128)(2,1)S(1)} %collective-permute-done.2.gate_other, bf16[2048,256]{1,0:T(8,128)(2,1)S(1)} %bitcast.22, ...), custom_call_target="tpu_custom_call" | custom-call | flops 1610612736 | bytes 8396800 | tf_op jit(solution)/shard_map/pallas_call | solution.py:37
  121.6 42.5 %all_to_all.29 = bf16[512,8,128]{2,1,0:T(8,128)(2,1)S(1)} all-to-all(bf16[512,8,128]{2,1,0:T(8,128)(2,1)S(1)} %bitcast.17), channel_id=1, replica_groups=mesh['z'=8,'x'=4,'y'=8,'c'=2] {'z','x','y','c'}, dimensions={0} | all-to-all | bytes 2097152 | tf_op jit(solution)/shard_map/all_to_all | solution.py:474
  164.2 1.0 shard_map.197
Async XLA Ops:
  1.5 6.2 %collective-permute-start = (f32[2,384]{1,0:T(2,128)S(1)}, f32[2,384]{1,0:T(2,128)S(1)}, u32[]{:S(2)}, u32[]{:S(2)}) collective-permute-start(f32[2,384]{1,0:T(2,128)S(1)} %get-tuple-element.35), channel_id=1, source_target_pairs={{0,16},{16,0},{32,48},{48,32},{64,80},{80,64},{96,112},{112,96},{1... | collective-permute-start | bytes 9224 | tf_op jit(solution)/shard_map/ppermute | solution.py:382
  5.4 2.3 %collective-permute-start.1 = (f32[2,384]{1,0:T(2,128)S(1)}, f32[2,384]{1,0:T(2,128)S(1)}, u32[]{:S(2)}, u32[]{:S(2)}) collective-permute-start(f32[2,384]{1,0:T(2,128)S(1)} %get-tuple-element.36), channel_id=1, source_target_pairs={{16,32},{32,16},{48,64},{64,48},{80,96},{96,80},{112,128},{128,112... | collective-permute-start | bytes 9224 | tf_op jit(solution)/shard_map/ppermute | solution.py:383
  7.7 34.8 %copy-start.4 = (bf16[128,128]{1,0:T(8,128)(2,1)S(1)}, bf16[128,128]{1,0:T(8,128)(2,1)}, u32[]{:S(2)}) copy-start(bf16[128,128]{1,0:T(8,128)(2,1)} %valve_ref.1) | copy-start | bytes 98308
  7.7 34.8 %copy-start.7 = (f32[128]{0:T(128)S(1)}, f32[128]{0:T(128)}, u32[]{:S(2)}) copy-start(f32[128]{0:T(128)} %param.31) | copy-start | bytes 1540
  8.8 35.0 %copy-start = (bf16[1,2048,256]{2,1,0:T(8,128)(2,1)S(1)}, bf16[1,2048,256]{2,1,0:T(8,128)(2,1)}, u32[]{:S(2)}) copy-start(bf16[1,2048,256]{2,1,0:T(8,128)(2,1)} %param.37) | copy-start | bytes 3145732
  8.8 41.8 %copy-start.1 = (bf16[1,2048,256]{2,1,0:T(8,128)(2,1)S(1)}, bf16[1,2048,256]{2,1,0:T(8,128)(2,1)}, u32[]{:S(2)}) copy-start(bf16[1,2048,256]{2,1,0:T(8,128)(2,1)} %param.38) | copy-start | bytes 3145732
  43.8 32.4 %copy-start.3 = (bf16[2048,128]{1,0:T(8,128)(2,1)S(1)}, bf16[2048,128]{1,0:T(8,128)(2,1)}, u32[]{:S(2)}) copy-start(bf16[2048,128]{1,0:T(8,128)(2,1)} %weight_ref.1) | copy-start | bytes 1572868
  43.8 30.1 %collective-permute-start.2 = (bf16[2048,256]{1,0:T(8,128)(2,1)S(1)}, bf16[2048,256]{1,0:T(8,128)(2,1)S(1)}, u32[]{:S(2)}, u32[]{:S(2)}) collective-permute-start(bf16[2048,256]{1,0:T(8,128)(2,1)S(1)} %bitcast.19), channel_id=1, source_target_pairs={{0,1},{1,0},{2,3},{3,2},{4,5},{5,4},{6,7},{7,6},{8,9},{9,8},{10,11... | collective-permute-start | bytes 3145736 | tf_op jit(solution)/shard_map/ppermute | solution.py:337
  50.6 23.3 %collective-permute-start.3 = (bf16[2048,256]{1,0:T(8,128)(2,1)S(1)}, bf16[2048,256]{1,0:T(8,128)(2,1)S(1)}, u32[]{:S(2)}, u32[]{:S(2)}) collective-permute-start(bf16[2048,256]{1,0:T(8,128)(2,1)S(1)} %bitcast.21), channel_id=1, source_target_pairs={{0,1},{1,0},{2,3},{3,2},{4,5},{5,4},{6,7},{7,6},{8,9},{9,8},{10,11... | collective-permute-start | bytes 3145736 | tf_op jit(solution)/shard_map/ppermute | solution.py:337
  52.5 21.4 %collective-permute-start.4 = (bf16[256,2048]{1,0:T(8,128)(2,1)}, bf16[256,2048]{1,0:T(8,128)(2,1)S(1)}, u32[]{:S(2)}, u32[]{:S(2)}) collective-permute-start(bf16[256,2048]{1,0:T(8,128)(2,1)} %bitcast.23), channel_id=1, source_target_pairs={{0,1},{1,0},{2,3},{3,2},{4,5},{5,4},{6,7},{7,6},{8,9},{9,8},{10,11... | collective-permute-start | bytes 3145736 | tf_op jit(solution)/shard_map/ppermute | solution.py:337
  73.9 2.3 %copy-start.5 = (bf16[128,128]{1,0:T(8,128)(2,1)S(1)}, bf16[128,128]{1,0:T(8,128)(2,1)}, u32[]{:S(2)}) copy-start(bf16[128,128]{1,0:T(8,128)(2,1)} %skip_ref.1) | copy-start | bytes 98308
  76.7 42.8 %copy-start.2 = (bf16[1,256,2048]{2,1,0:T(8,128)(2,1)S(1)}, bf16[1,256,2048]{2,1,0:T(8,128)(2,1)}, u32[]{:S(2)}) copy-start(bf16[1,256,2048]{2,1,0:T(8,128)(2,1)} %param.39) | copy-start | bytes 3145732
  76.7 42.8 %copy-start.6 = (f32[2048]{0:T(1024)S(1)}, f32[2048]{0:T(1024)}, u32[]{:S(2)}) copy-start(f32[2048]{0:T(1024)} %param.33) | copy-start | bytes 24580

commit v6 on v5

--- a/solution.py
+++ b/solution.py
@@ -14,7 +14,8 @@
 NS = 128
 CONV = 5
 SP = ("z", "x")
-TP = ("y", "c")
+ROW = ("yh", "p")
+TP = (*ROW, "c")
 
 HIGHEST = lax.Precision.HIGHEST
 group_eps = 1e-05
@@ -289,31 +290,69 @@
 
 
 def expert_kernel(
-    rows_ref, gain_ref, gate_own, gate_other, up_own, up_other, down_own, down_other, out_ref, scaled
+    place_ref, gate_in, up_in, down_in, own_ref, first_ref, second_ref, gain_ref, gate_own, up_own, down_own,
+    hidden_ref, first_out, second_out, scaled, gate_other, up_other, down_other, done,
 ):
-    blocks, features, half, lanes = rows_ref.shape
+    copies = [
+        pltpu.make_async_copy(a, b, done.at[n])
+        for n, (a, b) in enumerate(((gate_in, gate_other), (up_in, up_other), (down_in, down_other)))
+    ]
+    for copy in copies:
+        copy.start()
+    parity = place_ref[4]
+    blocks, features, half, lanes = own_ref.shape
     count = blocks * half
     squares = jnp.zeros((count, lanes), jnp.float32)
-    for k in range(features):
-        part = rows_ref[:, k].astype(jnp.float32).reshape(count, lanes)
-        squares = squares + part * part
-        at = slice(k * lanes, (k + 1) * lanes)
-        scaled[:, at] = (part * gain_ref[:, at]).astype(jnp.bfloat16)
+    for role, q in ((0, parity), (1, 1 - parity)):
+        for j in range(features):
+            if role == 0:
+                part = own_ref[:, j].astype(jnp.float32).reshape(count, lanes)
+            else:
+                part = jnp.concatenate([first_ref[:, j], second_ref[:, j]], axis=0)
+                part = part.astype(jnp.float32).reshape(count, lanes)
+            squares = squares + part * part
+            gain = gain_ref[j // 2, q][:, (j % 2) * lanes : (j % 2 + 1) * lanes]
+            scaled[role, :, j * lanes : (j + 1) * lanes] = (part * gain).astype(jnp.bfloat16)
     scale = lax.rsqrt(jnp.sum(squares, axis=1, keepdims=True) / D + stream_eps)
-    whole = scaled[...]
-    hidden = []
-    for gate_ref, up_ref in ((gate_own, up_own), (gate_other, up_other)):
-        gate = jnp.dot(whole, gate_ref[...], preferred_element_type=jnp.float32) * scale
-        upward = jnp.dot(whole, up_ref[...], preferred_element_type=jnp.float32) * scale
-        hidden.append((jax.nn.silu(gate) * upward).astype(jnp.bfloat16))
-    step = 2 * lanes
-    for j in range(features // 2):
-        at = slice(j * step, (j + 1) * step)
-        part = jnp.dot(hidden[0], down_own[:, at], preferred_element_type=jnp.float32)
-        part = part + jnp.dot(hidden[1], down_other[:, at], preferred_element_type=jnp.float32)
+
+    def product(weight_ref):
+        total = jnp.zeros((count, weight_ref.shape[-1]), jnp.float32)
+        for role, q in ((0, parity), (1, 1 - parity)):
+            for y in range(features // 2):
+                at = slice(2 * y * lanes, 2 * (y + 1) * lanes)
+                total = total + jnp.dot(
+                    scaled[role, :, at], weight_ref[y, q], preferred_element_type=jnp.float32
+                )
+        return total * scale
+
+    for n, (gate_ref, up_ref) in enumerate(((gate_own, up_own), (gate_other, up_other))):
+        if n == 1:
+            copies[0].wait()
+            copies[1].wait()
+        hidden_ref[n] = (jax.nn.silu(product(gate_ref)) * product(up_ref)).astype(jnp.bfloat16)
+    copies[2].wait()
+    for y in range(features // 2):
+        part = lowered(hidden_ref, down_own, down_other, y, 1 - parity).reshape(blocks, half, 2 * lanes)
         for n in range(2):
-            tile = part[:, n * lanes : (n + 1) * lanes].reshape(blocks, half, lanes)
-            out_ref[:, 2 * j + n] = tile.astype(jnp.bfloat16)
+            tile = part[:, :, n * lanes : (n + 1) * lanes].astype(jnp.bfloat16)
+            first_out[:, 2 * y + n] = tile[: blocks // 2]
+            second_out[:, 2 * y + n] = tile[blocks // 2 :]
+
+
+def lowered(hidden_ref, down_own, down_other, y, q):
+    at = pl.ds(pl.multiple_of((4 * y + 2 * q) * 128, 256), 256)
+    return jnp.dot(hidden_ref[0], down_own[:, at], preferred_element_type=jnp.float32) + jnp.dot(
+        hidden_ref[1], down_other[:, at], preferred_element_type=jnp.float32
+    )
+
+
+def own_columns_kernel(place_ref, hidden_ref, down_own, down_other, out_ref):
+    parity = place_ref[4]
+    blocks, features, half, lanes = out_ref.shape
+    for y in range(features // 2):
+        part = lowered(hidden_ref, down_own, down_other, y, parity).reshape(blocks, half, 2 * lanes)
+        for n in range(2):
+            out_ref[:, 2 * y + n] = part[:, :, n * lanes : (n + 1) * lanes].astype(jnp.bfloat16)
 
 
 def final_kernel(returned_ref, stream_ref, col_ref, out_ref):
@@ -335,6 +374,14 @@
 
 def swapped(value):
     return lax.ppermute(value, "c", [(0, 1), (1, 0)])
+
+
+def from_both_sides(first, second):
+    count = lax.axis_size(ROW)
+    return (
+        lax.ppermute(first, ROW, [((i + 1) % count, i) for i in range(count)]),
+        lax.ppermute(second, ROW, [(i, (i + 1) % count) for i in range(count)]),
+    )
 
 
 def body(
@@ -362,11 +409,11 @@
     f32, bf16 = jnp.float32, jnp.bfloat16
     length, width = unfiltered_channel_feed.shape
     blocks = lax.axis_size(SP)
-    peers_x, peers_y, peers_z = (lax.axis_size(a) for a in ("x", "y", "z"))
+    peers_x, peers_y, peers_z = (lax.axis_size(a) for a in ("x", ROW, "z"))
     capacity = 4 * length // blocks
     slots = blocks * capacity
     axes = [lax.axis_index(a) for a in ("x", "z", "c")]
-    place = jnp.stack([*axes, axes[0] % 2]).astype(jnp.int32)
+    place = jnp.stack([*axes, axes[0] % 2, lax.axis_index("p")]).astype(jnp.int32)
 
     rim = CONV // 2
     even_rim, odd_rim, *feeds = call(
@@ -444,35 +491,59 @@
     for weight in (gate_own, up_own, down_own):
         others.append(swapped(weight))
     gate_other, up_other, down_other = others
-    columns = lax.all_to_all(copies, "y", 0, 0, tiled=True)
+    columns = lax.all_to_all(copies, ROW, 0, 0, tiled=True)
     columns, gate_other, up_other, down_other = lax.optimization_barrier(
         (columns, gate_other, up_other, down_other)
     )
     gathered = lax.all_gather(columns, "c", axis=1, tiled=True)
     half = capacity // 2
-    spread = (blocks, peers_y, 2, half, width)
-    everyone = (*SP, *TP)
+    sides = peers_y // 2
+    spread = (blocks, sides, 2, half, width)
+    members = (*SP, "yh", "c")
     stream, outgoing = call(
         stream_kernel,
         [((length, width), bf16), (spread, bf16)],
         (gathered, final_projection_weights, skip_stream_entering, rows),
     )
     arrived = lax.all_to_all(
-        outgoing.reshape(-1, half, width), everyone, 0, 0, tiled=True
-    ).reshape(blocks, 2 * peers_y, half, width)
-    (partial_out,) = call(
+        outgoing.reshape(-1, half, width), members, 0, 0, tiled=True
+    ).reshape(blocks, 2 * sides, half, width)
+    first, second = from_both_sides(arrived[: blocks // 2], arrived[blocks // 2 :])
+    units = gate_own.shape[1]
+    wide = (sides, 2, 2 * width, units)
+    hidden, first_sent, second_sent = call(
         expert_kernel,
+        [((2, slots // 2, units), bf16), (first.shape, bf16), (second.shape, bf16)],
+        (
+            place, gate_other.reshape(wide), up_other.reshape(wide), down_other,
+            arrived, first, second, specialist_rescale_factor.reshape(sides, 2, 1, 2 * width),
+            gate_own.reshape(wide), up_own.reshape(wide), down_own,
+        ),
+        flops=5 * slots * units * D,
+        scratch=[
+            pltpu.VMEM((2, slots // 2, D // 2), bf16),
+            pltpu.VMEM(wide, bf16),
+            pltpu.VMEM(wide, bf16),
+            pltpu.VMEM(down_own.shape, bf16),
+            pltpu.SemaphoreType.DMA((3,)),
+        ],
+        smem=1,
+        hbm=3,
+        room=24,
+    )
+    first_partner, second_partner = from_both_sides(first_sent, second_sent)
+    (kept,) = call(
+        own_columns_kernel,
         [(arrived.shape, bf16)],
-        (
-            arrived, specialist_rescale_factor[None], gate_own, gate_other, up_own, up_other,
-            down_own, down_other,
-        ),
-        flops=6 * slots * gate_own.shape[1] * D,
-        scratch=[pltpu.VMEM((slots // 2, D), bf16)],
-        room=24,
-    )
+        (place, hidden, down_own, down_other),
+        flops=slots * units * D,
+        smem=1,
+        room=12,
+    )
+    partner = jnp.concatenate([first_partner, second_partner], axis=0)
+    partial_out = (kept.astype(f32) + partner.astype(f32)).astype(bf16)
     returned = lax.all_to_all(
-        partial_out.reshape(-1, half, width), everyone, 0, 0, tiled=True
+        partial_out.reshape(-1, half, width), members, 0, 0, tiled=True
     ).reshape(spread)
     (out,) = call(final_kernel, [((length, width), bf16)], (returned, stream, cols))
     return out
@@ -480,7 +551,9 @@
 
 def solution(mesh):
     sizes = dict(mesh.shape)
-    torus = Mesh(mesh.devices.reshape(8, 4, sizes["tp"] // 2, 2), ("z", "x", "y", "c"))
+    torus = Mesh(
+        mesh.devices.reshape(8, 4, sizes["tp"] // 4, 2, 2), ("z", "x", "yh", "p", "c")
+    )
     return jax.shard_map(
         body,
         mesh=torus,

time: 166 us -> 169 us (1.018)
  blocking collectives: 140 us -> 117 us
  waiting for transfers between devices: 0.01 us -> 12 us
  starting transfers between devices: 15.6 us -> 26.3 us
  Pallas kernels: 9.57 us -> 12.1 us
    all_to_all x3, blocking collectives: 104 us -> 81.8 us  [the longest x1 33.6 us: body(): lax.all_to_all(partial_out.reshape(-1, half, width), members, 0, 0, tiled...]
    ppermute x0 -> x4, waiting for transfers between devices: none -> 12 us  [the longest x2 7.66 us: from_both_sides(): lax.ppermute(second, ROW, [(i, (i + 1) % count) for i in range(count)])]
    ppermute x0 -> x4, starting transfers between devices: none -> 10.7 us  [the longest x2 5.39 us: from_both_sides(): lax.ppermute(first, ROW, [((i + 1) % count, i) for i in range(count)])]
    pallas_call x8 -> x9, Pallas kernels: 9.57 us -> 12.1 us  [call(): pl.pallas_call(kernel, out_shape=shapes, in_specs=[SMEM] * smem + [HBM] *...]
  transfers between devices with their start and end apart: 5 -> 9, of which waited for: 0 -> 4; matrix products, arithmetic and copies ran while one was open for 0% -> 0% of each run, Pallas kernels for 1% -> 2%
where the time goes in v6:
time: 169 us; the launch traced here: 168 us
  blocking collectives  117 us (69%)
  starting transfers between devices  26.3 us (16%)
  Pallas kernels  12.1 us (7%)
  waiting for transfers between devices  12 us (7%)
    all_to_all x1, blocking collectives, body(): lax.all_to_all(partial_out.reshape(-1, half, width), members, 0, 0, tiled...  33.6 us
    all_to_all x1, blocking collectives, body(): lax.all_to_all(outgoing.reshape(-1, half, width), members, 0, 0, tiled=True)  29.3 us
    all_to_all x1, blocking collectives, body(): got = lax.all_to_all(onward, 'z', 0, 0, tiled=True)  20.2 us
    all_to_all x1, blocking collectives, body(): columns = lax.all_to_all(copies, ROW, 0, 0, tiled=True)  19 us
    all_to_all x1, blocking collectives, body(): seen = lax.all_to_all(message, 'x', 0, 0, tiled=True)  12.8 us
    pallas_call x9, Pallas kernels, call(): pl.pallas_call(kernel, out_shape=shapes, in_specs=[SMEM] * smem + [HBM] *...  12.1 us
    ppermute x3, starting transfers between devices, swapped(): return lax.ppermute(value, 'c', [(0, 1), (1, 0)])  11 us
    ppermute x2, waiting for transfers between devices, from_both_sides(): lax.ppermute(second, ROW, [(i, (i + 1) % count) for i in range(count)])  7.66 us
  transfers between devices with their start and end apart: 9, of which 4 were waited for; matrix products, arithmetic and copies ran while one was open for 0% of the time, Pallas kernels for 2%

profile of v6, /device:TPU:1, one launch (start us, length us, event | category | flops | bytes accessed | tf_op | source)
XLA Modules:
  0.0 168.1 jit_solution(1871721425208467641)
XLA Ops:
  0.0 0.1 stack.23.place_ref
  0.1 1.4 shard_map.190
  1.5 3.9 %collective-permute-start = (f32[2,384]{1,0:T(2,128)S(1)}, f32[2,384]{1,0:T(2,128)S(1)}, u32[]{:S(2)}, u32[]{:S(2)}) collective-permute-start(f32[2,384]{1,0:T(2,128)S(1)} %get-tuple-element.38), channel_id=1, source_target_pairs={{0,16},{16,0},{32,48},{48,32},{64,80},{80,64},{96,112},{112,96},{1... | collective-permute-start | bytes 9224 | tf_op jit(solution)/shard_map/ppermute | solution.py:429
  5.4 0.7 collective-permute-start.1
  6.1 1.6 shard_map.191
  7.6 0.0 collective-permute-done.even_ref
  7.7 0.0 collective-permute-done.1.odd_ref
  7.7 0.0 copy-start.6
  7.7 0.0 copy-start.9
  7.7 1.1 shard_map.192
  8.8 0.0 copy-start.3
  8.8 0.0 copy-start
  8.8 12.8 %all_to_all.25.seen_ref = bf16[4,272,128]{2,1,0:T(8,128)(2,1)S(1)} all-to-all(bf16[4,272,128]{2,1,0:T(8,128)(2,1)S(1)} %get-tuple-element.44), channel_id=1, replica_groups=mesh['z'=8,'x'=4,'yh'=4,'p'=2,'c'=2] {'x'}, dimensions={0} | all-to-all | bytes 557056 | tf_op jit(solution)/shard_map/all_to_all | solution.py:465
  21.6 0.7 shard_map.193
  22.3 20.2 %all_to_all.26.got_ref = bf16[8,144,128]{2,1,0:T(8,128)(2,1)S(1)} all-to-all(bf16[8,144,128]{2,1,0:T(8,128)(2,1)S(1)} %get-tuple-element.45), channel_id=1, replica_groups=mesh['z'=8,'x'=4,'yh'=4,'p'=2,'c'=2] {'z'}, dimensions={0} | all-to-all | bytes 589824 | tf_op jit(solution)/shard_map/all_to_all | solution.py:472
  42.5 0.0 copy-done.6
  42.5 0.0 copy-done.9
  42.5 1.4 shard_map.194
  43.8 0.0 copy-done.3
  43.8 0.0 copy-start.5
  43.9 6.7 %collective-permute-start.2 = (bf16[2048,256]{1,0:T(8,128)(2,1)S(1)}, bf16[2048,256]{1,0:T(8,128)(2,1)S(1)}, u32[]{:S(2)}, u32[]{:S(2)}) collective-permute-start(bf16[2048,256]{1,0:T(8,128)(2,1)S(1)} %bitcast.28), channel_id=1, source_target_pairs={{0,1},{1,0},{2,3},{3,2},{4,5},{5,4},{6,7},{7,6},{8,9},{9,8},{10,11... | collective-permute-start | bytes 3145736 | tf_op jit(solution)/shard_map/ppermute | solution.py:376
  50.6 1.9 %collective-permute-start.3 = (bf16[2048,256]{1,0:T(8,128)(2,1)}, bf16[2048,256]{1,0:T(8,128)(2,1)S(1)}, u32[]{:S(2)}, u32[]{:S(2)}) collective-permute-start(bf16[2048,256]{1,0:T(8,128)(2,1)} %bitcast.30), channel_id=1, source_target_pairs={{0,1},{1,0},{2,3},{3,2},{4,5},{5,4},{6,7},{7,6},{8,9},{9,8},{10,11... | collective-permute-start | bytes 3145736 | tf_op jit(solution)/shard_map/ppermute | solution.py:376
  52.5 0.0 copy-done
  52.5 2.4 %collective-permute-start.4 = (bf16[256,2048]{1,0:T(8,128)(2,1)S(1)}, bf16[256,2048]{1,0:T(8,128)(2,1)S(1)}, u32[]{:S(2)}, u32[]{:S(2)}) collective-permute-start(bf16[256,2048]{1,0:T(8,128)(2,1)S(1)} %bitcast.24), channel_id=1, source_target_pairs={{0,1},{1,0},{2,3},{3,2},{4,5},{5,4},{6,7},{7,6},{8,9},{9,8},{10,11... | collective-permute-start | bytes 3145736 | tf_op jit(solution)/shard_map/ppermute | solution.py:376
  54.9 19.0 %all_to_all.27 = bf16[8,128,128]{2,1,0:T(8,128)(2,1)S(1)} all-to-all(bf16[8,128,128]{2,1,0:T(8,128)(2,1)S(1)} %shard_map.194), channel_id=1, replica_groups=mesh['z'=8,'x'=4,'yh'=4,'p'=2,'c'=2] {'yh','p'}, dimensions={0} | all-to-all | bytes 524288 | tf_op jit(solution)/shard_map/all_to_all | solution.py:494
  73.9 0.0 collective-permute-done.2
  73.9 0.0 collective-permute-done.3
  73.9 0.0 copy-start.11
  73.9 0.0 collective-permute-done.4.down_in.down_other
  74.0 2.3 %all_gather.3.mixed_ref = bf16[8,256,128]{2,1,0:T(8,128)(2,1)S(1)} all-gather(bf16[8,128,128]{2,1,0:T(8,128)(2,1)S(1)} %all_to_all.27), channel_id=1, replica_groups=mesh['z'=8,'x'=4,'yh'=4,'p'=2,'c'=2] {'c'}, dimensions={1}, use_global_device_ids=true | all-gather | bytes 786432 | tf_op jit(solution)/shard_map/all_gather | solution.py:498
  76.2 0.5 shard_map.195
  76.8 0.0 copy-start.4
  76.8 29.3 %all_to_all.28 = bf16[256,8,128]{2,1,0:T(8,128)(2,1)S(1)} all-to-all(bf16[256,8,128]{2,1,0:T(8,128)(2,1)S(1)} %bitcast.32), channel_id=1, replica_groups=mesh['z'=8,'x'=4,'yh'=4,'p'=2,'c'=2] {'z','x','yh','c'}, dimensions={0} | all-to-all | bytes 1048576 | tf_op jit(solution)/shard_map/all_to_all | solution.py:508
  106.1 0.0 copy-start.8
  106.1 1.9 %collective-permute-start.5 = (bf16[16,8,8,128]{3,2,1,0:T(8,128)(2,1)S(1)}, bf16[16,8,8,128]{3,2,1,0:T(8,128)(2,1)S(1)}, u32[]{:S(2)}, u32[]{:S(2)}) collective-permute-start(bf16[16,8,8,128]{3,2,1,0:T(8,128)(2,1)S(1)} %bitcast.39), channel_id=1, source_target_pairs={{2,0},{4,2},{6,4},{8,6},{10,8},{12,10},{14,12},{0,14},{3,1},{5,3},... | collective-permute-start | bytes 786440 | tf_op jit(solution)/shard_map/ppermute | solution.py:382
  108.0 3.4 %collective-permute-start.6 = (bf16[16,8,8,128]{3,2,1,0:T(8,128)(2,1)S(1)}, bf16[16,8,8,128]{3,2,1,0:T(8,128)(2,1)S(1)}, u32[]{:S(2)}, u32[]{:S(2)}) collective-permute-start(bf16[16,8,8,128]{3,2,1,0:T(8,128)(2,1)S(1)} %bitcast.38), channel_id=1, source_target_pairs={{0,2},{2,4},{4,6},{6,8},{8,10},{10,12},{12,14},{14,0},{1,3},{3,5},... | collective-permute-start | bytes 786440 | tf_op jit(solution)/shard_map/ppermute | solution.py:383
  111.4 3.2 %collective-permute-done.5.first_ref = bf16[16,8,8,128]{3,2,1,0:T(8,128)(2,1)S(1)} collective-permute-done((bf16[16,8,8,128]{3,2,1,0:T(8,128)(2,1)S(1)}, bf16[16,8,8,128]{3,2,1,0:T(8,128)(2,1)S(1)}, u32[]{:S(2)}, u32[]{:S(2)}) %collective-permute-start.5) | collective-permute-done | bytes 262176 | tf_op jit(solution)/shard_map/ppermute | solution.py:382
  114.5 3.1 %collective-permute-done.6.second_ref = bf16[16,8,8,128]{3,2,1,0:T(8,128)(2,1)S(1)} collective-permute-done((bf16[16,8,8,128]{3,2,1,0:T(8,128)(2,1)S(1)}, bf16[16,8,8,128]{3,2,1,0:T(8,128)(2,1)S(1)}, u32[]{:S(2)}, u32[]{:S(2)}) %collective-permute-start.6) | collective-permute-done | bytes 262176 | tf_op jit(solution)/shard_map/ppermute | solution.py:383
  117.7 3.6 %shard_map.196 = (bf16[2,256,256]{2,1,0:T(8,128)(2,1)S(1)}, bf16[16,8,8,128]{3,2,1,0:T(8,128)(2,1)S(1)}, bf16[16,8,8,128]{3,2,1,0:T(8,128)(2,1)S(1)}) custom-call(s32[5]{0:T(128)S(1)} %stack.23.place_ref, bf16[4,2,256,256]{3,2,1,0:T(8,128)(2,1)} %bitcast.36, bf16[4,2,256,256]{3,2,1,0:T(8,128)(2,1)} %bitcast.37, bf16[256,2048]{1,0:T(8,128)(2,1)} %copy-done.1, ...), custom_call_target="tpu_custom_call" | custom-call | flops 1342177280 | bytes 8134676 | tf_op jit(solution)/shard_map/pallas_call | solution.py:38
  121.3 3.5 %collective-permute-start.7 = (bf16[16,8,8,128]{3,2,1,0:T(8,128)(2,1)S(1)}, bf16[16,8,8,128]{3,2,1,0:T(8,128)(2,1)S(1)}, u32[]{:S(2)}, u32[]{:S(2)}) collective-permute-start(bf16[16,8,8,128]{3,2,1,0:T(8,128)(2,1)S(1)} %get-tuple-element.62), channel_id=1, source_target_pairs={{2,0},{4,2},{6,4},{8,6},{10,8},{12,10},{14,12},{0,14},{3,1},{5,3},... | collective-permute-start | bytes 786440 | tf_op jit(solution)/shard_map/ppermute | solution.py:382
  124.8 1.9 %collective-permute-start.8 = (bf16[16,8,8,128]{3,2,1,0:T(8,128)(2,1)S(1)}, bf16[16,8,8,128]{3,2,1,0:T(8,128)(2,1)S(1)}, u32[]{:S(2)}, u32[]{:S(2)}) collective-permute-start(bf16[16,8,8,128]{3,2,1,0:T(8,128)(2,1)S(1)} %get-tuple-element.63), channel_id=1, source_target_pairs={{0,2},{2,4},{4,6},{6,8},{8,10},{10,12},{12,14},{14,0},{1,3},{3,5},... | collective-permute-start | bytes 786440 | tf_op jit(solution)/shard_map/ppermute | solution.py:383
  126.7 0.0 copy-done.2
  126.7 1.0 shard_map.197
  127.8 1.2 collective-permute-done.7
  128.9 4.5 %collective-permute-done.8 = bf16[16,8,8,128]{3,2,1,0:T(8,128)(2,1)S(1)} collective-permute-done((bf16[16,8,8,128]{3,2,1,0:T(8,128)(2,1)S(1)}, bf16[16,8,8,128]{3,2,1,0:T(8,128)(2,1)S(1)}, u32[]{:S(2)}, u32[]{:S(2)}) %collective-permute-start.8) | collective-permute-done | bytes 262176 | tf_op jit(solution)/shard_map/ppermute | solution.py:383
  133.4 0.2 add_convert_fusion
  133.6 33.6 %all_to_all.29 = bf16[256,8,128]{2,1,0:T(8,128)(2,1)S(1)} all-to-all(bf16[256,8,128]{2,1,0:T(8,128)(2,1)S(1)} %bitcast.35), channel_id=1, replica_groups=mesh['z'=8,'x'=4,'yh'=4,'p'=2,'c'=2] {'z','x','yh','c'}, dimensions={0} | all-to-all | bytes 1048576 | tf_op jit(solution)/shard_map/all_to_all | solution.py:545
  167.2 0.9 shard_map.198
  (12 shorter events, 0.1 us)
Async XLA Ops:
  1.5 6.2 %collective-permute-start = (f32[2,384]{1,0:T(2,128)S(1)}, f32[2,384]{1,0:T(2,128)S(1)}, u32[]{:S(2)}, u32[]{:S(2)}) collective-permute-start(f32[2,384]{1,0:T(2,128)S(1)} %get-tuple-element.38), channel_id=1, source_target_pairs={{0,16},{16,0},{32,48},{48,32},{64,80},{80,64},{96,112},{112,96},{1... | collective-permute-start | bytes 9224 | tf_op jit(solution)/shard_map/ppermute | solution.py:429
  5.4 2.3 %collective-permute-start.1 = (f32[2,384]{1,0:T(2,128)S(1)}, f32[2,384]{1,0:T(2,128)S(1)}, u32[]{:S(2)}, u32[]{:S(2)}) collective-permute-start(f32[2,384]{1,0:T(2,128)S(1)} %get-tuple-element.39), channel_id=1, source_target_pairs={{16,32},{32,16},{48,64},{64,48},{80,96},{96,80},{112,128},{128,112... | collective-permute-start | bytes 9224 | tf_op jit(solution)/shard_map/ppermute | solution.py:430
  7.7 34.8 %copy-start.6 = (bf16[128,128]{1,0:T(8,128)(2,1)S(1)}, bf16[128,128]{1,0:T(8,128)(2,1)}, u32[]{:S(2)}) copy-start(bf16[128,128]{1,0:T(8,128)(2,1)} %valve_ref.1) | copy-start | bytes 98308
  7.7 34.8 %copy-start.9 = (f32[128]{0:T(128)S(1)}, f32[128]{0:T(128)}, u32[]{:S(2)}) copy-start(f32[128]{0:T(128)} %param.31) | copy-start | bytes 1540
  8.8 35.0 %copy-start.3 = (bf16[1,2048,256]{2,1,0:T(8,128)(2,1)S(1)}, bf16[1,2048,256]{2,1,0:T(8,128)(2,1)}, u32[]{:S(2)}) copy-start(bf16[1,2048,256]{2,1,0:T(8,128)(2,1)} %param.37) | copy-start | bytes 3145732
  8.8 43.7 %copy-start = (bf16[1,256,2048]{2,1,0:T(8,128)(2,1)S(1)}, bf16[1,256,2048]{2,1,0:T(8,128)(2,1)}, u32[]{:S(2)}) copy-start(bf16[1,256,2048]{2,1,0:T(8,128)(2,1)} %param.39) | copy-start | bytes 3145732
  43.8 32.4 %copy-start.5 = (bf16[2048,128]{1,0:T(8,128)(2,1)S(1)}, bf16[2048,128]{1,0:T(8,128)(2,1)}, u32[]{:S(2)}) copy-start(bf16[2048,128]{1,0:T(8,128)(2,1)} %weight_ref.1) | copy-start | bytes 1572868
  43.9 30.1 %collective-permute-start.2 = (bf16[2048,256]{1,0:T(8,128)(2,1)S(1)}, bf16[2048,256]{1,0:T(8,128)(2,1)S(1)}, u32[]{:S(2)}, u32[]{:S(2)}) collective-permute-start(bf16[2048,256]{1,0:T(8,128)(2,1)S(1)} %bitcast.28), channel_id=1, source_target_pairs={{0,1},{1,0},{2,3},{3,2},{4,5},{5,4},{6,7},{7,6},{8,9},{9,8},{10,11... | collective-permute-start | bytes 3145736 | tf_op jit(solution)/shard_map/ppermute | solution.py:376
  50.6 23.3 %collective-permute-start.3 = (bf16[2048,256]{1,0:T(8,128)(2,1)}, bf16[2048,256]{1,0:T(8,128)(2,1)S(1)}, u32[]{:S(2)}, u32[]{:S(2)}) collective-permute-start(bf16[2048,256]{1,0:T(8,128)(2,1)} %bitcast.30), channel_id=1, source_target_pairs={{0,1},{1,0},{2,3},{3,2},{4,5},{5,4},{6,7},{7,6},{8,9},{9,8},{10,11... | collective-permute-start | bytes 3145736 | tf_op jit(solution)/shard_map/ppermute | solution.py:376
  52.5 21.4 %collective-permute-start.4 = (bf16[256,2048]{1,0:T(8,128)(2,1)S(1)}, bf16[256,2048]{1,0:T(8,128)(2,1)S(1)}, u32[]{:S(2)}, u32[]{:S(2)}) collective-permute-start(bf16[256,2048]{1,0:T(8,128)(2,1)S(1)} %bitcast.24), channel_id=1, source_target_pairs={{0,1},{1,0},{2,3},{3,2},{4,5},{5,4},{6,7},{7,6},{8,9},{9,8},{10,11... | collective-permute-start | bytes 3145736 | tf_op jit(solution)/shard_map/ppermute | solution.py:376
  73.9 2.3 %copy-start.7 = (bf16[128,128]{1,0:T(8,128)(2,1)S(1)}, bf16[128,128]{1,0:T(8,128)(2,1)}, u32[]{:S(2)}) copy-start(bf16[128,128]{1,0:T(8,128)(2,1)} %skip_ref.1) | copy-start | bytes 98308
  73.9 32.1 %copy-start.10 = (bf16[2048,256]{1,0:T(8,128)(2,1)}, bf16[2048,256]{1,0:T(8,128)(2,1)S(1)}, u32[]{:S(2)}) copy-start(bf16[2048,256]{1,0:T(8,128)(2,1)S(1)} %collective-permute-done.2) | copy-start | bytes 3145732
  73.9 43.8 %copy-start.11 = (bf16[2048,256]{1,0:T(8,128)(2,1)}, bf16[2048,256]{1,0:T(8,128)(2,1)S(1)}, u32[]{:S(2)}) copy-start(bf16[2048,256]{1,0:T(8,128)(2,1)S(1)} %collective-permute-done.3) | copy-start | bytes 3145732
  74.0 32.1 %copy-start.1 = (bf16[256,2048]{1,0:T(8,128)(2,1)}, bf16[256,2048]{1,0:T(8,128)(2,1)S(1)}, u32[]{:S(2)}) copy-start(bf16[256,2048]{1,0:T(8,128)(2,1)S(1)} %collective-permute-done.4.down_in.down_other) | copy-start | bytes 3145732
  76.8 40.9 %copy-start.4 = (bf16[1,2048,256]{2,1,0:T(8,128)(2,1)S(1)}, bf16[1,2048,256]{2,1,0:T(8,128)(2,1)}, u32[]{:S(2)}) copy-start(bf16[1,2048,256]{2,1,0:T(8,128)(2,1)} %param.38) | copy-start | bytes 3145732
  106.1 11.6 %copy-start.8 = (f32[2048]{0:T(1024)S(1)}, f32[2048]{0:T(1024)}, u32[]{:S(2)}) copy-start(f32[2048]{0:T(1024)} %param.33) | copy-start | bytes 24580
  106.1 8.5 %collective-permute-start.5 = (bf16[16,8,8,128]{3,2,1,0:T(8,128)(2,1)S(1)}, bf16[16,8,8,128]{3,2,1,0:T(8,128)(2,1)S(1)}, u32[]{:S(2)}, u32[]{:S(2)}) collective-permute-start(bf16[16,8,8,128]{3,2,1,0:T(8,128)(2,1)S(1)} %bitcast.39), channel_id=1, source_target_pairs={{2,0},{4,2},{6,4},{8,6},{10,8},{12,10},{14,12},{0,14},{3,1},{5,3},... | collective-permute-start | bytes 786440 | tf_op jit(solution)/shard_map/ppermute | solution.py:382
  108.0 9.7 %collective-permute-start.6 = (bf16[16,8,8,128]{3,2,1,0:T(8,128)(2,1)S(1)}, bf16[16,8,8,128]{3,2,1,0:T(8,128)(2,1)S(1)}, u32[]{:S(2)}, u32[]{:S(2)}) collective-permute-start(bf16[16,8,8,128]{3,2,1,0:T(8,128)(2,1)S(1)} %bitcast.38), channel_id=1, source_target_pairs={{0,2},{2,4},{4,6},{6,8},{8,10},{10,12},{12,14},{14,0},{1,3},{3,5},... | collective-permute-start | bytes 786440 | tf_op jit(solution)/shard_map/ppermute | solution.py:383
  117.7 9.0 %copy-start.2 = (bf16[256,2048]{1,0:T(8,128)(2,1)S(1)}, bf16[256,2048]{1,0:T(8,128)(2,1)}, u32[]{:S(2)}) copy-start(bf16[256,2048]{1,0:T(8,128)(2,1)} %copy-done.1) | copy-start | bytes 3145732
  121.3 7.6 %collective-permute-start.7 = (bf16[16,8,8,128]{3,2,1,0:T(8,128)(2,1)S(1)}, bf16[16,8,8,128]{3,2,1,0:T(8,128)(2,1)S(1)}, u32[]{:S(2)}, u32[]{:S(2)}) collective-permute-start(bf16[16,8,8,128]{3,2,1,0:T(8,128)(2,1)S(1)} %get-tuple-element.62), channel_id=1, source_target_pairs={{2,0},{4,2},{6,4},{8,6},{10,8},{12,10},{14,12},{0,14},{3,1},{5,3},... | collective-permute-start | bytes 786440 | tf_op jit(solution)/shard_map/ppermute | solution.py:382
  124.8 8.6 %collective-permute-start.8 = (bf16[16,8,8,128]{3,2,1,0:T(8,128)(2,1)S(1)}, bf16[16,8,8,128]{3,2,1,0:T(8,128)(2,1)S(1)}, u32[]{:S(2)}, u32[]{:S(2)}) collective-permute-start(bf16[16,8,8,128]{3,2,1,0:T(8,128)(2,1)S(1)} %get-tuple-element.63), channel_id=1, source_target_pairs={{0,2},{2,4},{4,6},{6,8},{8,10},{10,12},{12,14},{14,0},{1,3},{3,5},... | collective-permute-start | bytes 786440 | tf_op jit(solution)/shard_map/ppermute | solution.py:383

commit v7 on v5

--- a/solution.py
+++ b/solution.py
@@ -289,8 +289,15 @@
 
 
 def expert_kernel(
-    rows_ref, gain_ref, gate_own, gate_other, up_own, up_other, down_own, down_other, out_ref, scaled
+    gate_in, up_in, down_in, rows_ref, gain_ref, gate_own, up_own, down_own, out_ref,
+    scaled, gate_other, up_other, down_other, done,
 ):
+    copies = [
+        pltpu.make_async_copy(a, b, done.at[n])
+        for n, (a, b) in enumerate(((gate_in, gate_other), (up_in, up_other), (down_in, down_other)))
+    ]
+    for copy in copies:
+        copy.start()
     blocks, features, half, lanes = rows_ref.shape
     count = blocks * half
     squares = jnp.zeros((count, lanes), jnp.float32)
@@ -302,10 +309,14 @@
     scale = lax.rsqrt(jnp.sum(squares, axis=1, keepdims=True) / D + stream_eps)
     whole = scaled[...]
     hidden = []
-    for gate_ref, up_ref in ((gate_own, up_own), (gate_other, up_other)):
+    for n, (gate_ref, up_ref) in enumerate(((gate_own, up_own), (gate_other, up_other))):
+        if n == 1:
+            copies[0].wait()
+            copies[1].wait()
         gate = jnp.dot(whole, gate_ref[...], preferred_element_type=jnp.float32) * scale
         upward = jnp.dot(whole, up_ref[...], preferred_element_type=jnp.float32) * scale
         hidden.append((jax.nn.silu(gate) * upward).astype(jnp.bfloat16))
+    copies[2].wait()
     step = 2 * lanes
     for j in range(features // 2):
         at = slice(j * step, (j + 1) * step)
@@ -464,11 +475,18 @@
         expert_kernel,
         [(arrived.shape, bf16)],
         (
-            arrived, specialist_rescale_factor[None], gate_own, gate_other, up_own, up_other,
-            down_own, down_other,
+            gate_other, up_other, down_other, arrived, specialist_rescale_factor[None],
+            gate_own, up_own, down_own,
         ),
         flops=6 * slots * gate_own.shape[1] * D,
-        scratch=[pltpu.VMEM((slots // 2, D), bf16)],
+        scratch=[
+            pltpu.VMEM((slots // 2, D), bf16),
+            pltpu.VMEM(gate_own.shape, bf16),
+            pltpu.VMEM(up_own.shape, bf16),
+            pltpu.VMEM(down_own.shape, bf16),
+            pltpu.SemaphoreType.DMA((3,)),
+        ],
+        hbm=3,
         room=24,
     )
     returned = lax.all_to_all(

time: 166 us -> 167 us (level)
  no operation moved by 1% of the time
where the time goes in v7:
time: 167 us
  blocking collectives  140 us (84%)
  starting transfers between devices  15.6 us (9%)
  Pallas kernels  11.2 us (7%)
    all_to_all x1, blocking collectives, body(): lax.all_to_all(outgoing.reshape(-1, half, width), everyone, 0, 0, tiled=T...  42.8 us
    all_to_all x1, blocking collectives, body(): lax.all_to_all(partial_out.reshape(-1, half, width), everyone, 0, 0, tile...  42.5 us
    all_to_all x1, blocking collectives, body(): got = lax.all_to_all(onward, 'z', 0, 0, tiled=True)  20.2 us
    all_to_all x1, blocking collectives, body(): columns = lax.all_to_all(copies, 'y', 0, 0, tiled=True)  19 us
    all_to_all x1, blocking collectives, body(): seen = lax.all_to_all(message, 'x', 0, 0, tiled=True)  12.8 us
    pallas_call x8, Pallas kernels, call(): pl.pallas_call(kernel, out_shape=shapes, in_specs=[SMEM] * smem + [HBM] *...  11.2 us
    ppermute x3, starting transfers between devices, swapped(): return lax.ppermute(value, 'c', [(0, 1), (1, 0)])  11 us
    ppermute x1, starting transfers between devices, body(): lax.ppermute(even_rim, SP, [p for a, b in pairs[0::2] for p in ((a, b), (...  3.94 us
  transfers between devices with their start and end apart: 5, of which 0 were waited for; matrix products, arithmetic and copies ran while one was open for 0% of the time, Pallas kernels for 1%

profile of v7, /device:TPU:1, one launch (start us, length us, event | category | flops | bytes accessed | tf_op | source)
XLA Modules:
  0.0 166.8 jit_solution(14871738895861975239)
XLA Ops:
  0.0 0.1 pad_add_fusion.place_ref
  0.1 1.4 shard_map.190
  1.5 3.9 %collective-permute-start = (f32[2,384]{1,0:T(2,128)S(1)}, f32[2,384]{1,0:T(2,128)S(1)}, u32[]{:S(2)}, u32[]{:S(2)}) collective-permute-start(f32[2,384]{1,0:T(2,128)S(1)} %get-tuple-element.35), channel_id=1, source_target_pairs={{0,16},{16,0},{32,48},{48,32},{64,80},{80,64},{96,112},{112,96},{1... | collective-permute-start | bytes 9224 | tf_op jit(solution)/shard_map/ppermute | solution.py:393
  5.4 0.7 collective-permute-start.1
  6.1 1.6 shard_map.191
  7.6 0.0 collective-permute-done.even_ref
  7.6 0.0 collective-permute-done.1.odd_ref
  7.7 0.0 copy-start.4
  7.7 0.0 copy-start.7
  7.7 1.1 shard_map.192
  8.8 0.0 copy-start
  8.8 0.0 copy-start.1
  8.8 12.8 %all_to_all.25.seen_ref = bf16[4,272,128]{2,1,0:T(8,128)(2,1)S(1)} all-to-all(bf16[4,272,128]{2,1,0:T(8,128)(2,1)S(1)} %get-tuple-element.41), channel_id=1, replica_groups=mesh['z'=8,'x'=4,'y'=8,'c'=2] {'x'}, dimensions={0} | all-to-all | bytes 557056 | tf_op jit(solution)/shard_map/all_to_all | solution.py:429
  21.6 0.7 shard_map.193
  22.3 20.2 %all_to_all.26.got_ref = bf16[8,144,128]{2,1,0:T(8,128)(2,1)S(1)} all-to-all(bf16[8,144,128]{2,1,0:T(8,128)(2,1)S(1)} %get-tuple-element.42), channel_id=1, replica_groups=mesh['z'=8,'x'=4,'y'=8,'c'=2] {'z'}, dimensions={0} | all-to-all | bytes 589824 | tf_op jit(solution)/shard_map/all_to_all | solution.py:436
  42.5 0.0 copy-done.4
  42.5 0.0 copy-done.7
  42.5 1.4 shard_map.194
  43.8 0.0 copy-done
  43.8 0.0 copy-start.3
  43.9 6.7 %collective-permute-start.2 = (bf16[2048,256]{1,0:T(8,128)(2,1)S(1)}, bf16[2048,256]{1,0:T(8,128)(2,1)S(1)}, u32[]{:S(2)}, u32[]{:S(2)}) collective-permute-start(bf16[2048,256]{1,0:T(8,128)(2,1)S(1)} %bitcast.19), channel_id=1, source_target_pairs={{0,1},{1,0},{2,3},{3,2},{4,5},{5,4},{6,7},{7,6},{8,9},{9,8},{10,11... | collective-permute-start | bytes 3145736 | tf_op jit(solution)/shard_map/ppermute | solution.py:348
  50.6 0.0 copy-done.1
  50.6 1.9 %collective-permute-start.3 = (bf16[2048,256]{1,0:T(8,128)(2,1)S(1)}, bf16[2048,256]{1,0:T(8,128)(2,1)S(1)}, u32[]{:S(2)}, u32[]{:S(2)}) collective-permute-start(bf16[2048,256]{1,0:T(8,128)(2,1)S(1)} %bitcast.21), channel_id=1, source_target_pairs={{0,1},{1,0},{2,3},{3,2},{4,5},{5,4},{6,7},{7,6},{8,9},{9,8},{10,11... | collective-permute-start | bytes 3145736 | tf_op jit(solution)/shard_map/ppermute | solution.py:348
  52.5 2.4 %collective-permute-start.4 = (bf16[256,2048]{1,0:T(8,128)(2,1)}, bf16[256,2048]{1,0:T(8,128)(2,1)S(1)}, u32[]{:S(2)}, u32[]{:S(2)}) collective-permute-start(bf16[256,2048]{1,0:T(8,128)(2,1)} %bitcast.23), channel_id=1, source_target_pairs={{0,1},{1,0},{2,3},{3,2},{4,5},{5,4},{6,7},{7,6},{8,9},{9,8},{10,11... | collective-permute-start | bytes 3145736 | tf_op jit(solution)/shard_map/ppermute | solution.py:348
  54.9 19.0 %all_to_all.27 = bf16[8,128,128]{2,1,0:T(8,128)(2,1)S(1)} all-to-all(bf16[8,128,128]{2,1,0:T(8,128)(2,1)S(1)} %shard_map.194), channel_id=1, replica_groups=mesh['z'=8,'x'=4,'y'=8,'c'=2] {'y'}, dimensions={0} | all-to-all | bytes 524288 | tf_op jit(solution)/shard_map/all_to_all | solution.py:458
  73.9 0.0 copy-start.5
  73.9 0.0 collective-permute-done.2.gate_in
  73.9 0.0 copy-start.8
  73.9 0.0 collective-permute-done.3.up_in
  73.9 0.0 copy-start.9
  73.9 0.0 collective-permute-done.4.down_in
  73.9 0.0 copy-start.10
  74.0 2.3 %all_gather.3.mixed_ref = bf16[8,256,128]{2,1,0:T(8,128)(2,1)S(1)} all-gather(bf16[8,128,128]{2,1,0:T(8,128)(2,1)S(1)} %all_to_all.27), channel_id=1, replica_groups=mesh['z'=8,'x'=4,'y'=8,'c'=2] {'c'}, dimensions={1}, use_global_device_ids=true | all-gather | bytes 786432 | tf_op jit(solution)/shard_map/all_gather | solution.py:462
  76.2 0.0 copy-done.3
  76.2 0.0 copy-done.5
  76.2 0.5 shard_map.195
  76.8 0.0 copy-start.2
  76.8 0.0 copy-start.6
  76.8 42.8 %all_to_all.28 = bf16[512,8,128]{2,1,0:T(8,128)(2,1)S(1)} all-to-all(bf16[512,8,128]{2,1,0:T(8,128)(2,1)S(1)} %bitcast.25), channel_id=1, replica_groups=mesh['z'=8,'x'=4,'y'=8,'c'=2] {'z','x','y','c'}, dimensions={0} | all-to-all | bytes 2097152 | tf_op jit(solution)/shard_map/all_to_all | solution.py:471
  119.6 0.0 copy-done.8
  119.6 0.0 copy-done.9
  119.6 0.0 copy-done.10
  119.6 0.0 copy-done.2
  119.6 0.0 copy-done.6
  119.6 3.6 %shard_map.196 = bf16[32,16,8,128]{3,2,1,0:T(8,128)(2,1)S(1)} custom-call(bf16[2048,256]{1,0:T(8,128)(2,1)} %copy-done.8, bf16[2048,256]{1,0:T(8,128)(2,1)} %copy-done.9, bf16[256,2048]{1,0:T(8,128)(2,1)} %copy-done.10, bf16[32,16,8,128]{3,2,1,0:T(8,128)(2,1)S(1)} %bitcast.16, f32[1,2048]{1,0:T(1,128)S(1)} %bitcast.26, bf16[2048,256]{1,0:T(8,128)(2,1)S(1)} %bitcast.20, ...), custom_call_target="tpu_custom_call" | custom-call | flops 1610612736 | bytes 8396800 | tf_op jit(solution)/shard_map/pallas_call | solution.py:37
  123.3 42.5 %all_to_all.29 = bf16[512,8,128]{2,1,0:T(8,128)(2,1)S(1)} all-to-all(bf16[512,8,128]{2,1,0:T(8,128)(2,1)S(1)} %bitcast.17), channel_id=1, replica_groups=mesh['z'=8,'x'=4,'y'=8,'c'=2] {'z','x','y','c'}, dimensions={0} | all-to-all | bytes 2097152 | tf_op jit(solution)/shard_map/all_to_all | solution.py:492
  165.8 1.0 shard_map.197
Async XLA Ops:
  1.5 6.2 %collective-permute-start = (f32[2,384]{1,0:T(2,128)S(1)}, f32[2,384]{1,0:T(2,128)S(1)}, u32[]{:S(2)}, u32[]{:S(2)}) collective-permute-start(f32[2,384]{1,0:T(2,128)S(1)} %get-tuple-element.35), channel_id=1, source_target_pairs={{0,16},{16,0},{32,48},{48,32},{64,80},{80,64},{96,112},{112,96},{1... | collective-permute-start | bytes 9224 | tf_op jit(solution)/shard_map/ppermute | solution.py:393
  5.4 2.3 %collective-permute-start.1 = (f32[2,384]{1,0:T(2,128)S(1)}, f32[2,384]{1,0:T(2,128)S(1)}, u32[]{:S(2)}, u32[]{:S(2)}) collective-permute-start(f32[2,384]{1,0:T(2,128)S(1)} %get-tuple-element.36), channel_id=1, source_target_pairs={{16,32},{32,16},{48,64},{64,48},{80,96},{96,80},{112,128},{128,112... | collective-permute-start | bytes 9224 | tf_op jit(solution)/shard_map/ppermute | solution.py:394
  7.7 34.8 %copy-start.4 = (bf16[128,128]{1,0:T(8,128)(2,1)S(1)}, bf16[128,128]{1,0:T(8,128)(2,1)}, u32[]{:S(2)}) copy-start(bf16[128,128]{1,0:T(8,128)(2,1)} %valve_ref.1) | copy-start | bytes 98308
  7.7 34.8 %copy-start.7 = (f32[128]{0:T(128)S(1)}, f32[128]{0:T(128)}, u32[]{:S(2)}) copy-start(f32[128]{0:T(128)} %param.31) | copy-start | bytes 1540
  8.8 35.0 %copy-start = (bf16[1,2048,256]{2,1,0:T(8,128)(2,1)S(1)}, bf16[1,2048,256]{2,1,0:T(8,128)(2,1)}, u32[]{:S(2)}) copy-start(bf16[1,2048,256]{2,1,0:T(8,128)(2,1)} %param.37) | copy-start | bytes 3145732
  8.8 41.8 %copy-start.1 = (bf16[1,2048,256]{2,1,0:T(8,128)(2,1)S(1)}, bf16[1,2048,256]{2,1,0:T(8,128)(2,1)}, u32[]{:S(2)}) copy-start(bf16[1,2048,256]{2,1,0:T(8,128)(2,1)} %param.38) | copy-start | bytes 3145732
  43.8 32.4 %copy-start.3 = (bf16[2048,128]{1,0:T(8,128)(2,1)S(1)}, bf16[2048,128]{1,0:T(8,128)(2,1)}, u32[]{:S(2)}) copy-start(bf16[2048,128]{1,0:T(8,128)(2,1)} %weight_ref.1) | copy-start | bytes 1572868
  43.9 30.1 %collective-permute-start.2 = (bf16[2048,256]{1,0:T(8,128)(2,1)S(1)}, bf16[2048,256]{1,0:T(8,128)(2,1)S(1)}, u32[]{:S(2)}, u32[]{:S(2)}) collective-permute-start(bf16[2048,256]{1,0:T(8,128)(2,1)S(1)} %bitcast.19), channel_id=1, source_target_pairs={{0,1},{1,0},{2,3},{3,2},{4,5},{5,4},{6,7},{7,6},{8,9},{9,8},{10,11... | collective-permute-start | bytes 3145736 | tf_op jit(solution)/shard_map/ppermute | solution.py:348
  50.6 23.3 %collective-permute-start.3 = (bf16[2048,256]{1,0:T(8,128)(2,1)S(1)}, bf16[2048,256]{1,0:T(8,128)(2,1)S(1)}, u32[]{:S(2)}, u32[]{:S(2)}) collective-permute-start(bf16[2048,256]{1,0:T(8,128)(2,1)S(1)} %bitcast.21), channel_id=1, source_target_pairs={{0,1},{1,0},{2,3},{3,2},{4,5},{5,4},{6,7},{7,6},{8,9},{9,8},{10,11... | collective-permute-start | bytes 3145736 | tf_op jit(solution)/shard_map/ppermute | solution.py:348
  52.5 21.4 %collective-permute-start.4 = (bf16[256,2048]{1,0:T(8,128)(2,1)}, bf16[256,2048]{1,0:T(8,128)(2,1)S(1)}, u32[]{:S(2)}, u32[]{:S(2)}) collective-permute-start(bf16[256,2048]{1,0:T(8,128)(2,1)} %bitcast.23), channel_id=1, source_target_pairs={{0,1},{1,0},{2,3},{3,2},{4,5},{5,4},{6,7},{7,6},{8,9},{9,8},{10,11... | collective-permute-start | bytes 3145736 | tf_op jit(solution)/shard_map/ppermute | solution.py:348
  73.9 2.3 %copy-start.5 = (bf16[128,128]{1,0:T(8,128)(2,1)S(1)}, bf16[128,128]{1,0:T(8,128)(2,1)}, u32[]{:S(2)}) copy-start(bf16[128,128]{1,0:T(8,128)(2,1)} %skip_ref.1) | copy-start | bytes 98308
  73.9 45.7 %copy-start.8 = (bf16[2048,256]{1,0:T(8,128)(2,1)}, bf16[2048,256]{1,0:T(8,128)(2,1)S(1)}, u32[]{:S(2)}) copy-start(bf16[2048,256]{1,0:T(8,128)(2,1)S(1)} %collective-permute-done.2.gate_in) | copy-start | bytes 3145732
  73.9 45.7 %copy-start.9 = (bf16[2048,256]{1,0:T(8,128)(2,1)}, bf16[2048,256]{1,0:T(8,128)(2,1)S(1)}, u32[]{:S(2)}) copy-start(bf16[2048,256]{1,0:T(8,128)(2,1)S(1)} %collective-permute-done.3.up_in) | copy-start | bytes 3145732
  73.9 45.7 %copy-start.10 = (bf16[256,2048]{1,0:T(8,128)(2,1)}, bf16[256,2048]{1,0:T(8,128)(2,1)S(1)}, u32[]{:S(2)}) copy-start(bf16[256,2048]{1,0:T(8,128)(2,1)S(1)} %collective-permute-done.4.down_in) | copy-start | bytes 3145732
  76.8 42.9 %copy-start.2 = (bf16[1,256,2048]{2,1,0:T(8,128)(2,1)S(1)}, bf16[1,256,2048]{2,1,0:T(8,128)(2,1)}, u32[]{:S(2)}) copy-start(bf16[1,256,2048]{2,1,0:T(8,128)(2,1)} %param.39) | copy-start | bytes 3145732
  76.8 42.9 %copy-start.6 = (f32[2048]{0:T(1024)S(1)}, f32[2048]{0:T(1024)}, u32[]{:S(2)}) copy-start(f32[2048]{0:T(1024)} %param.33) | copy-start | bytes 24580

commit v8 on v7

--- a/solution.py
+++ b/solution.py
@@ -157,8 +157,8 @@
     x_block = parts[0].astype(jnp.float32)
     b_block = parts[1].astype(jnp.float32)
     left = iota((length, width), 1) < HD
-    logs = jnp.zeros((16, width), jnp.float32)
-    line = iota((16, width), 0)
+    logs = jnp.zeros((8, width), jnp.float32)
+    line = iota((8, width), 0)
     for d, last in ((0, length - 1), (1, 0)):
         weight = []
         for h in range(2):
@@ -205,7 +205,7 @@
 def row_kernel(place_ref, seen_ref, message_ref, near_ref, ahead_ref):
     my_x, my_z = place_ref[0], place_ref[1]
     peers, rows = seen_ref.shape[0], near_ref.shape[1]
-    line = iota((16, 128), 0)
+    line = iota((8, 128), 0)
     out = []
     ahead_ref[...] = jnp.zeros_like(ahead_ref)
     for d in range(2):
@@ -222,7 +222,7 @@
                 far[h] = far[h] + logs[h]
                 ahead[h] = ahead[h] + jnp.where(passed, logs[h], 0.0)
         near_ref[d] = near
-        tile = jnp.zeros((16, 128), jnp.float32)
+        tile = jnp.zeros((8, 128), jnp.float32)
         for h in range(2):
             ahead_ref[2 * d + h : 2 * d + h + 1, :] = ahead[h]
             high = far[h].astype(jnp.bfloat16).astype(jnp.float32)
@@ -312,8 +312,9 @@
     for n, (gate_ref, up_ref) in enumerate(((gate_own, up_own), (gate_other, up_other))):
         if n == 1:
             copies[0].wait()
+        gate = jnp.dot(whole, gate_ref[...], preferred_element_type=jnp.float32) * scale
+        if n == 1:
             copies[1].wait()
-        gate = jnp.dot(whole, gate_ref[...], preferred_element_type=jnp.float32) * scale
         upward = jnp.dot(whole, up_ref[...], preferred_element_type=jnp.float32) * scale
         hidden.append((jax.nn.silu(gate) * upward).astype(jnp.bfloat16))
     copies[2].wait()
@@ -420,7 +421,7 @@
     )
     message, x_conv, b_conv, c_conv = call(
         conv_kernel,
-        [((peers_x, 2 * width + 16, NS), bf16)] + [((length, width), bf16)] * 3,
+        [((peers_x, 2 * width + 8, NS), bf16)] + [((length, width), bf16)] * 3,
         (place, *feeds, even_rim, odd_rim, *filters, cols),
         flops=4_000_000,
         scratch=[pltpu.VMEM((length + 16, width), f32)],
@@ -429,7 +430,7 @@
     seen = lax.all_to_all(message, "x", 0, 0, tiled=True)
     onward, near, ahead = call(
         row_kernel,
-        [((peers_z, width + 16, NS), bf16), ((2, width, NS), f32), ((8, NS), f32)],
+        [((peers_z, width + 8, NS), bf16), ((2, width, NS), f32), ((8, NS), f32)],
         (place, seen),
         smem=1,
     )

time: 167 us -> 167 us (level)
  no operation moved by 1% of the time
where the time goes in v8:
time: 167 us
  blocking collectives  139 us (83%)
  starting transfers between devices  15.6 us (9%)
  Pallas kernels  11.5 us (7%)
    all_to_all x1, blocking collectives, body(): lax.all_to_all(outgoing.reshape(-1, half, width), everyone, 0, 0, tiled=T...  42.8 us
    all_to_all x1, blocking collectives, body(): lax.all_to_all(partial_out.reshape(-1, half, width), everyone, 0, 0, tile...  42.5 us
    all_to_all x1, blocking collectives, body(): got = lax.all_to_all(onward, 'z', 0, 0, tiled=True)  20 us
    all_to_all x1, blocking collectives, body(): columns = lax.all_to_all(copies, 'y', 0, 0, tiled=True)  19 us
    all_to_all x1, blocking collectives, body(): seen = lax.all_to_all(message, 'x', 0, 0, tiled=True)  12.8 us
    pallas_call x8, Pallas kernels, call(): pl.pallas_call(kernel, out_shape=shapes, in_specs=[SMEM] * smem + [HBM] *...  11.5 us
    ppermute x3, starting transfers between devices, swapped(): return lax.ppermute(value, 'c', [(0, 1), (1, 0)])  11.1 us
    ppermute x1, starting transfers between devices, body(): lax.ppermute(even_rim, SP, [p for a, b in pairs[0::2] for p in ((a, b), (...  3.94 us
  transfers between devices with their start and end apart: 5, of which 0 were waited for; matrix products, arithmetic and copies ran while one was open for 0% of the time, Pallas kernels for 1%

profile of v8, /device:TPU:1, one launch (start us, length us, event | category | flops | bytes accessed | tf_op | source)
XLA Modules:
  0.0 166.9 jit_solution(11255061710512394655)
XLA Ops:
  0.0 0.1 pad_add_fusion.place_ref
  0.1 1.4 shard_map.190
  1.5 3.9 %collective-permute-start = (f32[2,384]{1,0:T(2,128)S(1)}, f32[2,384]{1,0:T(2,128)S(1)}, u32[]{:S(2)}, u32[]{:S(2)}) collective-permute-start(f32[2,384]{1,0:T(2,128)S(1)} %get-tuple-element.35), channel_id=1, source_target_pairs={{0,16},{16,0},{32,48},{48,32},{64,80},{80,64},{96,112},{112,96},{1... | collective-permute-start | bytes 9224 | tf_op jit(solution)/shard_map/ppermute | solution.py:394
  5.4 0.7 collective-permute-start.1
  6.1 1.6 shard_map.191
  7.6 0.0 collective-permute-done.even_ref
  7.6 0.0 collective-permute-done.1.odd_ref
  7.7 0.0 copy-start.5
  7.7 0.0 copy-start.7
  7.7 1.1 shard_map.192
  8.8 0.0 copy-start
  8.8 0.0 copy-start.1
  8.8 12.8 %all_to_all.25.seen_ref = bf16[4,264,128]{2,1,0:T(8,128)(2,1)S(1)} all-to-all(bf16[4,264,128]{2,1,0:T(8,128)(2,1)S(1)} %get-tuple-element.41), channel_id=1, replica_groups=mesh['z'=8,'x'=4,'y'=8,'c'=2] {'x'}, dimensions={0} | all-to-all | bytes 540672 | tf_op jit(solution)/shard_map/all_to_all | solution.py:430
  21.6 0.7 shard_map.193
  22.2 20.0 %all_to_all.26.got_ref = bf16[8,136,128]{2,1,0:T(8,128)(2,1)S(1)} all-to-all(bf16[8,136,128]{2,1,0:T(8,128)(2,1)S(1)} %get-tuple-element.42), channel_id=1, replica_groups=mesh['z'=8,'x'=4,'y'=8,'c'=2] {'z'}, dimensions={0} | all-to-all | bytes 557056 | tf_op jit(solution)/shard_map/all_to_all | solution.py:437
  42.3 0.0 copy-done.5
  42.3 0.0 copy-done.7
  42.3 1.4 shard_map.194
  43.6 0.0 copy-done
  43.6 0.0 copy-start.3
  43.7 6.7 %collective-permute-start.2 = (bf16[2048,256]{1,0:T(8,128)(2,1)S(1)}, bf16[2048,256]{1,0:T(8,128)(2,1)S(1)}, u32[]{:S(2)}, u32[]{:S(2)}) collective-permute-start(bf16[2048,256]{1,0:T(8,128)(2,1)S(1)} %bitcast.19), channel_id=1, source_target_pairs={{0,1},{1,0},{2,3},{3,2},{4,5},{5,4},{6,7},{7,6},{8,9},{9,8},{10,11... | collective-permute-start | bytes 3145736 | tf_op jit(solution)/shard_map/ppermute | solution.py:349
  50.4 0.0 copy-done.1
  50.4 1.9 %collective-permute-start.3 = (bf16[2048,256]{1,0:T(8,128)(2,1)S(1)}, bf16[2048,256]{1,0:T(8,128)(2,1)S(1)}, u32[]{:S(2)}, u32[]{:S(2)}) collective-permute-start(bf16[2048,256]{1,0:T(8,128)(2,1)S(1)} %bitcast.21), channel_id=1, source_target_pairs={{0,1},{1,0},{2,3},{3,2},{4,5},{5,4},{6,7},{7,6},{8,9},{9,8},{10,11... | collective-permute-start | bytes 3145736 | tf_op jit(solution)/shard_map/ppermute | solution.py:349
  52.3 2.4 %collective-permute-start.4 = (bf16[256,2048]{1,0:T(8,128)(2,1)}, bf16[256,2048]{1,0:T(8,128)(2,1)S(1)}, u32[]{:S(2)}, u32[]{:S(2)}) collective-permute-start(bf16[256,2048]{1,0:T(8,128)(2,1)} %bitcast.23), channel_id=1, source_target_pairs={{0,1},{1,0},{2,3},{3,2},{4,5},{5,4},{6,7},{7,6},{8,9},{9,8},{10,11... | collective-permute-start | bytes 3145736 | tf_op jit(solution)/shard_map/ppermute | solution.py:349
  54.7 19.0 %all_to_all.27 = bf16[8,128,128]{2,1,0:T(8,128)(2,1)S(1)} all-to-all(bf16[8,128,128]{2,1,0:T(8,128)(2,1)S(1)} %shard_map.194), channel_id=1, replica_groups=mesh['z'=8,'x'=4,'y'=8,'c'=2] {'y'}, dimensions={0} | all-to-all | bytes 524288 | tf_op jit(solution)/shard_map/all_to_all | solution.py:459
  73.7 0.0 copy-start.4
  73.7 0.0 collective-permute-done.2.gate_in
  73.7 0.0 copy-start.8
  73.7 0.0 collective-permute-done.3.up_in
  73.7 0.0 copy-start.9
  73.7 0.0 collective-permute-done.4.down_in
  73.8 0.0 copy-start.10
  73.8 2.3 %all_gather.3.mixed_ref = bf16[8,256,128]{2,1,0:T(8,128)(2,1)S(1)} all-gather(bf16[8,128,128]{2,1,0:T(8,128)(2,1)S(1)} %all_to_all.27), channel_id=1, replica_groups=mesh['z'=8,'x'=4,'y'=8,'c'=2] {'c'}, dimensions={1}, use_global_device_ids=true | all-gather | bytes 786432 | tf_op jit(solution)/shard_map/all_gather | solution.py:463
  76.0 0.0 copy-done.3
  76.0 0.0 copy-done.4
  76.0 0.5 shard_map.195
  76.6 0.0 copy-start.2
  76.6 0.0 copy-start.6
  76.6 42.8 %all_to_all.28 = bf16[512,8,128]{2,1,0:T(8,128)(2,1)S(1)} all-to-all(bf16[512,8,128]{2,1,0:T(8,128)(2,1)S(1)} %bitcast.25), channel_id=1, replica_groups=mesh['z'=8,'x'=4,'y'=8,'c'=2] {'z','x','y','c'}, dimensions={0} | all-to-all | bytes 2097152 | tf_op jit(solution)/shard_map/all_to_all | solution.py:472
  119.4 0.0 copy-done.8
  119.4 0.0 copy-done.9
  119.4 0.0 copy-done.10
  119.4 0.0 copy-done.2
  119.4 0.0 copy-done.6
  119.4 4.0 %shard_map.196 = bf16[32,16,8,128]{3,2,1,0:T(8,128)(2,1)S(1)} custom-call(bf16[2048,256]{1,0:T(8,128)(2,1)} %copy-done.8, bf16[2048,256]{1,0:T(8,128)(2,1)} %copy-done.9, bf16[256,2048]{1,0:T(8,128)(2,1)} %copy-done.10, bf16[32,16,8,128]{3,2,1,0:T(8,128)(2,1)S(1)} %bitcast.16, f32[1,2048]{1,0:T(1,128)S(1)} %bitcast.26, bf16[2048,256]{1,0:T(8,128)(2,1)S(1)} %bitcast.20, ...), custom_call_target="tpu_custom_call" | custom-call | flops 1610612736 | bytes 8396800 | tf_op jit(solution)/shard_map/pallas_call | solution.py:37
  123.5 42.5 %all_to_all.29 = bf16[512,8,128]{2,1,0:T(8,128)(2,1)S(1)} all-to-all(bf16[512,8,128]{2,1,0:T(8,128)(2,1)S(1)} %bitcast.17), channel_id=1, replica_groups=mesh['z'=8,'x'=4,'y'=8,'c'=2] {'z','x','y','c'}, dimensions={0} | all-to-all | bytes 2097152 | tf_op jit(solution)/shard_map/all_to_all | solution.py:493
  166.0 1.0 shard_map.197
Async XLA Ops:
  1.5 6.2 %collective-permute-start = (f32[2,384]{1,0:T(2,128)S(1)}, f32[2,384]{1,0:T(2,128)S(1)}, u32[]{:S(2)}, u32[]{:S(2)}) collective-permute-start(f32[2,384]{1,0:T(2,128)S(1)} %get-tuple-element.35), channel_id=1, source_target_pairs={{0,16},{16,0},{32,48},{48,32},{64,80},{80,64},{96,112},{112,96},{1... | collective-permute-start | bytes 9224 | tf_op jit(solution)/shard_map/ppermute | solution.py:394
  5.4 2.3 %collective-permute-start.1 = (f32[2,384]{1,0:T(2,128)S(1)}, f32[2,384]{1,0:T(2,128)S(1)}, u32[]{:S(2)}, u32[]{:S(2)}) collective-permute-start(f32[2,384]{1,0:T(2,128)S(1)} %get-tuple-element.36), channel_id=1, source_target_pairs={{16,32},{32,16},{48,64},{64,48},{80,96},{96,80},{112,128},{128,112... | collective-permute-start | bytes 9224 | tf_op jit(solution)/shard_map/ppermute | solution.py:395
  7.7 34.6 %copy-start.5 = (bf16[128,128]{1,0:T(8,128)(2,1)S(1)}, bf16[128,128]{1,0:T(8,128)(2,1)}, u32[]{:S(2)}) copy-start(bf16[128,128]{1,0:T(8,128)(2,1)} %valve_ref.1) | copy-start | bytes 98308
  7.7 34.6 %copy-start.7 = (f32[128]{0:T(128)S(1)}, f32[128]{0:T(128)}, u32[]{:S(2)}) copy-start(f32[128]{0:T(128)} %param.31) | copy-start | bytes 1540
  8.8 34.8 %copy-start = (bf16[1,2048,256]{2,1,0:T(8,128)(2,1)S(1)}, bf16[1,2048,256]{2,1,0:T(8,128)(2,1)}, u32[]{:S(2)}) copy-start(bf16[1,2048,256]{2,1,0:T(8,128)(2,1)} %param.37) | copy-start | bytes 3145732
  8.8 41.6 %copy-start.1 = (bf16[1,2048,256]{2,1,0:T(8,128)(2,1)S(1)}, bf16[1,2048,256]{2,1,0:T(8,128)(2,1)}, u32[]{:S(2)}) copy-start(bf16[1,2048,256]{2,1,0:T(8,128)(2,1)} %param.38) | copy-start | bytes 3145732
  43.6 32.4 %copy-start.3 = (bf16[2048,128]{1,0:T(8,128)(2,1)S(1)}, bf16[2048,128]{1,0:T(8,128)(2,1)}, u32[]{:S(2)}) copy-start(bf16[2048,128]{1,0:T(8,128)(2,1)} %weight_ref.1) | copy-start | bytes 1572868
  43.7 30.1 %collective-permute-start.2 = (bf16[2048,256]{1,0:T(8,128)(2,1)S(1)}, bf16[2048,256]{1,0:T(8,128)(2,1)S(1)}, u32[]{:S(2)}, u32[]{:S(2)}) collective-permute-start(bf16[2048,256]{1,0:T(8,128)(2,1)S(1)} %bitcast.19), channel_id=1, source_target_pairs={{0,1},{1,0},{2,3},{3,2},{4,5},{5,4},{6,7},{7,6},{8,9},{9,8},{10,11... | collective-permute-start | bytes 3145736 | tf_op jit(solution)/shard_map/ppermute | solution.py:349
  50.4 23.3 %collective-permute-start.3 = (bf16[2048,256]{1,0:T(8,128)(2,1)S(1)}, bf16[2048,256]{1,0:T(8,128)(2,1)S(1)}, u32[]{:S(2)}, u32[]{:S(2)}) collective-permute-start(bf16[2048,256]{1,0:T(8,128)(2,1)S(1)} %bitcast.21), channel_id=1, source_target_pairs={{0,1},{1,0},{2,3},{3,2},{4,5},{5,4},{6,7},{7,6},{8,9},{9,8},{10,11... | collective-permute-start | bytes 3145736 | tf_op jit(solution)/shard_map/ppermute | solution.py:349
  52.3 21.4 %collective-permute-start.4 = (bf16[256,2048]{1,0:T(8,128)(2,1)}, bf16[256,2048]{1,0:T(8,128)(2,1)S(1)}, u32[]{:S(2)}, u32[]{:S(2)}) collective-permute-start(bf16[256,2048]{1,0:T(8,128)(2,1)} %bitcast.23), channel_id=1, source_target_pairs={{0,1},{1,0},{2,3},{3,2},{4,5},{5,4},{6,7},{7,6},{8,9},{9,8},{10,11... | collective-permute-start | bytes 3145736 | tf_op jit(solution)/shard_map/ppermute | solution.py:349
  73.7 2.3 %copy-start.4 = (bf16[128,128]{1,0:T(8,128)(2,1)S(1)}, bf16[128,128]{1,0:T(8,128)(2,1)}, u32[]{:S(2)}) copy-start(bf16[128,128]{1,0:T(8,128)(2,1)} %skip_ref.1) | copy-start | bytes 98308
  73.7 45.7 %copy-start.8 = (bf16[2048,256]{1,0:T(8,128)(2,1)}, bf16[2048,256]{1,0:T(8,128)(2,1)S(1)}, u32[]{:S(2)}) copy-start(bf16[2048,256]{1,0:T(8,128)(2,1)S(1)} %collective-permute-done.2.gate_in) | copy-start | bytes 3145732
  73.7 45.7 %copy-start.9 = (bf16[2048,256]{1,0:T(8,128)(2,1)}, bf16[2048,256]{1,0:T(8,128)(2,1)S(1)}, u32[]{:S(2)}) copy-start(bf16[2048,256]{1,0:T(8,128)(2,1)S(1)} %collective-permute-done.3.up_in) | copy-start | bytes 3145732
  73.8 45.7 %copy-start.10 = (bf16[256,2048]{1,0:T(8,128)(2,1)}, bf16[256,2048]{1,0:T(8,128)(2,1)S(1)}, u32[]{:S(2)}) copy-start(bf16[256,2048]{1,0:T(8,128)(2,1)S(1)} %collective-permute-done.4.down_in) | copy-start | bytes 3145732
  76.6 42.9 %copy-start.2 = (bf16[1,256,2048]{2,1,0:T(8,128)(2,1)S(1)}, bf16[1,256,2048]{2,1,0:T(8,128)(2,1)}, u32[]{:S(2)}) copy-start(bf16[1,256,2048]{2,1,0:T(8,128)(2,1)} %param.39) | copy-start | bytes 3145732
  76.6 42.9 %copy-start.6 = (f32[2048]{0:T(1024)S(1)}, f32[2048]{0:T(1024)}, u32[]{:S(2)}) copy-start(f32[2048]{0:T(1024)} %param.33) | copy-start | bytes 24580
